TPU v7x, 512 devices: a whole 4x8x8 slice. The times are simulated.
512 devices in a mesh: sp: 64 (over z, y), tp: 8 (over x, core).
Axes of the slice: x: 4, y: 8, z: 8, core: 2. Of those that a mesh axis runs over, the one named last changes fastest.
Arguments:
- hidden_in: bfloat16 [32768, 2048], P('sp'), may hold values from -64 to 64
- pre_gain: float32 [2048], replicated, may hold values from 0.1 to 1.9
- query_proj: bfloat16 [2048, 2048], P(None, 'tp'), may hold values from -2 to 2
- key_proj: bfloat16 [2048, 2048], P('sp', 'tp'), may hold values from -2 to 2
- value_proj: bfloat16 [2048, 2048], P('sp', 'tp'), may hold values from -0.125 to 0.125
- out_proj: bfloat16 [2048, 2048], P('tp'), may hold values from -0.125 to 0.125
- post_gain: float32 [2048], replicated, may hold values from 0.1 to 1.9
Outputs:
- layer_out: bfloat16 [32768, 2048], P(('sp', 'tp'))
- log_weight: float32 [32, 32768], P('tp', 'sp')
All inputs are finite; a program needn't handle non-finite values.
Results may differ from a plain program's by a relative error of at most 0.018.
The roundings to bfloat16 on the way count: a program that leaves them out, or rounds other values in their place, can miss the bound.
Values may be sent and summed in bfloat16 or wider, within the bound.
No kernel may reach another device: no remote copies, remote signals or barrier semaphores. Data moves between devices by JAX's collectives and lax.ppermute only.
A program may use at most 64 MiB of HBM per device.

v0:
```python
import functools

import jax
import jax.numpy as jnp
import numpy as np
from jax import lax
from jax.experimental import pallas as pl
from jax.experimental.pallas import tpu as pltpu
from jax.sharding import Mesh
from jax.sharding import PartitionSpec as P

HEAD_DIM = 64
SPAN = 128
EPS = 1e-06
ROPE_BASE = 10000.0
LOW = -1e30
SP = ("zh", "zl", "y")
Z = ("zh", "zl")
TP = ("x", "c")
F32 = jnp.float32
BF16 = jnp.bfloat16
NT = (((1,), (1,)), ((), ()))
HOPS = (0, 3, 1, 2)


def ring(count, steps):
    return [(i, (i + steps) % count) for i in range(count)]


def natural(i):
    return (i & 31) * 16 + ((i >> 5) & 3) * 4 + (i >> 7)


def to_residue(rows, columns=None):
    i = lax.broadcasted_iota(jnp.int32, (rows, rows), 0)
    if columns is None:
        columns = lax.broadcasted_iota(jnp.int32, (rows, rows), 1)
    return (natural(i) == columns).astype(BF16)


def to_natural(rows):
    i = lax.broadcasted_iota(jnp.int32, (rows, rows), 1)
    n = lax.broadcasted_iota(jnp.int32, (rows, rows), 0)
    return (natural(i) == n).astype(BF16)


def rotated(x, cos, sin):
    width = x.shape[1]
    lane = lax.broadcasted_iota(jnp.int32, x.shape, 1)
    other = jnp.where((lane & 63) < 32, pltpu.roll(x, width - 32, 1), pltpu.roll(x, 32, 1))
    return x * cos + other * sin


def permuted(perm, x):
    return jnp.dot(perm, x, preferred_element_type=F32).astype(BF16)


def normed_rows(x, gain):
    x = x.astype(F32)
    scale = lax.rsqrt(jnp.mean(x * x, axis=1, keepdims=True) + EPS)
    return (x * scale * gain).astype(BF16)


def spread(turn_ref, part):
    cos, sin = turn_ref[0, :, part], turn_ref[1, :, part]
    cos = jnp.concatenate([cos] * 4, axis=0).T
    sin = jnp.concatenate([-sin, sin] * 2, axis=0).T
    return jnp.concatenate([cos, cos], axis=1), jnp.concatenate([sin, sin], axis=1)


def query_kernel(hidden_ref, gain_ref, weight_ref, turn_ref, normed_ref, query_ref):
    rows = hidden_ref.shape[0]
    gain = gain_ref[...]

    def step(i, carry):
        part = pl.ds(pl.multiple_of(i * 64, 64), 64)
        normed_ref[part, :] = normed_rows(hidden_ref[part, :], gain)
        return carry

    lax.fori_loop(0, rows // 64, step, 0)
    query = jnp.dot(normed_ref[...], weight_ref[...], preferred_element_type=F32)
    cos, sin = spread(turn_ref, slice(0, rows))
    query = rotated(query, cos, sin).astype(BF16) * 0.125
    query_ref[...] = permuted(to_residue(rows), query)


def copies_kernel(key_ref, value_ref, out_ref):
    both = jnp.concatenate([key_ref[...], value_ref[...]], axis=1)
    for n in range(out_ref.shape[0]):
        out_ref[n] = both


def assembled(place_ref, mine_ref, below_ref, above_ref, weight_ref, columns):
    low = place_ref[1]
    for k in range(4):
        weight_ref[pl.ds(pl.multiple_of((2 * k + low) * 256, 256), 256), :] = mine_ref[k, :, columns]
    for k in range(2):
        weight_ref[pl.ds(pl.multiple_of((2 * k + 1 - low) * 256, 256), 256), :] = below_ref[k]
        weight_ref[pl.ds(pl.multiple_of((2 * k + 5 - low) * 256, 256), 256), :] = above_ref[k]


def key_kernel(place_ref, normed_ref, mine_ref, below_ref, above_ref, turn_ref, key_ref, weight_ref):
    rows, width = key_ref.shape
    assembled(place_ref, mine_ref, below_ref, above_ref, weight_ref, slice(0, width))
    key = jnp.dot(normed_ref[...], weight_ref[...], preferred_element_type=F32)
    key = rotated(key, *spread(turn_ref, slice(0, rows))).astype(BF16)
    key_ref[...] = permuted(to_residue(rows), key)


def value_kernel(place_ref, normed_ref, mine_ref, below_ref, above_ref, value_ref, weight_ref):
    rows, width = value_ref.shape
    assembled(place_ref, mine_ref, below_ref, above_ref, weight_ref, slice(width, 2 * width))
    value = jnp.dot(normed_ref[...], weight_ref[...], preferred_element_type=F32).astype(BF16)
    value_ref[...] = permuted(to_residue(rows), value)


def stack_heads(q):
    lane = lax.broadcasted_iota(jnp.int32, q.shape, 1) >> 6
    return jnp.concatenate([jnp.where(lane == h, q, jnp.zeros_like(q)) for h in range(q.shape[1] // HEAD_DIM)], axis=0)


def own_heads(stacked):
    width = stacked.shape[1]
    heads = width // HEAD_DIM
    rows = stacked.shape[0] // heads
    lane = lax.broadcasted_iota(jnp.int32, (rows, width), 1) >> 6
    out = stacked[:rows]
    for h in range(1, heads):
        out = jnp.where(lane == h, stacked[h * rows : (h + 1) * rows], out)
    return out


def far_bias(block, back):
    qi = lax.broadcasted_iota(jnp.int32, (128, 128), 0)
    ki = lax.broadcasted_iota(jnp.int32, (128, 128), 1)
    ok = ((qi >> 5) == (ki >> 5)) & (block >= back)
    if back == 4:
        ok = ok & ((ki & 31) >= (qi & 31))
    return jnp.where(ok, 0.0, LOW).astype(F32)


def times_seen(o):
    count = (o <= SPAN).astype(F32)
    count = count + (((o & 3) == 0) & (o <= 4 * SPAN)).astype(F32)
    return count + ((o & 15) == 0).astype(F32)


def query_places(cls):
    i = lax.broadcasted_iota(jnp.int32, (128, 1), 0)
    return (i & 31) * 16 + (i >> 5) * 4 + cls


def own_kernel(q_ref, k_ref, v_ref, max_ref, sum_ref, acc_ref, s_ref, p_ref, bias_ref, count_ref, stat_ref):
    keys, width = k_ref.shape
    heads = width // HEAD_DIM
    o = query_places(pl.program_id(0)) - natural(lax.broadcasted_iota(jnp.int32, (1, keys), 1))
    count = jnp.where(o >= 0, times_seen(o), 0.0)
    count_ref[...] = count
    bias_ref[...] = jnp.where(count > 0, 0.0, LOW).astype(F32)
    s_ref[...] = lax.dot_general(stack_heads(q_ref[...]), k_ref[...], NT, preferred_element_type=F32)
    step = 32
    for r in range(0, heads * 128, step):
        mask = slice(r % 128, r % 128 + step)
        s = s_ref[r : r + step, :] + bias_ref[mask, :]
        m = jnp.max(s, axis=1, keepdims=True)
        p = jnp.exp(s - m) * count_ref[mask, :]
        stat_ref[0, r : r + step, :] = jnp.broadcast_to(m, (step, width))
        stat_ref[1, r : r + step, :] = jnp.broadcast_to(jnp.sum(p, axis=1, keepdims=True), (step, width))
        p_ref[r : r + step, :] = p.astype(BF16)
    pv = jnp.dot(p_ref[...], v_ref[...], preferred_element_type=F32)
    max_ref[...] = own_heads(stat_ref[0])
    sum_ref[...] = own_heads(stat_ref[1])
    acc_ref[...] = own_heads(pv)


def merged(q, key, value, bias, count, max_ref, sum_ref, acc_ref, s_ref, p_ref, stat_ref):
    width = max_ref.shape[1]
    s_ref[...] = lax.dot_general(stack_heads(q), key, NT, preferred_element_type=F32)
    for h in range(width // HEAD_DIM):
        part = slice(h * 128, (h + 1) * 128)
        s = s_ref[part, :] + bias
        m = jnp.maximum(jnp.max(s, axis=1, keepdims=True), max_ref[:, h * HEAD_DIM : h * HEAD_DIM + 1])
        p = jnp.exp(s - m)
        if count is not None:
            p = p * count
        p_ref[part, :] = p.astype(BF16)
        stat_ref[0, part, :] = jnp.broadcast_to(m, (128, width))
        stat_ref[1, part, :] = jnp.broadcast_to(jnp.sum(p, axis=1, keepdims=True), (128, width))
    pv = jnp.dot(p_ref[...], value, preferred_element_type=F32)
    m = own_heads(stat_ref[0])
    alpha = jnp.exp(max_ref[...] - m)
    total = sum_ref[...] * alpha + own_heads(stat_ref[1])
    return m, total, acc_ref[...] * alpha + own_heads(pv)


def before_kernel(place_ref, q_ref, max_ref, sum_ref, acc_ref, k_ref, v_ref, new_max, new_sum, new_acc, s_ref, p_ref, stat_ref, tail_ref):
    cls = pl.program_id(0)
    keys = k_ref.shape[0]
    mine = pl.ds(pl.multiple_of(cls * 128, 128), 128)

    @pl.when(cls == 0)
    def _():
        j = lax.broadcasted_iota(jnp.int32, (128, keys), 0)
        i = lax.broadcasted_iota(jnp.int32, (128, keys), 1)
        pick = (i == (j >> 3) * 32 + 24 + (j & 7)).astype(BF16)
        tail_ref[0] = permuted(pick, k_ref[...])
        tail_ref[1] = permuted(pick, v_ref[...])

    seen = place_ref[0] >= 1
    qn = query_places(cls)
    k = lax.broadcasted_iota(jnp.int32, (1, 128), 1)
    same = times_seen(qn - ((k & 31) * 16 + (k >> 5) * 4 + cls) + keys)
    last = qn - ((24 + (k & 7)) * 16 + ((k >> 3) & 3) * 4 + (k >> 5)) + keys
    last = ((last <= SPAN) & ((k >> 5) != cls)).astype(F32)
    count = jnp.where(seen, jnp.concatenate([same, last], axis=1), 0.0)
    bias = jnp.where(count > 0, 0.0, LOW).astype(F32)
    key = jnp.concatenate([k_ref[mine, :], tail_ref[0]], axis=0)
    value = jnp.concatenate([v_ref[mine, :], tail_ref[1]], axis=0)
    state = merged(q_ref[...], key, value, bias, count, max_ref, sum_ref, acc_ref, s_ref, p_ref, stat_ref)
    for ref, part in zip((new_max, new_sum, new_acc), state):
        ref[...] = part


def far_kernel(backs, last, place_ref, q_ref, max_ref, sum_ref, acc_ref, *refs):
    count = len(backs)
    sources, outs = refs[: 2 * count], refs[2 * count :]
    s_ref, p_ref, stat_ref = outs[-3:]
    bias = jnp.concatenate([far_bias(place_ref[0], back) for back in backs], axis=1)
    key = jnp.concatenate([ref[...] for ref in sources[0::2]], axis=0)
    value = jnp.concatenate([ref[...] for ref in sources[1::2]], axis=0)
    m, total, acc = merged(q_ref[...], key, value, bias, None, max_ref, sum_ref, acc_ref, s_ref, p_ref, stat_ref)
    if last:
        cls = pl.program_id(0)
        out_ref, log_ref, att_ref = outs[:3]
        att_ref[pl.ds(pl.multiple_of(cls * 128, 128), 128), :] = (acc / total).astype(BF16)
        log_ref[...] = m + jnp.log(total)

        @pl.when(cls == pl.num_programs(0) - 1)
        def _():
            out_ref[...] = permuted(to_natural(att_ref.shape[0]), att_ref[...])
    else:
        for ref, part in zip(outs[:3], (m, total, acc)):
            ref[...] = part


def log_kernel(lw_ref, log_ref):
    rows, width = lw_ref.shape
    perm = to_natural(rows)
    rest = lw_ref[...]
    ordered = jnp.zeros((rows, width), F32)
    for _ in range(3):
        piece = rest.astype(BF16)
        rest = rest - piece.astype(F32)
        ordered = ordered + jnp.dot(perm, piece, preferred_element_type=F32)
    flipped = ordered.T
    for head in range(width // HEAD_DIM):
        log_ref[head : head + 1, :] = flipped[head * HEAD_DIM : head * HEAD_DIM + 1, :]


def out_kernel(place_ref, att_ref, *refs):
    weights, (gain_ref, out_ref, sum_ref) = refs[:8], refs[8:]
    x, core = place_ref[2], place_ref[3]
    n = pl.program_id(0)
    columns = weights[0].shape[1]
    total = None
    for half, c in enumerate((core, 1 - core)):
        for k, hop in enumerate(HOPS):
            group = lax.rem(x + hop, 4) * 2 + c
            part = jnp.dot(att_ref[group], weights[half * 4 + k][...], preferred_element_type=F32)
            part = part.astype(BF16).astype(F32)
            total = part if total is None else total + part
    sum_ref[:, pl.ds(pl.multiple_of(n * columns, columns), columns)] = total

    @pl.when(n == pl.num_programs(0) - 1)
    def _():
        summed = sum_ref[...]
        scale = lax.rsqrt(jnp.mean(summed * summed, axis=1, keepdims=True) + EPS)
        out_ref[...] = (summed * scale * gain_ref[...]).astype(BF16)


SMEM = pl.BlockSpec(memory_space=pltpu.SMEM)
VMEM = pl.BlockSpec(memory_space=pltpu.VMEM)


def kernel_call(body, outs, args, flops, limit, scratch=(), **more):
    if "grid_spec" not in more:
        more["scratch_shapes"] = [pltpu.VMEM(s, t) for s, t in scratch]
    if "in_specs" not in more and "grid_spec" not in more:
        more["in_specs"] = [SMEM if a.dtype == jnp.int32 else VMEM for a in args]
        more["out_specs"] = tuple(VMEM for _ in outs)
    data = sum(a.size * a.dtype.itemsize for a in args)
    return pl.pallas_call(
        body,
        out_shape=tuple(jax.ShapeDtypeStruct(s, t) for s, t in outs),
        compiler_params=pltpu.CompilerParams(vmem_limit_bytes=limit * 1024 * 1024),
        cost_estimate=pl.CostEstimate(flops=flops, bytes_accessed=data, transcendentals=0),
        **more,
    )(*args)


def layer(hidden_in, pre_gain, query_proj, key_proj, value_proj, out_proj, post_gain):
    rows, depth = hidden_in.shape
    width = query_proj.shape[1]
    heads = width // HEAD_DIM
    piece = rows // 8
    sp, x, core = lax.axis_index(SP), lax.axis_index("x"), lax.axis_index("c")
    place = jnp.stack([sp, lax.axis_index("zl"), x, core]).astype(jnp.int32)
    gain = pre_gain[None]
    row = (rows, width)

    (copies,) = kernel_call(copies_kernel, [((32, key_proj.shape[0], 2 * width), BF16)], (key_proj, value_proj), 1000, 8)
    mine = lax.all_to_all(copies, ("zh", "y"), split_axis=0, concat_axis=0, tiled=True)
    mine = mine.reshape(4, 256, 2 * width)
    slabs = []
    for columns in (slice(0, width), slice(width, 2 * width)):
        below = lax.ppermute(mine[:2, :, columns], Z, ring(8, 1))
        above = lax.ppermute(mine[2:, :, columns], Z, ring(8, -1))
        slabs.append((mine, below, above))

    groups = [out_proj]
    for steps in (1, -1, 2):
        groups.append(lax.ppermute(out_proj, "x", ring(4, steps)))
    for n in range(4):
        groups.append(lax.ppermute(groups[n], "c", ring(2, 1)))

    quarter = HEAD_DIM // 2
    frequency = ROPE_BASE ** (-(jnp.arange(quarter, dtype=F32) * 2.0 / HEAD_DIM))
    positions = (sp * rows + jnp.arange(rows, dtype=jnp.int32)).astype(F32)
    angles = positions[None, :] * frequency[:, None]
    turns = jnp.stack([jnp.cos(angles), jnp.sin(angles)])

    normed, query = kernel_call(
        query_kernel, [((rows, depth), BF16), (row, BF16)], (hidden_in, gain, query_proj, turns), 2 * rows * depth * width, 12
    )
    weight = [((depth, width), BF16)]
    (key,) = kernel_call(key_kernel, [(row, BF16)], (place, normed, *slabs[0], turns), 2 * rows * depth * width, 14, weight)
    (value,) = kernel_call(value_kernel, [(row, BF16)], (place, normed, *slabs[1]), 2 * rows * depth * width, 14, weight)
    forward = [(i, i + 1) for i in range(63)]
    keys, values = [key], [value]
    for _ in range(1, 5):
        keys.append(lax.ppermute(keys[-1], SP, forward))
        values.append(lax.ppermute(values[-1], SP, forward))
    whole = pl.BlockSpec(row, lambda c: (0, 0))
    part = pl.BlockSpec((128, width), lambda c: (c, 0))
    pair = ((512, 256), F32), ((512, 256), BF16), ((2, 512, width), F32)
    state = kernel_call(
        own_kernel,
        [(row, F32)] * 3,
        (query, keys[0], values[0]),
        8 * rows * rows * width,
        10,
        [((512, 512), F32), ((512, 512), BF16), ((128, 512), F32), ((128, 512), F32), ((2, 512, width), F32)],
        grid=(rows // 128,),
        in_specs=[part, whole, whole],
        out_specs=(part,) * 3,
    )
    state = kernel_call(
        before_kernel,
        [(row, F32)] * 3,
        (place, query, *state, keys[1], values[1]),
        4 * rows * rows * width,
        10,
        [*pair, ((2, 128, width), BF16)],
        grid=(rows // 128,),
        in_specs=[SMEM] + [part] * 4 + [whole, whole],
        out_specs=(part,) * 3,
    )
    for back in (2, 3, 4):
        last = back == 4
        state = kernel_call(
            functools.partial(far_kernel, (back,), last),
            [(row, BF16), (row, F32)] if last else [(row, F32)] * 3,
            (place, query, *state, keys[back], values[back]),
            4 * rows * 512 * width,
            16,
            ([(row, BF16)] if last else []) + [((512, 128), t) for t in (F32, BF16)] + [((2, 512, width), F32)],
            grid=(rows // 128,),
            in_specs=[SMEM] + [part] * 6,
            out_specs=(whole, part) if last else (part,) * 3,
        )
    attended, logs = state

    arrived = lax.all_to_all(attended.reshape(8, piece, width), TP, split_axis=0, concat_axis=0, tiled=True)
    (log_weight,) = kernel_call(log_kernel, [((heads, rows), F32)], (logs,), 6 * rows * rows * width, 8)
    columns = depth // 4
    (layer_out,) = kernel_call(
        out_kernel,
        [((piece, depth), BF16)],
        (place, arrived, *groups, post_gain[None]),
        2 * piece * depth * depth,
        12,
        [((piece, depth), F32)],
        grid=(4,),
        in_specs=[SMEM, pl.BlockSpec((8, piece, width), lambda n: (0, 0, 0))]
        + [pl.BlockSpec((width, columns), lambda n: (0, n))] * 8
        + [pl.BlockSpec((1, depth), lambda n: (0, 0))],
        out_specs=(pl.BlockSpec((piece, depth), lambda n: (0, 0)),),
    )
    return layer_out, log_weight


def solution(mesh):
    fine = Mesh(np.asarray(mesh.devices).reshape(4, 2, 8, 4, 2), ("zh", "zl", "y", "x", "c"))
    placed = (P(SP, None), P(), P(None, TP), P(SP, TP), P(SP, TP), P(TP, None), P())
    return jax.shard_map(
        layer,
        mesh=fine,
        in_specs=placed,
        out_specs=(P(SP + TP, None), P(TP, SP)),
        check_vma=False,
    )
```

profile of v0, /device:TPU:24, one launch (start us, length us, event | category | flops | bytes accessed | tf_op | source)
XLA Modules:
  0.0 171.1 jit_solution(14463464603083085466)
XLA Ops:
  0.6 0.7 copy-done.4
  1.4 0.7 copy-done.5
  2.1 1.1 shard_map.87
  3.2 16.1 %all-to-all-start = ((bf16[32,32,512]{2,1,0:T(8,128)(2,1)}), bf16[32,32,512]{2,1,0:T(8,128)(2,1)S(1)}, u32[]{:S(2)}, u32[]{:S(2)}) async-start(bf16[32,32,512]{2,1,0:T(8,128)(2,1)} %shard_map.87), calls=%async_computation | async-start | bytes 2097152 | tf_op jit(solution)/shard_map/all_to_all | solution.py:312
  19.3 3.4 %collective-permute-start.12 = (bf16[256,2048]{1,0:T(8,128)(2,1)}, bf16[256,2048]{1,0:T(8,128)(2,1)}, u32[]{:S(2)}, u32[]{:S(2)}) collective-permute-start(bf16[256,2048]{1,0:T(8,128)(2,1)} %refs_0_.1), channel_id=1, source_target_pairs={{0,2},{2,4},{4,6},{6,0},{1,3},{3,5},{5,7},{7,1},{8,10},{10,12},{12... | collective-permute-start | bytes 3145736 | tf_op jit(solution)/shard_map/ppermute | solution.py:322
  22.7 3.7 %collective-permute-start.13 = (bf16[256,2048]{1,0:T(8,128)(2,1)}, bf16[256,2048]{1,0:T(8,128)(2,1)}, u32[]{:S(2)}, u32[]{:S(2)}) collective-permute-start(bf16[256,2048]{1,0:T(8,128)(2,1)} %refs_0_.1), channel_id=1, source_target_pairs={{0,6},{2,0},{4,2},{6,4},{1,7},{3,1},{5,3},{7,5},{8,14},{10,8},{12,... | collective-permute-start | bytes 3145736 | tf_op jit(solution)/shard_map/ppermute | solution.py:322
  26.4 3.7 %collective-permute-start.14 = (bf16[256,2048]{1,0:T(8,128)(2,1)}, bf16[256,2048]{1,0:T(8,128)(2,1)}, u32[]{:S(2)}, u32[]{:S(2)}) collective-permute-start(bf16[256,2048]{1,0:T(8,128)(2,1)} %refs_0_.1), channel_id=1, source_target_pairs={{0,4},{2,6},{4,0},{6,2},{1,5},{3,7},{5,1},{7,3},{8,12},{10,14},{12... | collective-permute-start | bytes 3145736 | tf_op jit(solution)/shard_map/ppermute | solution.py:322
  30.1 19.3 %all-to-all-done = bf16[32,32,512]{2,1,0:T(8,128)(2,1)S(1)} async-done(((bf16[32,32,512]{2,1,0:T(8,128)(2,1)}), bf16[32,32,512]{2,1,0:T(8,128)(2,1)S(1)}, u32[]{:S(2)}, u32[]{:S(2)}) %all-to-all-start) | async-done | bytes 1048608 | tf_op jit(solution)/shard_map/all_to_all | solution.py:312
  49.5 1.0 fusion
  50.5 4.1 %collective-permute-start = (bf16[2,256,256]{2,1,0:T(8,128)(2,1)}, bf16[2,256,256]{2,1,0:T(8,128)(2,1)S(1)}, u32[]{:S(2)}, u32[]{:S(2)}) collective-permute-start(bf16[2,256,256]{2,1,0:T(8,128)(2,1)} %get-tuple-element.37), channel_id=1, source_target_pairs={{0,64},{64,128},{128,192},{192,256},{256,320},{320,384},{384,448},... | collective-permute-start | bytes 786440 | tf_op jit(solution)/shard_map/ppermute | solution.py:316
  54.5 3.0 %collective-permute-start.1 = (bf16[2,256,256]{2,1,0:T(8,128)(2,1)}, bf16[2,256,256]{2,1,0:T(8,128)(2,1)}, u32[]{:S(2)}, u32[]{:S(2)}) collective-permute-start(bf16[2,256,256]{2,1,0:T(8,128)(2,1)} %get-tuple-element.36), channel_id=1, source_target_pairs={{0,448},{64,0},{128,64},{192,128},{256,192},{320,256},{384,320},{4... | collective-permute-start | bytes 786440 | tf_op jit(solution)/shard_map/ppermute | solution.py:317
  57.5 0.3 multiply_cosine_fusion
  57.8 2.3 %collective-permute-done.below_ref = bf16[2,256,256]{2,1,0:T(8,128)(2,1)S(1)} collective-permute-done((bf16[2,256,256]{2,1,0:T(8,128)(2,1)}, bf16[2,256,256]{2,1,0:T(8,128)(2,1)S(1)}, u32[]{:S(2)}, u32[]{:S(2)}) %collective-permute-start) | collective-permute-done | bytes 262176 | tf_op jit(solution)/shard_map/ppermute | solution.py:316
  60.1 2.9 %collective-permute-start.2 = (bf16[2,256,256]{2,1,0:T(8,128)(2,1)}, bf16[2,256,256]{2,1,0:T(8,128)(2,1)S(1)}, u32[]{:S(2)}, u32[]{:S(2)}) collective-permute-start(bf16[2,256,256]{2,1,0:T(8,128)(2,1)} %get-tuple-element.35), channel_id=1, source_target_pairs={{0,64},{64,128},{128,192},{192,256},{256,320},{320,384},{384,448},... | collective-permute-start | bytes 786440 | tf_op jit(solution)/shard_map/ppermute | solution.py:316
  63.0 0.1 pad_add_fusion.place_ref
  63.1 0.2 collective-permute-done.1.above_ref
  63.3 4.0 %collective-permute-start.3 = (bf16[2,256,256]{2,1,0:T(8,128)(2,1)}, bf16[2,256,256]{2,1,0:T(8,128)(2,1)S(1)}, u32[]{:S(2)}, u32[]{:S(2)}) collective-permute-start(bf16[2,256,256]{2,1,0:T(8,128)(2,1)} %get-tuple-element.34), channel_id=1, source_target_pairs={{0,448},{64,0},{128,64},{192,128},{256,192},{320,256},{384,320},{4... | collective-permute-start | bytes 786440 | tf_op jit(solution)/shard_map/ppermute | solution.py:317
  67.3 0.0 copy-start.1
  67.3 1.2 copy-done.1
  68.6 2.7 %shard_map.86 = (bf16[512,2048]{1,0:T(8,128)(2,1)S(1)}, bf16[512,256]{1,0:T(8,128)(2,1)S(1)}) custom-call(bf16[512,2048]{1,0:T(8,128)(2,1)S(1)} %copy-done, f32[1,2048]{1,0:T(1,128)S(1)} %bitcast.12, bf16[2048,256]{1,0:T(8,128)(2,1)S(1)} %copy-done.1, f32[2,32,512]{2,1,0:T(8,128)S(1)} %pad_maximum_fusion.turn_ref), custom_call_target="tpu_custom_call" | custom-call | flops 536870912 | bytes 3284992 | tf_op jit(solution)/shard_map/pallas_call | solution.py:292
  71.3 2.4 %shard_map.88.k_ref = bf16[512,256]{1,0:T(8,128)(2,1)S(1)} custom-call(s32[4]{0:T(128)S(1)} %pad_add_fusion.place_ref, bf16[512,2048]{1,0:T(8,128)(2,1)S(1)} %get-tuple-element.19.normed_ref, bf16[4,256,512]{2,1,0:T(8,128)(2,1)S(1)} %bitcast.9, bf16[2,256,256]{2,1,0:T(8,128)(2,1)S(1)} %collective-permute-done.below_ref, ...), custom_call_target="tpu_custom_call" | custom-call | flops 536870912 | bytes 3801104 | tf_op jit(solution)/shard_map/pallas_call | solution.py:292
  73.7 0.0 copy-start.2
  73.7 0.0 collective-permute-done.2.below_ref
  73.7 3.1 %collective-permute-start.4 = (bf16[512,256]{1,0:T(8,128)(2,1)S(1)}, bf16[512,256]{1,0:T(8,128)(2,1)S(1)}, u32[]{:S(2)}, u32[]{:S(2)}) collective-permute-start(bf16[512,256]{1,0:T(8,128)(2,1)S(1)} %shard_map.88.k_ref), channel_id=1, source_target_pairs={{0,8},{8,16},{16,24},{24,32},{32,40},{40,48},{48,56},{56,64},{64,7... | collective-permute-start | bytes 786440 | tf_op jit(solution)/shard_map/ppermute | solution.py:341
  76.8 0.0 collective-permute-done.3.above_ref
  76.8 1.8 %shard_map.89.v_ref = bf16[512,256]{1,0:T(8,128)(2,1)S(1)} custom-call(s32[4]{0:T(128)S(1)} %pad_add_fusion.place_ref, bf16[512,2048]{1,0:T(8,128)(2,1)S(1)} %get-tuple-element.19.normed_ref, bf16[4,256,512]{2,1,0:T(8,128)(2,1)S(1)} %bitcast.10, bf16[2,256,256]{2,1,0:T(8,128)(2,1)S(1)} %collective-permute-done.2.below_ref, ...), custom_call_target="tpu_custom_call" | custom-call | flops 536870912 | bytes 3670032 | tf_op jit(solution)/shard_map/pallas_call | solution.py:292
  78.6 2.4 %collective-permute-start.5 = (bf16[512,256]{1,0:T(8,128)(2,1)S(1)}, bf16[512,256]{1,0:T(8,128)(2,1)S(1)}, u32[]{:S(2)}, u32[]{:S(2)}) collective-permute-start(bf16[512,256]{1,0:T(8,128)(2,1)S(1)} %shard_map.89.v_ref), channel_id=1, source_target_pairs={{0,8},{8,16},{16,24},{24,32},{32,40},{40,48},{48,56},{56,64},{64,7... | collective-permute-start | bytes 786440 | tf_op jit(solution)/shard_map/ppermute | solution.py:342
  81.0 3.0 %collective-permute-done.4.k_ref = bf16[512,256]{1,0:T(8,128)(2,1)S(1)} collective-permute-done((bf16[512,256]{1,0:T(8,128)(2,1)S(1)}, bf16[512,256]{1,0:T(8,128)(2,1)S(1)}, u32[]{:S(2)}, u32[]{:S(2)}) %collective-permute-start.4) | collective-permute-done | bytes 262176 | tf_op jit(solution)/shard_map/ppermute | solution.py:341
  84.0 4.9 %collective-permute-start.6 = (bf16[512,256]{1,0:T(8,128)(2,1)S(1)}, bf16[512,256]{1,0:T(8,128)(2,1)S(1)}, u32[]{:S(2)}, u32[]{:S(2)}) collective-permute-start(bf16[512,256]{1,0:T(8,128)(2,1)S(1)} %collective-permute-done.4.k_ref), channel_id=1, source_target_pairs={{0,8},{8,16},{16,24},{24,32},{32,40},{40,48},{48,56},{56,64},{64,7... | collective-permute-start | bytes 786440 | tf_op jit(solution)/shard_map/ppermute | solution.py:341
  88.9 0.8 collective-permute-done.5.v_ref
  89.6 4.9 %collective-permute-start.7 = (bf16[512,256]{1,0:T(8,128)(2,1)S(1)}, bf16[512,256]{1,0:T(8,128)(2,1)S(1)}, u32[]{:S(2)}, u32[]{:S(2)}) collective-permute-start(bf16[512,256]{1,0:T(8,128)(2,1)S(1)} %collective-permute-done.5.v_ref), channel_id=1, source_target_pairs={{0,8},{8,16},{16,24},{24,32},{32,40},{40,48},{48,56},{56,64},{64,7... | collective-permute-start | bytes 786440 | tf_op jit(solution)/shard_map/ppermute | solution.py:342
  94.5 0.8 collective-permute-done.6.refs_0_
  95.3 5.6 %collective-permute-start.8 = (bf16[512,256]{1,0:T(8,128)(2,1)S(1)}, bf16[512,256]{1,0:T(8,128)(2,1)S(1)}, u32[]{:S(2)}, u32[]{:S(2)}) collective-permute-start(bf16[512,256]{1,0:T(8,128)(2,1)S(1)} %collective-permute-done.6.refs_0_), channel_id=1, source_target_pairs={{0,8},{8,16},{16,24},{24,32},{32,40},{40,48},{48,56},{56,64},{64,7... | collective-permute-start | bytes 786440 | tf_op jit(solution)/shard_map/ppermute | solution.py:341
  100.9 0.0 collective-permute-done.12.refs_1_
  101.0 1.9 %collective-permute-start.15 = (bf16[256,2048]{1,0:T(8,128)(2,1)S(1)}, bf16[256,2048]{1,0:T(8,128)(2,1)S(1)}, u32[]{:S(2)}, u32[]{:S(2)}) collective-permute-start(bf16[256,2048]{1,0:T(8,128)(2,1)S(1)} %copy-done.2), channel_id=1, source_target_pairs={{0,1},{1,0},{2,3},{3,2},{4,5},{5,4},{6,7},{7,6},{8,9},{9,8},{10,11... | collective-permute-start | bytes 3145736 | tf_op jit(solution)/shard_map/ppermute | solution.py:324
  102.9 0.0 collective-permute-done.13.refs_2_
  102.9 2.4 %collective-permute-start.16 = (bf16[256,2048]{1,0:T(8,128)(2,1)}, bf16[256,2048]{1,0:T(8,128)(2,1)S(1)}, u32[]{:S(2)}, u32[]{:S(2)}) collective-permute-start(bf16[256,2048]{1,0:T(8,128)(2,1)} %collective-permute-done.12.refs_1_), channel_id=1, source_target_pairs={{0,1},{1,0},{2,3},{3,2},{4,5},{5,4},{6,7},{7,6},{8,9},{9,8},{10,11... | collective-permute-start | bytes 3145736 | tf_op jit(solution)/shard_map/ppermute | solution.py:324
  105.3 0.0 collective-permute-done.14.refs_3_
  105.3 1.9 %collective-permute-start.17 = (bf16[256,2048]{1,0:T(8,128)(2,1)}, bf16[256,2048]{1,0:T(8,128)(2,1)}, u32[]{:S(2)}, u32[]{:S(2)}) collective-permute-start(bf16[256,2048]{1,0:T(8,128)(2,1)} %collective-permute-done.13.refs_2_), channel_id=1, source_target_pairs={{0,1},{1,0},{2,3},{3,2},{4,5},{5,4},{6,7},{7,6},{8,9},{9,8},{10,11... | collective-permute-start | bytes 3145736 | tf_op jit(solution)/shard_map/ppermute | solution.py:324
  107.3 0.0 collective-permute-done.7.refs_1_
  107.3 2.4 %collective-permute-start.18 = (bf16[256,2048]{1,0:T(8,128)(2,1)}, bf16[256,2048]{1,0:T(8,128)(2,1)}, u32[]{:S(2)}, u32[]{:S(2)}) collective-permute-start(bf16[256,2048]{1,0:T(8,128)(2,1)} %collective-permute-done.14.refs_3_), channel_id=1, source_target_pairs={{0,1},{1,0},{2,3},{3,2},{4,5},{5,4},{6,7},{7,6},{8,9},{9,8},{10,11... | collective-permute-start | bytes 3145736 | tf_op jit(solution)/shard_map/ppermute | solution.py:324
  109.7 0.0 collective-permute-done.8.refs_0_
  109.7 1.9 %collective-permute-start.9 = (bf16[512,256]{1,0:T(8,128)(2,1)S(1)}, bf16[512,256]{1,0:T(8,128)(2,1)S(1)}, u32[]{:S(2)}, u32[]{:S(2)}) collective-permute-start(bf16[512,256]{1,0:T(8,128)(2,1)S(1)} %collective-permute-done.7.refs_1_), channel_id=1, source_target_pairs={{0,8},{8,16},{16,24},{24,32},{32,40},{40,48},{48,56},{56,64},{64,7... | collective-permute-start | bytes 786440 | tf_op jit(solution)/shard_map/ppermute | solution.py:342
  111.6 8.2 %collective-permute-done.9.refs_1_ = bf16[512,256]{1,0:T(8,128)(2,1)S(1)} collective-permute-done((bf16[512,256]{1,0:T(8,128)(2,1)S(1)}, bf16[512,256]{1,0:T(8,128)(2,1)S(1)}, u32[]{:S(2)}, u32[]{:S(2)}) %collective-permute-start.9) | collective-permute-done | bytes 262176 | tf_op jit(solution)/shard_map/ppermute | solution.py:342
  119.8 3.4 %collective-permute-start.10 = (bf16[512,256]{1,0:T(8,128)(2,1)S(1)}, bf16[512,256]{1,0:T(8,128)(2,1)S(1)}, u32[]{:S(2)}, u32[]{:S(2)}) collective-permute-start(bf16[512,256]{1,0:T(8,128)(2,1)S(1)} %collective-permute-done.8.refs_0_), channel_id=1, source_target_pairs={{0,8},{8,16},{16,24},{24,32},{32,40},{40,48},{48,56},{56,64},{64,7... | collective-permute-start | bytes 786440 | tf_op jit(solution)/shard_map/ppermute | solution.py:341
  123.2 5.8 %collective-permute-done.10.refs_0_ = bf16[512,256]{1,0:T(8,128)(2,1)S(1)} collective-permute-done((bf16[512,256]{1,0:T(8,128)(2,1)S(1)}, bf16[512,256]{1,0:T(8,128)(2,1)S(1)}, u32[]{:S(2)}, u32[]{:S(2)}) %collective-permute-start.10) | collective-permute-done | bytes 262176 | tf_op jit(solution)/shard_map/ppermute | solution.py:341
  129.1 4.9 %collective-permute-start.11 = (bf16[512,256]{1,0:T(8,128)(2,1)S(1)}, bf16[512,256]{1,0:T(8,128)(2,1)S(1)}, u32[]{:S(2)}, u32[]{:S(2)}) collective-permute-start(bf16[512,256]{1,0:T(8,128)(2,1)S(1)} %collective-permute-done.9.refs_1_), channel_id=1, source_target_pairs={{0,8},{8,16},{16,24},{24,32},{32,40},{40,48},{48,56},{56,64},{64,7... | collective-permute-start | bytes 786440 | tf_op jit(solution)/shard_map/ppermute | solution.py:342
  134.0 3.5 %shard_map.90 = (f32[512,256]{1,0:T(8,128)S(1)}, f32[512,256]{1,0:T(8,128)S(1)}, f32[512,256]{1,0:T(8,128)S(1)}) custom-call(bf16[512,256]{1,0:T(8,128)(2,1)S(1)} %get-tuple-element.18.q_ref, bf16[512,256]{1,0:T(8,128)(2,1)S(1)} %shard_map.88.k_ref, bf16[512,256]{1,0:T(8,128)(2,1)S(1)} %shard_map.89.v_ref), custom_call_target="tpu_custom_call" | custom-call | flops 536870912 | bytes 786432 | tf_op jit(solution)/shard_map/pallas_call | solution.py:292
  137.5 4.1 %shard_map.91 = (f32[512,256]{1,0:T(8,128)S(1)}, f32[512,256]{1,0:T(8,128)S(1)}, f32[512,256]{1,0:T(8,128)S(1)}) custom-call(s32[4]{0:T(128)S(1)} %pad_add_fusion.place_ref, bf16[512,256]{1,0:T(8,128)(2,1)S(1)} %get-tuple-element.18.q_ref, f32[512,256]{1,0:T(8,128)S(1)} %get-tuple-element.20.max_ref, f32[512,256]{1,0:T(8,128)S(1)} %get-tuple-element.21.sum_ref, ...), custom_call_target="tpu_custom_call" | custom-call | flops 268435456 | bytes 2359312 | tf_op jit(solution)/shard_map/pallas_call | solution.py:292
  141.6 3.6 %shard_map.92 = (f32[512,256]{1,0:T(8,128)S(1)}, f32[512,256]{1,0:T(8,128)S(1)}, f32[512,256]{1,0:T(8,128)S(1)}) custom-call(s32[4]{0:T(128)S(1)} %pad_add_fusion.place_ref, bf16[512,256]{1,0:T(8,128)(2,1)S(1)} %get-tuple-element.18.q_ref, f32[512,256]{1,0:T(8,128)S(1)} %get-tuple-element.23.max_ref, f32[512,256]{1,0:T(8,128)S(1)} %get-tuple-element.24.sum_ref, ...), custom_call_target="tpu_custom_call" | custom-call | flops 268435456 | bytes 2359312 | tf_op jit(solution)/shard_map/pallas_call | solution.py:292
  145.2 3.6 %shard_map.93 = (f32[512,256]{1,0:T(8,128)S(1)}, f32[512,256]{1,0:T(8,128)S(1)}, f32[512,256]{1,0:T(8,128)S(1)}) custom-call(s32[4]{0:T(128)S(1)} %pad_add_fusion.place_ref, bf16[512,256]{1,0:T(8,128)(2,1)S(1)} %get-tuple-element.18.q_ref, f32[512,256]{1,0:T(8,128)S(1)} %get-tuple-element.26.max_ref, f32[512,256]{1,0:T(8,128)S(1)} %get-tuple-element.27.sum_ref, ...), custom_call_target="tpu_custom_call" | custom-call | flops 268435456 | bytes 2359312 | tf_op jit(solution)/shard_map/pallas_call | solution.py:292
  148.8 0.0 collective-permute-done.11.refs_1_
  148.8 0.0 copy-start.7
  148.8 3.9 %shard_map.94 = (bf16[512,256]{1,0:T(8,128)(2,1)S(1)}, f32[512,256]{1,0:T(8,128)S(1)}) custom-call(s32[4]{0:T(128)S(1)} %pad_add_fusion.place_ref, bf16[512,256]{1,0:T(8,128)(2,1)S(1)} %get-tuple-element.18.q_ref, f32[512,256]{1,0:T(8,128)S(1)} %get-tuple-element.29.max_ref, f32[512,256]{1,0:T(8,128)S(1)} %get-tuple-element.30.sum_ref, ...), custom_call_target="tpu_custom_call" | custom-call | flops 268435456 | bytes 2359312 | tf_op jit(solution)/shard_map/pallas_call | solution.py:292
  152.7 0.8 copy-done.8
  153.5 0.7 copy-done.3
  154.2 4.3 %all-to-all-start.1 = ((bf16[8,64,256]{2,1,0:T(8,128)(2,1)}), bf16[8,64,256]{2,1,0:T(8,128)(2,1)S(1)}, u32[]{:S(2)}, u32[]{:S(2)}) async-start(bf16[8,64,256]{2,1,0:T(8,128)(2,1)} %bitcast.11), calls=%async_computation.1 | async-start | bytes 524288 | tf_op jit(solution)/shard_map/all_to_all | solution.py:383
  158.5 1.0 copy-done.9
  159.5 1.3 shard_map.96
  160.8 0.0 collective-permute-done.15.refs_4_
  160.8 0.0 collective-permute-done.16.refs_5_
  160.8 0.0 collective-permute-done.18.refs_7_
  160.8 5.2 %all-to-all-done.1.att_ref = bf16[8,64,256]{2,1,0:T(8,128)(2,1)S(1)} async-done(((bf16[8,64,256]{2,1,0:T(8,128)(2,1)}), bf16[8,64,256]{2,1,0:T(8,128)(2,1)S(1)}, u32[]{:S(2)}, u32[]{:S(2)}) %all-to-all-start.1) | async-done | bytes 262176 | tf_op jit(solution)/shard_map/all_to_all | solution.py:383
  166.0 5.1 %shard_map.95 = bf16[64,2048]{1,0:T(8,128)(2,1)} custom-call(s32[4]{0:T(128)S(1)} %pad_add_fusion.place_ref, bf16[8,64,256]{2,1,0:T(8,128)(2,1)S(1)} %all-to-all-done.1.att_ref, bf16[256,2048]{1,0:T(8,128)(2,1)S(1)} %copy-done.2, bf16[256,2048]{1,0:T(8,128)(2,1)} %collective-permute-done.12.refs_1_, bf16[256,2048]{1,0:T(8,128)(2,1)} %collective-permute-done.13.refs_2_, ...), custom_call_target="tpu_custom_call" | custom-call | flops 536870912 | bytes 8658960 | tf_op jit(solution)/shard_map/pallas_call | solution.py:292
  (15 shorter events, 0.0 us)
Async XLA Ops:
  0.6 0.7 copy-start.4
  1.3 0.7 copy-start.5
  3.2 64.1 %copy-start = (bf16[512,2048]{1,0:T(8,128)(2,1)S(1)}, bf16[512,2048]{1,0:T(8,128)(2,1)}, u32[]{:S(2)}) copy-start(bf16[512,2048]{1,0:T(8,128)(2,1)} %hidden_ref.1) | copy-start | bytes 6291460
  3.2 64.1 %copy-start.6 = (f32[2048]{0:T(1024)S(1)}, f32[2048]{0:T(1024)}, u32[]{:S(2)}) copy-start(f32[2048]{0:T(1024)} %param.8) | copy-start | bytes 24580
  3.2 46.3 %all-to-all-start = ((bf16[32,32,512]{2,1,0:T(8,128)(2,1)}), bf16[32,32,512]{2,1,0:T(8,128)(2,1)S(1)}, u32[]{:S(2)}, u32[]{:S(2)}) async-start(bf16[32,32,512]{2,1,0:T(8,128)(2,1)} %shard_map.87), calls=%async_computation | async-start | bytes 2097152 | tf_op jit(solution)/shard_map/all_to_all | solution.py:312
  19.3 81.7 %collective-permute-start.12 = (bf16[256,2048]{1,0:T(8,128)(2,1)}, bf16[256,2048]{1,0:T(8,128)(2,1)}, u32[]{:S(2)}, u32[]{:S(2)}) collective-permute-start(bf16[256,2048]{1,0:T(8,128)(2,1)} %refs_0_.1), channel_id=1, source_target_pairs={{0,2},{2,4},{4,6},{6,0},{1,3},{3,5},{5,7},{7,1},{8,10},{10,12},{12... | collective-permute-start | bytes 3145736 | tf_op jit(solution)/shard_map/ppermute | solution.py:322
  22.7 80.2 %collective-permute-start.13 = (bf16[256,2048]{1,0:T(8,128)(2,1)}, bf16[256,2048]{1,0:T(8,128)(2,1)}, u32[]{:S(2)}, u32[]{:S(2)}) collective-permute-start(bf16[256,2048]{1,0:T(8,128)(2,1)} %refs_0_.1), channel_id=1, source_target_pairs={{0,6},{2,0},{4,2},{6,4},{1,7},{3,1},{5,3},{7,5},{8,14},{10,8},{12,... | collective-permute-start | bytes 3145736 | tf_op jit(solution)/shard_map/ppermute | solution.py:322
  26.4 79.0 %collective-permute-start.14 = (bf16[256,2048]{1,0:T(8,128)(2,1)}, bf16[256,2048]{1,0:T(8,128)(2,1)}, u32[]{:S(2)}, u32[]{:S(2)}) collective-permute-start(bf16[256,2048]{1,0:T(8,128)(2,1)} %refs_0_.1), channel_id=1, source_target_pairs={{0,4},{2,6},{4,0},{6,2},{1,5},{3,7},{5,1},{7,3},{8,12},{10,14},{12... | collective-permute-start | bytes 3145736 | tf_op jit(solution)/shard_map/ppermute | solution.py:322
  50.5 9.7 %collective-permute-start = (bf16[2,256,256]{2,1,0:T(8,128)(2,1)}, bf16[2,256,256]{2,1,0:T(8,128)(2,1)S(1)}, u32[]{:S(2)}, u32[]{:S(2)}) collective-permute-start(bf16[2,256,256]{2,1,0:T(8,128)(2,1)} %get-tuple-element.37), channel_id=1, source_target_pairs={{0,64},{64,128},{128,192},{192,256},{256,320},{320,384},{384,448},... | collective-permute-start | bytes 786440 | tf_op jit(solution)/shard_map/ppermute | solution.py:316
  54.5 8.8 %collective-permute-start.1 = (bf16[2,256,256]{2,1,0:T(8,128)(2,1)}, bf16[2,256,256]{2,1,0:T(8,128)(2,1)}, u32[]{:S(2)}, u32[]{:S(2)}) collective-permute-start(bf16[2,256,256]{2,1,0:T(8,128)(2,1)} %get-tuple-element.36), channel_id=1, source_target_pairs={{0,448},{64,0},{128,64},{192,128},{256,192},{320,256},{384,320},{4... | collective-permute-start | bytes 786440 | tf_op jit(solution)/shard_map/ppermute | solution.py:317
  60.1 13.5 %collective-permute-start.2 = (bf16[2,256,256]{2,1,0:T(8,128)(2,1)}, bf16[2,256,256]{2,1,0:T(8,128)(2,1)S(1)}, u32[]{:S(2)}, u32[]{:S(2)}) collective-permute-start(bf16[2,256,256]{2,1,0:T(8,128)(2,1)} %get-tuple-element.35), channel_id=1, source_target_pairs={{0,64},{64,128},{128,192},{192,256},{256,320},{320,384},{384,448},... | collective-permute-start | bytes 786440 | tf_op jit(solution)/shard_map/ppermute | solution.py:316
  63.3 13.5 %collective-permute-start.3 = (bf16[2,256,256]{2,1,0:T(8,128)(2,1)}, bf16[2,256,256]{2,1,0:T(8,128)(2,1)S(1)}, u32[]{:S(2)}, u32[]{:S(2)}) collective-permute-start(bf16[2,256,256]{2,1,0:T(8,128)(2,1)} %get-tuple-element.34), channel_id=1, source_target_pairs={{0,448},{64,0},{128,64},{192,128},{256,192},{320,256},{384,320},{4... | collective-permute-start | bytes 786440 | tf_op jit(solution)/shard_map/ppermute | solution.py:317
  67.3 1.2 copy-start.1
  73.7 27.3 %copy-start.2 = (bf16[256,2048]{1,0:T(8,128)(2,1)S(1)}, bf16[256,2048]{1,0:T(8,128)(2,1)}, u32[]{:S(2)}) copy-start(bf16[256,2048]{1,0:T(8,128)(2,1)} %refs_0_.1) | copy-start | bytes 3145732
  73.7 10.3 %collective-permute-start.4 = (bf16[512,256]{1,0:T(8,128)(2,1)S(1)}, bf16[512,256]{1,0:T(8,128)(2,1)S(1)}, u32[]{:S(2)}, u32[]{:S(2)}) collective-permute-start(bf16[512,256]{1,0:T(8,128)(2,1)S(1)} %shard_map.88.k_ref), channel_id=1, source_target_pairs={{0,8},{8,16},{16,24},{24,32},{32,40},{40,48},{48,56},{56,64},{64,7... | collective-permute-start | bytes 786440 | tf_op jit(solution)/shard_map/ppermute | solution.py:341
  78.6 11.1 %collective-permute-start.5 = (bf16[512,256]{1,0:T(8,128)(2,1)S(1)}, bf16[512,256]{1,0:T(8,128)(2,1)S(1)}, u32[]{:S(2)}, u32[]{:S(2)}) collective-permute-start(bf16[512,256]{1,0:T(8,128)(2,1)S(1)} %shard_map.89.v_ref), channel_id=1, source_target_pairs={{0,8},{8,16},{16,24},{24,32},{32,40},{40,48},{48,56},{56,64},{64,7... | collective-permute-start | bytes 786440 | tf_op jit(solution)/shard_map/ppermute | solution.py:342
  84.0 11.4 %collective-permute-start.6 = (bf16[512,256]{1,0:T(8,128)(2,1)S(1)}, bf16[512,256]{1,0:T(8,128)(2,1)S(1)}, u32[]{:S(2)}, u32[]{:S(2)}) collective-permute-start(bf16[512,256]{1,0:T(8,128)(2,1)S(1)} %collective-permute-done.4.k_ref), channel_id=1, source_target_pairs={{0,8},{8,16},{16,24},{24,32},{32,40},{40,48},{48,56},{56,64},{64,7... | collective-permute-start | bytes 786440 | tf_op jit(solution)/shard_map/ppermute | solution.py:341
  89.6 17.6 %collective-permute-start.7 = (bf16[512,256]{1,0:T(8,128)(2,1)S(1)}, bf16[512,256]{1,0:T(8,128)(2,1)S(1)}, u32[]{:S(2)}, u32[]{:S(2)}) collective-permute-start(bf16[512,256]{1,0:T(8,128)(2,1)S(1)} %collective-permute-done.5.v_ref), channel_id=1, source_target_pairs={{0,8},{8,16},{16,24},{24,32},{32,40},{40,48},{48,56},{56,64},{64,7... | collective-permute-start | bytes 786440 | tf_op jit(solution)/shard_map/ppermute | solution.py:342
  95.3 14.3 %collective-permute-start.8 = (bf16[512,256]{1,0:T(8,128)(2,1)S(1)}, bf16[512,256]{1,0:T(8,128)(2,1)S(1)}, u32[]{:S(2)}, u32[]{:S(2)}) collective-permute-start(bf16[512,256]{1,0:T(8,128)(2,1)S(1)} %collective-permute-done.6.refs_0_), channel_id=1, source_target_pairs={{0,8},{8,16},{16,24},{24,32},{32,40},{40,48},{48,56},{56,64},{64,7... | collective-permute-start | bytes 786440 | tf_op jit(solution)/shard_map/ppermute | solution.py:341
  101.0 59.8 %collective-permute-start.15 = (bf16[256,2048]{1,0:T(8,128)(2,1)S(1)}, bf16[256,2048]{1,0:T(8,128)(2,1)S(1)}, u32[]{:S(2)}, u32[]{:S(2)}) collective-permute-start(bf16[256,2048]{1,0:T(8,128)(2,1)S(1)} %copy-done.2), channel_id=1, source_target_pairs={{0,1},{1,0},{2,3},{3,2},{4,5},{5,4},{6,7},{7,6},{8,9},{9,8},{10,11... | collective-permute-start | bytes 3145736 | tf_op jit(solution)/shard_map/ppermute | solution.py:324
  102.9 57.9 %collective-permute-start.16 = (bf16[256,2048]{1,0:T(8,128)(2,1)}, bf16[256,2048]{1,0:T(8,128)(2,1)S(1)}, u32[]{:S(2)}, u32[]{:S(2)}) collective-permute-start(bf16[256,2048]{1,0:T(8,128)(2,1)} %collective-permute-done.12.refs_1_), channel_id=1, source_target_pairs={{0,1},{1,0},{2,3},{3,2},{4,5},{5,4},{6,7},{7,6},{8,9},{9,8},{10,11... | collective-permute-start | bytes 3145736 | tf_op jit(solution)/shard_map/ppermute | solution.py:324
  105.3 55.5 %collective-permute-start.17 = (bf16[256,2048]{1,0:T(8,128)(2,1)}, bf16[256,2048]{1,0:T(8,128)(2,1)}, u32[]{:S(2)}, u32[]{:S(2)}) collective-permute-start(bf16[256,2048]{1,0:T(8,128)(2,1)} %collective-permute-done.13.refs_2_), channel_id=1, source_target_pairs={{0,1},{1,0},{2,3},{3,2},{4,5},{5,4},{6,7},{7,6},{8,9},{9,8},{10,11... | collective-permute-start | bytes 3145736 | tf_op jit(solution)/shard_map/ppermute | solution.py:324
  107.3 53.5 %collective-permute-start.18 = (bf16[256,2048]{1,0:T(8,128)(2,1)}, bf16[256,2048]{1,0:T(8,128)(2,1)}, u32[]{:S(2)}, u32[]{:S(2)}) collective-permute-start(bf16[256,2048]{1,0:T(8,128)(2,1)} %collective-permute-done.14.refs_3_), channel_id=1, source_target_pairs={{0,1},{1,0},{2,3},{3,2},{4,5},{5,4},{6,7},{7,6},{8,9},{9,8},{10,11... | collective-permute-start | bytes 3145736 | tf_op jit(solution)/shard_map/ppermute | solution.py:324
  109.7 10.1 %collective-permute-start.9 = (bf16[512,256]{1,0:T(8,128)(2,1)S(1)}, bf16[512,256]{1,0:T(8,128)(2,1)S(1)}, u32[]{:S(2)}, u32[]{:S(2)}) collective-permute-start(bf16[512,256]{1,0:T(8,128)(2,1)S(1)} %collective-permute-done.7.refs_1_), channel_id=1, source_target_pairs={{0,8},{8,16},{16,24},{24,32},{32,40},{40,48},{48,56},{56,64},{64,7... | collective-permute-start | bytes 786440 | tf_op jit(solution)/shard_map/ppermute | solution.py:342
  119.8 9.2 %collective-permute-start.10 = (bf16[512,256]{1,0:T(8,128)(2,1)S(1)}, bf16[512,256]{1,0:T(8,128)(2,1)S(1)}, u32[]{:S(2)}, u32[]{:S(2)}) collective-permute-start(bf16[512,256]{1,0:T(8,128)(2,1)S(1)} %collective-permute-done.8.refs_0_), channel_id=1, source_target_pairs={{0,8},{8,16},{16,24},{24,32},{32,40},{40,48},{48,56},{56,64},{64,7... | collective-permute-start | bytes 786440 | tf_op jit(solution)/shard_map/ppermute | solution.py:341
  129.1 19.7 %collective-permute-start.11 = (bf16[512,256]{1,0:T(8,128)(2,1)S(1)}, bf16[512,256]{1,0:T(8,128)(2,1)S(1)}, u32[]{:S(2)}, u32[]{:S(2)}) collective-permute-start(bf16[512,256]{1,0:T(8,128)(2,1)S(1)} %collective-permute-done.9.refs_1_), channel_id=1, source_target_pairs={{0,8},{8,16},{16,24},{24,32},{32,40},{40,48},{48,56},{56,64},{64,7... | collective-permute-start | bytes 786440 | tf_op jit(solution)/shard_map/ppermute | solution.py:342
  148.8 17.2 %copy-start.7 = (f32[2048]{0:T(1024)S(1)}, f32[2048]{0:T(1024)}, u32[]{:S(2)}) copy-start(f32[2048]{0:T(1024)} %param.13) | copy-start | bytes 24580
  152.7 0.8 copy-start.8
  153.5 0.7 copy-start.3
  154.2 11.8 %all-to-all-start.1 = ((bf16[8,64,256]{2,1,0:T(8,128)(2,1)}), bf16[8,64,256]{2,1,0:T(8,128)(2,1)S(1)}, u32[]{:S(2)}, u32[]{:S(2)}) async-start(bf16[8,64,256]{2,1,0:T(8,128)(2,1)} %bitcast.11), calls=%async_computation.1 | async-start | bytes 524288 | tf_op jit(solution)/shard_map/all_to_all | solution.py:383
  158.5 1.0 copy-start.9
where the time goes:
time: 172 us; the launch traced here: 171 us
  starting transfers between devices  84.8 us (49%)
  waiting for transfers between devices  45.6 us (27%)
  Pallas kernels  33.1 us (19%)
  local copies, waits for them, and re-layouts  6.18 us (4%)
    pallas_call x11, Pallas kernels, kernel_call(): pl.pallas_call(body, out_shape=tuple((jax.ShapeDtypeStruct(s, t) for s, t...  33.1 us
    all_to_all x1, waiting for transfers between devices, layer(): lax.all_to_all(copies, ('zh', 'y'), split_axis=0, concat_axis=0, tiled=True)  19.3 us
    ppermute x4, starting transfers between devices, layer(): keys.append(lax.ppermute(keys[-1], SP, forward))  17 us
    all_to_all x1, starting transfers between devices, layer(): lax.all_to_all(copies, ('zh', 'y'), split_axis=0, concat_axis=0, tiled=True)  16.1 us
    ppermute x4, starting transfers between devices, layer(): values.append(lax.ppermute(values[-1], SP, forward))  14.1 us
    ppermute x3, starting transfers between devices, layer(): groups.append(lax.ppermute(out_proj, 'x', ring(4, steps)))  10.8 us
    ppermute x4, waiting for transfers between devices, layer(): keys.append(lax.ppermute(keys[-1], SP, forward))  9.65 us
    ppermute x4, waiting for transfers between devices, layer(): values.append(lax.ppermute(values[-1], SP, forward))  8.95 us
  transfers between devices with their start and end apart: 21, of which 9 were waited for; matrix products, arithmetic and copies ran while one was open for 1% of the time, Pallas kernels for 16%

commit v1 on v0

--- a/solution.py
+++ b/solution.py
@@ -233,7 +233,12 @@
         cls = pl.program_id(0)
         out_ref, log_ref, att_ref = outs[:3]
         att_ref[pl.ds(pl.multiple_of(cls * 128, 128), 128), :] = (acc / total).astype(BF16)
-        log_ref[...] = m + jnp.log(total)
+        lw = m + jnp.log(total)
+        lane = lax.broadcasted_iota(jnp.int32, log_ref.shape, 1)
+        compact = jnp.zeros(log_ref.shape, F32)
+        for h in range(lw.shape[1] // HEAD_DIM):
+            compact = jnp.where(lane == h, lw[:, h * HEAD_DIM : h * HEAD_DIM + 1], compact)
+        log_ref[...] = compact
 
         @pl.when(cls == pl.num_programs(0) - 1)
         def _():
@@ -244,17 +249,15 @@
 
 
 def log_kernel(lw_ref, log_ref):
-    rows, width = lw_ref.shape
+    rows, lanes = lw_ref.shape
     perm = to_natural(rows)
     rest = lw_ref[...]
-    ordered = jnp.zeros((rows, width), F32)
+    ordered = jnp.zeros((rows, lanes), F32)
     for _ in range(3):
         piece = rest.astype(BF16)
         rest = rest - piece.astype(F32)
         ordered = ordered + jnp.dot(perm, piece, preferred_element_type=F32)
-    flipped = ordered.T
-    for head in range(width // HEAD_DIM):
-        log_ref[head : head + 1, :] = flipped[head * HEAD_DIM : head * HEAD_DIM + 1, :]
+    log_ref[...] = ordered.T[: log_ref.shape[0]]
 
 
 def out_kernel(place_ref, att_ref, *refs):
@@ -308,7 +311,17 @@
     gain = pre_gain[None]
     row = (rows, width)
 
-    (copies,) = kernel_call(copies_kernel, [((32, key_proj.shape[0], 2 * width), BF16)], (key_proj, value_proj), 1000, 8)
+    shard_spec = pl.BlockSpec(key_proj.shape, lambda n: (0, 0))
+    (copies,) = kernel_call(
+        copies_kernel,
+        [((32, key_proj.shape[0], 2 * width), BF16)],
+        (key_proj, value_proj),
+        1000,
+        56,
+        grid=(4,),
+        in_specs=[shard_spec] * 2,
+        out_specs=(pl.BlockSpec((8, key_proj.shape[0], 2 * width), lambda n: (n, 0, 0)),),
+    )
     mine = lax.all_to_all(copies, ("zh", "y"), split_axis=0, concat_axis=0, tiled=True)
     mine = mine.reshape(4, 256, 2 * width)
     slabs = []
@@ -369,14 +382,14 @@
         last = back == 4
         state = kernel_call(
             functools.partial(far_kernel, (back,), last),
-            [(row, BF16), (row, F32)] if last else [(row, F32)] * 3,
+            [(row, BF16), ((rows, 128), F32)] if last else [(row, F32)] * 3,
             (place, query, *state, keys[back], values[back]),
             4 * rows * 512 * width,
             16,
             ([(row, BF16)] if last else []) + [((512, 128), t) for t in (F32, BF16)] + [((2, 512, width), F32)],
             grid=(rows // 128,),
             in_specs=[SMEM] + [part] * 6,
-            out_specs=(whole, part) if last else (part,) * 3,
+            out_specs=(whole, pl.BlockSpec((128, 128), lambda c: (c, 0))) if last else (part,) * 3,
         )
     attended, logs = state
 

time: 172 us -> 174 us (1.012)
  Pallas kernels: 33.1 us -> 36.5 us
    pallas_call x11, Pallas kernels: 33.1 us -> 36.5 us  [kernel_call(): pl.pallas_call(body, out_shape=tuple((jax.ShapeDtypeStruct(s, t) for s, t...]
    unnamed x20 -> x16, local copies, waits for them, and re-layouts: 5.18 us -> 3.58 us
  transfers between devices with their start and end apart: 21 -> 21, of which waited for: 9 -> 9; matrix products, arithmetic and copies ran while one was open for 1% -> 1% of each run, Pallas kernels for 16% -> 17%
where the time goes in v1:
time: 174 us; the launch traced here: 173 us
  starting transfers between devices  84.9 us (49%)
  waiting for transfers between devices  45.7 us (26%)
  Pallas kernels  36.5 us (21%)
  local copies, waits for them, and re-layouts  4.58 us (3%)
    pallas_call x11, Pallas kernels, kernel_call(): pl.pallas_call(body, out_shape=tuple((jax.ShapeDtypeStruct(s, t) for s, t...  36.5 us
    all_to_all x1, waiting for transfers between devices, layer(): lax.all_to_all(copies, ('zh', 'y'), split_axis=0, concat_axis=0, tiled=True)  19.3 us
    ppermute x4, starting transfers between devices, layer(): keys.append(lax.ppermute(keys[-1], SP, forward))  17 us
    all_to_all x1, starting transfers between devices, layer(): lax.all_to_all(copies, ('zh', 'y'), split_axis=0, concat_axis=0, tiled=True)  16.1 us
    ppermute x4, starting transfers between devices, layer(): values.append(lax.ppermute(values[-1], SP, forward))  14.1 us
    ppermute x3, starting transfers between devices, layer(): groups.append(lax.ppermute(out_proj, 'x', ring(4, steps)))  10.8 us
    ppermute x4, waiting for transfers between devices, layer(): keys.append(lax.ppermute(keys[-1], SP, forward))  9.62 us
    ppermute x4, waiting for transfers between devices, layer(): values.append(lax.ppermute(values[-1], SP, forward))  8.94 us
  transfers between devices with their start and end apart: 21, of which 9 were waited for; matrix products, arithmetic and copies ran while one was open for 1% of the time, Pallas kernels for 17%

profile of v1, /device:TPU:24, one launch (start us, length us, event | category | flops | bytes accessed | tf_op | source)
XLA Modules:
  0.0 173.1 jit_solution(17654254913058147122)
XLA Ops:
  0.6 2.3 %shard_map.87 = bf16[32,32,512]{2,1,0:T(8,128)(2,1)} custom-call(bf16[32,256]{1,0:T(8,128)(2,1)} %key_ref.1, bf16[32,256]{1,0:T(8,128)(2,1)} %value_ref.1), custom_call_target="tpu_custom_call" | custom-call | flops 1000 | bytes 32768 | tf_op jit(solution)/shard_map/pallas_call | solution.py:295
  2.9 16.1 %all-to-all-start = ((bf16[32,32,512]{2,1,0:T(8,128)(2,1)}), bf16[32,32,512]{2,1,0:T(8,128)(2,1)S(1)}, u32[]{:S(2)}, u32[]{:S(2)}) async-start(bf16[32,32,512]{2,1,0:T(8,128)(2,1)} %shard_map.87), calls=%async_computation | async-start | bytes 2097152 | tf_op jit(solution)/shard_map/all_to_all | solution.py:325
  19.0 3.4 %collective-permute-start.12 = (bf16[256,2048]{1,0:T(8,128)(2,1)}, bf16[256,2048]{1,0:T(8,128)(2,1)}, u32[]{:S(2)}, u32[]{:S(2)}) collective-permute-start(bf16[256,2048]{1,0:T(8,128)(2,1)} %refs_0_.1), channel_id=1, source_target_pairs={{0,2},{2,4},{4,6},{6,0},{1,3},{3,5},{5,7},{7,1},{8,10},{10,12},{12... | collective-permute-start | bytes 3145736 | tf_op jit(solution)/shard_map/ppermute | solution.py:335
  22.4 3.7 %collective-permute-start.13 = (bf16[256,2048]{1,0:T(8,128)(2,1)}, bf16[256,2048]{1,0:T(8,128)(2,1)}, u32[]{:S(2)}, u32[]{:S(2)}) collective-permute-start(bf16[256,2048]{1,0:T(8,128)(2,1)} %refs_0_.1), channel_id=1, source_target_pairs={{0,6},{2,0},{4,2},{6,4},{1,7},{3,1},{5,3},{7,5},{8,14},{10,8},{12,... | collective-permute-start | bytes 3145736 | tf_op jit(solution)/shard_map/ppermute | solution.py:335
  26.1 3.7 %collective-permute-start.14 = (bf16[256,2048]{1,0:T(8,128)(2,1)}, bf16[256,2048]{1,0:T(8,128)(2,1)}, u32[]{:S(2)}, u32[]{:S(2)}) collective-permute-start(bf16[256,2048]{1,0:T(8,128)(2,1)} %refs_0_.1), channel_id=1, source_target_pairs={{0,4},{2,6},{4,0},{6,2},{1,5},{3,7},{5,1},{7,3},{8,12},{10,14},{12... | collective-permute-start | bytes 3145736 | tf_op jit(solution)/shard_map/ppermute | solution.py:335
  29.9 19.3 %all-to-all-done = bf16[32,32,512]{2,1,0:T(8,128)(2,1)S(1)} async-done(((bf16[32,32,512]{2,1,0:T(8,128)(2,1)}), bf16[32,32,512]{2,1,0:T(8,128)(2,1)S(1)}, u32[]{:S(2)}, u32[]{:S(2)}) %all-to-all-start) | async-done | bytes 1048608 | tf_op jit(solution)/shard_map/all_to_all | solution.py:325
  49.2 1.0 fusion
  50.2 4.1 %collective-permute-start = (bf16[2,256,256]{2,1,0:T(8,128)(2,1)}, bf16[2,256,256]{2,1,0:T(8,128)(2,1)S(1)}, u32[]{:S(2)}, u32[]{:S(2)}) collective-permute-start(bf16[2,256,256]{2,1,0:T(8,128)(2,1)} %get-tuple-element.37), channel_id=1, source_target_pairs={{0,64},{64,128},{128,192},{192,256},{256,320},{320,384},{384,448},... | collective-permute-start | bytes 786440 | tf_op jit(solution)/shard_map/ppermute | solution.py:329
  54.3 3.0 %collective-permute-start.1 = (bf16[2,256,256]{2,1,0:T(8,128)(2,1)}, bf16[2,256,256]{2,1,0:T(8,128)(2,1)}, u32[]{:S(2)}, u32[]{:S(2)}) collective-permute-start(bf16[2,256,256]{2,1,0:T(8,128)(2,1)} %get-tuple-element.36), channel_id=1, source_target_pairs={{0,448},{64,0},{128,64},{192,128},{256,192},{320,256},{384,320},{4... | collective-permute-start | bytes 786440 | tf_op jit(solution)/shard_map/ppermute | solution.py:330
  57.3 0.3 multiply_cosine_fusion
  57.6 2.3 %collective-permute-done.below_ref = bf16[2,256,256]{2,1,0:T(8,128)(2,1)S(1)} collective-permute-done((bf16[2,256,256]{2,1,0:T(8,128)(2,1)}, bf16[2,256,256]{2,1,0:T(8,128)(2,1)S(1)}, u32[]{:S(2)}, u32[]{:S(2)}) %collective-permute-start) | collective-permute-done | bytes 262176 | tf_op jit(solution)/shard_map/ppermute | solution.py:329
  59.9 2.9 %collective-permute-start.2 = (bf16[2,256,256]{2,1,0:T(8,128)(2,1)}, bf16[2,256,256]{2,1,0:T(8,128)(2,1)S(1)}, u32[]{:S(2)}, u32[]{:S(2)}) collective-permute-start(bf16[2,256,256]{2,1,0:T(8,128)(2,1)} %get-tuple-element.35), channel_id=1, source_target_pairs={{0,64},{64,128},{128,192},{192,256},{256,320},{320,384},{384,448},... | collective-permute-start | bytes 786440 | tf_op jit(solution)/shard_map/ppermute | solution.py:329
  62.7 0.1 pad_add_fusion.place_ref
  62.8 0.2 collective-permute-done.1.above_ref
  63.0 4.0 %collective-permute-start.3 = (bf16[2,256,256]{2,1,0:T(8,128)(2,1)}, bf16[2,256,256]{2,1,0:T(8,128)(2,1)S(1)}, u32[]{:S(2)}, u32[]{:S(2)}) collective-permute-start(bf16[2,256,256]{2,1,0:T(8,128)(2,1)} %get-tuple-element.34), channel_id=1, source_target_pairs={{0,448},{64,0},{128,64},{192,128},{256,192},{320,256},{384,320},{4... | collective-permute-start | bytes 786440 | tf_op jit(solution)/shard_map/ppermute | solution.py:330
  67.1 0.0 copy-start.1
  67.1 1.2 copy-done.1
  68.3 2.7 %shard_map.86 = (bf16[512,2048]{1,0:T(8,128)(2,1)S(1)}, bf16[512,256]{1,0:T(8,128)(2,1)S(1)}) custom-call(bf16[512,2048]{1,0:T(8,128)(2,1)S(1)} %copy-done, f32[1,2048]{1,0:T(1,128)S(1)} %bitcast.12, bf16[2048,256]{1,0:T(8,128)(2,1)S(1)} %copy-done.1, f32[2,32,512]{2,1,0:T(8,128)S(1)} %pad_maximum_fusion.turn_ref), custom_call_target="tpu_custom_call" | custom-call | flops 536870912 | bytes 3284992 | tf_op jit(solution)/shard_map/pallas_call | solution.py:295
  71.0 2.4 %shard_map.88.k_ref = bf16[512,256]{1,0:T(8,128)(2,1)S(1)} custom-call(s32[4]{0:T(128)S(1)} %pad_add_fusion.place_ref, bf16[512,2048]{1,0:T(8,128)(2,1)S(1)} %get-tuple-element.19.normed_ref, bf16[4,256,512]{2,1,0:T(8,128)(2,1)S(1)} %bitcast.9, bf16[2,256,256]{2,1,0:T(8,128)(2,1)S(1)} %collective-permute-done.below_ref, ...), custom_call_target="tpu_custom_call" | custom-call | flops 536870912 | bytes 3801104 | tf_op jit(solution)/shard_map/pallas_call | solution.py:295
  73.4 0.0 copy-start.2
  73.4 0.0 collective-permute-done.2.below_ref
  73.4 3.1 %collective-permute-start.4 = (bf16[512,256]{1,0:T(8,128)(2,1)S(1)}, bf16[512,256]{1,0:T(8,128)(2,1)S(1)}, u32[]{:S(2)}, u32[]{:S(2)}) collective-permute-start(bf16[512,256]{1,0:T(8,128)(2,1)S(1)} %shard_map.88.k_ref), channel_id=1, source_target_pairs={{0,8},{8,16},{16,24},{24,32},{32,40},{40,48},{48,56},{56,64},{64,7... | collective-permute-start | bytes 786440 | tf_op jit(solution)/shard_map/ppermute | solution.py:354
  76.5 0.0 collective-permute-done.3.above_ref
  76.5 1.8 %shard_map.89.v_ref = bf16[512,256]{1,0:T(8,128)(2,1)S(1)} custom-call(s32[4]{0:T(128)S(1)} %pad_add_fusion.place_ref, bf16[512,2048]{1,0:T(8,128)(2,1)S(1)} %get-tuple-element.19.normed_ref, bf16[4,256,512]{2,1,0:T(8,128)(2,1)S(1)} %bitcast.10, bf16[2,256,256]{2,1,0:T(8,128)(2,1)S(1)} %collective-permute-done.2.below_ref, ...), custom_call_target="tpu_custom_call" | custom-call | flops 536870912 | bytes 3670032 | tf_op jit(solution)/shard_map/pallas_call | solution.py:295
  78.3 2.4 %collective-permute-start.5 = (bf16[512,256]{1,0:T(8,128)(2,1)S(1)}, bf16[512,256]{1,0:T(8,128)(2,1)S(1)}, u32[]{:S(2)}, u32[]{:S(2)}) collective-permute-start(bf16[512,256]{1,0:T(8,128)(2,1)S(1)} %shard_map.89.v_ref), channel_id=1, source_target_pairs={{0,8},{8,16},{16,24},{24,32},{32,40},{40,48},{48,56},{56,64},{64,7... | collective-permute-start | bytes 786440 | tf_op jit(solution)/shard_map/ppermute | solution.py:355
  80.7 3.0 %collective-permute-done.4.k_ref = bf16[512,256]{1,0:T(8,128)(2,1)S(1)} collective-permute-done((bf16[512,256]{1,0:T(8,128)(2,1)S(1)}, bf16[512,256]{1,0:T(8,128)(2,1)S(1)}, u32[]{:S(2)}, u32[]{:S(2)}) %collective-permute-start.4) | collective-permute-done | bytes 262176 | tf_op jit(solution)/shard_map/ppermute | solution.py:354
  83.7 4.9 %collective-permute-start.6 = (bf16[512,256]{1,0:T(8,128)(2,1)S(1)}, bf16[512,256]{1,0:T(8,128)(2,1)S(1)}, u32[]{:S(2)}, u32[]{:S(2)}) collective-permute-start(bf16[512,256]{1,0:T(8,128)(2,1)S(1)} %collective-permute-done.4.k_ref), channel_id=1, source_target_pairs={{0,8},{8,16},{16,24},{24,32},{32,40},{40,48},{48,56},{56,64},{64,7... | collective-permute-start | bytes 786440 | tf_op jit(solution)/shard_map/ppermute | solution.py:354
  88.6 0.7 collective-permute-done.5.v_ref
  89.4 4.9 %collective-permute-start.7 = (bf16[512,256]{1,0:T(8,128)(2,1)S(1)}, bf16[512,256]{1,0:T(8,128)(2,1)S(1)}, u32[]{:S(2)}, u32[]{:S(2)}) collective-permute-start(bf16[512,256]{1,0:T(8,128)(2,1)S(1)} %collective-permute-done.5.v_ref), channel_id=1, source_target_pairs={{0,8},{8,16},{16,24},{24,32},{32,40},{40,48},{48,56},{56,64},{64,7... | collective-permute-start | bytes 786440 | tf_op jit(solution)/shard_map/ppermute | solution.py:355
  94.2 0.8 collective-permute-done.6.refs_0_
  95.1 5.6 %collective-permute-start.8 = (bf16[512,256]{1,0:T(8,128)(2,1)S(1)}, bf16[512,256]{1,0:T(8,128)(2,1)S(1)}, u32[]{:S(2)}, u32[]{:S(2)}) collective-permute-start(bf16[512,256]{1,0:T(8,128)(2,1)S(1)} %collective-permute-done.6.refs_0_), channel_id=1, source_target_pairs={{0,8},{8,16},{16,24},{24,32},{32,40},{40,48},{48,56},{56,64},{64,7... | collective-permute-start | bytes 786440 | tf_op jit(solution)/shard_map/ppermute | solution.py:354
  100.7 0.0 collective-permute-done.12.refs_1_
  100.7 0.0 copy-done.2
  100.7 1.9 %collective-permute-start.15 = (bf16[256,2048]{1,0:T(8,128)(2,1)S(1)}, bf16[256,2048]{1,0:T(8,128)(2,1)S(1)}, u32[]{:S(2)}, u32[]{:S(2)}) collective-permute-start(bf16[256,2048]{1,0:T(8,128)(2,1)S(1)} %copy-done.2), channel_id=1, source_target_pairs={{0,1},{1,0},{2,3},{3,2},{4,5},{5,4},{6,7},{7,6},{8,9},{9,8},{10,11... | collective-permute-start | bytes 3145736 | tf_op jit(solution)/shard_map/ppermute | solution.py:337
  102.6 0.0 collective-permute-done.13.refs_2_
  102.6 2.4 %collective-permute-start.16 = (bf16[256,2048]{1,0:T(8,128)(2,1)}, bf16[256,2048]{1,0:T(8,128)(2,1)S(1)}, u32[]{:S(2)}, u32[]{:S(2)}) collective-permute-start(bf16[256,2048]{1,0:T(8,128)(2,1)} %collective-permute-done.12.refs_1_), channel_id=1, source_target_pairs={{0,1},{1,0},{2,3},{3,2},{4,5},{5,4},{6,7},{7,6},{8,9},{9,8},{10,11... | collective-permute-start | bytes 3145736 | tf_op jit(solution)/shard_map/ppermute | solution.py:337
  105.0 0.0 collective-permute-done.14.refs_3_
  105.1 1.9 %collective-permute-start.17 = (bf16[256,2048]{1,0:T(8,128)(2,1)}, bf16[256,2048]{1,0:T(8,128)(2,1)}, u32[]{:S(2)}, u32[]{:S(2)}) collective-permute-start(bf16[256,2048]{1,0:T(8,128)(2,1)} %collective-permute-done.13.refs_2_), channel_id=1, source_target_pairs={{0,1},{1,0},{2,3},{3,2},{4,5},{5,4},{6,7},{7,6},{8,9},{9,8},{10,11... | collective-permute-start | bytes 3145736 | tf_op jit(solution)/shard_map/ppermute | solution.py:337
  107.0 0.0 collective-permute-done.7.refs_1_
  107.0 2.4 %collective-permute-start.18 = (bf16[256,2048]{1,0:T(8,128)(2,1)}, bf16[256,2048]{1,0:T(8,128)(2,1)}, u32[]{:S(2)}, u32[]{:S(2)}) collective-permute-start(bf16[256,2048]{1,0:T(8,128)(2,1)} %collective-permute-done.14.refs_3_), channel_id=1, source_target_pairs={{0,1},{1,0},{2,3},{3,2},{4,5},{5,4},{6,7},{7,6},{8,9},{9,8},{10,11... | collective-permute-start | bytes 3145736 | tf_op jit(solution)/shard_map/ppermute | solution.py:337
  109.4 0.0 collective-permute-done.8.refs_0_
  109.4 1.9 %collective-permute-start.9 = (bf16[512,256]{1,0:T(8,128)(2,1)S(1)}, bf16[512,256]{1,0:T(8,128)(2,1)S(1)}, u32[]{:S(2)}, u32[]{:S(2)}) collective-permute-start(bf16[512,256]{1,0:T(8,128)(2,1)S(1)} %collective-permute-done.7.refs_1_), channel_id=1, source_target_pairs={{0,8},{8,16},{16,24},{24,32},{32,40},{40,48},{48,56},{56,64},{64,7... | collective-permute-start | bytes 786440 | tf_op jit(solution)/shard_map/ppermute | solution.py:355
  111.4 8.2 %collective-permute-done.9.refs_1_ = bf16[512,256]{1,0:T(8,128)(2,1)S(1)} collective-permute-done((bf16[512,256]{1,0:T(8,128)(2,1)S(1)}, bf16[512,256]{1,0:T(8,128)(2,1)S(1)}, u32[]{:S(2)}, u32[]{:S(2)}) %collective-permute-start.9) | collective-permute-done | bytes 262176 | tf_op jit(solution)/shard_map/ppermute | solution.py:355
  119.5 3.4 %collective-permute-start.10 = (bf16[512,256]{1,0:T(8,128)(2,1)S(1)}, bf16[512,256]{1,0:T(8,128)(2,1)S(1)}, u32[]{:S(2)}, u32[]{:S(2)}) collective-permute-start(bf16[512,256]{1,0:T(8,128)(2,1)S(1)} %collective-permute-done.8.refs_0_), channel_id=1, source_target_pairs={{0,8},{8,16},{16,24},{24,32},{32,40},{40,48},{48,56},{56,64},{64,7... | collective-permute-start | bytes 786440 | tf_op jit(solution)/shard_map/ppermute | solution.py:354
  122.9 5.8 %collective-permute-done.10.refs_0_ = bf16[512,256]{1,0:T(8,128)(2,1)S(1)} collective-permute-done((bf16[512,256]{1,0:T(8,128)(2,1)S(1)}, bf16[512,256]{1,0:T(8,128)(2,1)S(1)}, u32[]{:S(2)}, u32[]{:S(2)}) %collective-permute-start.10) | collective-permute-done | bytes 262176 | tf_op jit(solution)/shard_map/ppermute | solution.py:354
  128.8 4.9 %collective-permute-start.11 = (bf16[512,256]{1,0:T(8,128)(2,1)S(1)}, bf16[512,256]{1,0:T(8,128)(2,1)S(1)}, u32[]{:S(2)}, u32[]{:S(2)}) collective-permute-start(bf16[512,256]{1,0:T(8,128)(2,1)S(1)} %collective-permute-done.9.refs_1_), channel_id=1, source_target_pairs={{0,8},{8,16},{16,24},{24,32},{32,40},{40,48},{48,56},{56,64},{64,7... | collective-permute-start | bytes 786440 | tf_op jit(solution)/shard_map/ppermute | solution.py:355
  133.7 3.5 %shard_map.90 = (f32[512,256]{1,0:T(8,128)S(1)}, f32[512,256]{1,0:T(8,128)S(1)}, f32[512,256]{1,0:T(8,128)S(1)}) custom-call(bf16[512,256]{1,0:T(8,128)(2,1)S(1)} %get-tuple-element.18.q_ref, bf16[512,256]{1,0:T(8,128)(2,1)S(1)} %shard_map.88.k_ref, bf16[512,256]{1,0:T(8,128)(2,1)S(1)} %shard_map.89.v_ref), custom_call_target="tpu_custom_call" | custom-call | flops 536870912 | bytes 786432 | tf_op jit(solution)/shard_map/pallas_call | solution.py:295
  137.2 4.1 %shard_map.91 = (f32[512,256]{1,0:T(8,128)S(1)}, f32[512,256]{1,0:T(8,128)S(1)}, f32[512,256]{1,0:T(8,128)S(1)}) custom-call(s32[4]{0:T(128)S(1)} %pad_add_fusion.place_ref, bf16[512,256]{1,0:T(8,128)(2,1)S(1)} %get-tuple-element.18.q_ref, f32[512,256]{1,0:T(8,128)S(1)} %get-tuple-element.20.max_ref, f32[512,256]{1,0:T(8,128)S(1)} %get-tuple-element.21.sum_ref, ...), custom_call_target="tpu_custom_call" | custom-call | flops 268435456 | bytes 2359312 | tf_op jit(solution)/shard_map/pallas_call | solution.py:295
  141.4 3.6 %shard_map.92 = (f32[512,256]{1,0:T(8,128)S(1)}, f32[512,256]{1,0:T(8,128)S(1)}, f32[512,256]{1,0:T(8,128)S(1)}) custom-call(s32[4]{0:T(128)S(1)} %pad_add_fusion.place_ref, bf16[512,256]{1,0:T(8,128)(2,1)S(1)} %get-tuple-element.18.q_ref, f32[512,256]{1,0:T(8,128)S(1)} %get-tuple-element.23.max_ref, f32[512,256]{1,0:T(8,128)S(1)} %get-tuple-element.24.sum_ref, ...), custom_call_target="tpu_custom_call" | custom-call | flops 268435456 | bytes 2359312 | tf_op jit(solution)/shard_map/pallas_call | solution.py:295
  144.9 3.6 %shard_map.93 = (f32[512,256]{1,0:T(8,128)S(1)}, f32[512,256]{1,0:T(8,128)S(1)}, f32[512,256]{1,0:T(8,128)S(1)}) custom-call(s32[4]{0:T(128)S(1)} %pad_add_fusion.place_ref, bf16[512,256]{1,0:T(8,128)(2,1)S(1)} %get-tuple-element.18.q_ref, f32[512,256]{1,0:T(8,128)S(1)} %get-tuple-element.26.max_ref, f32[512,256]{1,0:T(8,128)S(1)} %get-tuple-element.27.sum_ref, ...), custom_call_target="tpu_custom_call" | custom-call | flops 268435456 | bytes 2359312 | tf_op jit(solution)/shard_map/pallas_call | solution.py:295
  148.5 0.0 collective-permute-done.11.refs_1_
  148.5 0.0 copy-start.5
  148.5 6.2 %shard_map.94 = (bf16[512,256]{1,0:T(8,128)(2,1)S(1)}, f32[512,128]{1,0:T(8,128)S(1)}) custom-call(s32[4]{0:T(128)S(1)} %pad_add_fusion.place_ref, bf16[512,256]{1,0:T(8,128)(2,1)S(1)} %get-tuple-element.18.q_ref, f32[512,256]{1,0:T(8,128)S(1)} %get-tuple-element.29.max_ref, f32[512,256]{1,0:T(8,128)S(1)} %get-tuple-element.30.sum_ref, ...), custom_call_target="tpu_custom_call" | custom-call | flops 268435456 | bytes 2359312 | tf_op jit(solution)/shard_map/pallas_call | solution.py:295
  154.7 0.7 copy-done.6
  155.4 0.7 copy-done.3
  156.1 4.3 %all-to-all-start.1 = ((bf16[8,64,256]{2,1,0:T(8,128)(2,1)}), bf16[8,64,256]{2,1,0:T(8,128)(2,1)S(1)}, u32[]{:S(2)}, u32[]{:S(2)}) async-start(bf16[8,64,256]{2,1,0:T(8,128)(2,1)} %bitcast.11), calls=%async_computation.1 | async-start | bytes 524288 | tf_op jit(solution)/shard_map/all_to_all | solution.py:396
  160.4 0.9 copy-done.7
  161.4 1.2 shard_map.96
  162.6 0.0 collective-permute-done.15.refs_4_
  162.6 0.0 collective-permute-done.16.refs_5_
  162.6 0.0 collective-permute-done.17.refs_6_
  162.6 0.0 collective-permute-done.18.refs_7_
  162.6 5.3 %all-to-all-done.1.att_ref = bf16[8,64,256]{2,1,0:T(8,128)(2,1)S(1)} async-done(((bf16[8,64,256]{2,1,0:T(8,128)(2,1)}), bf16[8,64,256]{2,1,0:T(8,128)(2,1)S(1)}, u32[]{:S(2)}, u32[]{:S(2)}) %all-to-all-start.1) | async-done | bytes 262176 | tf_op jit(solution)/shard_map/all_to_all | solution.py:396
  167.9 5.1 %shard_map.95 = bf16[64,2048]{1,0:T(8,128)(2,1)} custom-call(s32[4]{0:T(128)S(1)} %pad_add_fusion.place_ref, bf16[8,64,256]{2,1,0:T(8,128)(2,1)S(1)} %all-to-all-done.1.att_ref, bf16[256,2048]{1,0:T(8,128)(2,1)S(1)} %copy-done.2, bf16[256,2048]{1,0:T(8,128)(2,1)} %collective-permute-done.12.refs_1_, bf16[256,2048]{1,0:T(8,128)(2,1)} %collective-permute-done.13.refs_2_, ...), custom_call_target="tpu_custom_call" | custom-call | flops 536870912 | bytes 8658960 | tf_op jit(solution)/shard_map/pallas_call | solution.py:295
  (11 shorter events, 0.0 us)
Async XLA Ops:
  2.9 64.1 %copy-start = (bf16[512,2048]{1,0:T(8,128)(2,1)S(1)}, bf16[512,2048]{1,0:T(8,128)(2,1)}, u32[]{:S(2)}) copy-start(bf16[512,2048]{1,0:T(8,128)(2,1)} %hidden_ref.1) | copy-start | bytes 6291460
  2.9 64.1 %copy-start.4 = (f32[2048]{0:T(1024)S(1)}, f32[2048]{0:T(1024)}, u32[]{:S(2)}) copy-start(f32[2048]{0:T(1024)} %param.8) | copy-start | bytes 24580
  2.9 46.3 %all-to-all-start = ((bf16[32,32,512]{2,1,0:T(8,128)(2,1)}), bf16[32,32,512]{2,1,0:T(8,128)(2,1)S(1)}, u32[]{:S(2)}, u32[]{:S(2)}) async-start(bf16[32,32,512]{2,1,0:T(8,128)(2,1)} %shard_map.87), calls=%async_computation | async-start | bytes 2097152 | tf_op jit(solution)/shard_map/all_to_all | solution.py:325
  19.0 81.7 %collective-permute-start.12 = (bf16[256,2048]{1,0:T(8,128)(2,1)}, bf16[256,2048]{1,0:T(8,128)(2,1)}, u32[]{:S(2)}, u32[]{:S(2)}) collective-permute-start(bf16[256,2048]{1,0:T(8,128)(2,1)} %refs_0_.1), channel_id=1, source_target_pairs={{0,2},{2,4},{4,6},{6,0},{1,3},{3,5},{5,7},{7,1},{8,10},{10,12},{12... | collective-permute-start | bytes 3145736 | tf_op jit(solution)/shard_map/ppermute | solution.py:335
  22.4 80.2 %collective-permute-start.13 = (bf16[256,2048]{1,0:T(8,128)(2,1)}, bf16[256,2048]{1,0:T(8,128)(2,1)}, u32[]{:S(2)}, u32[]{:S(2)}) collective-permute-start(bf16[256,2048]{1,0:T(8,128)(2,1)} %refs_0_.1), channel_id=1, source_target_pairs={{0,6},{2,0},{4,2},{6,4},{1,7},{3,1},{5,3},{7,5},{8,14},{10,8},{12,... | collective-permute-start | bytes 3145736 | tf_op jit(solution)/shard_map/ppermute | solution.py:335
  26.1 78.9 %collective-permute-start.14 = (bf16[256,2048]{1,0:T(8,128)(2,1)}, bf16[256,2048]{1,0:T(8,128)(2,1)}, u32[]{:S(2)}, u32[]{:S(2)}) collective-permute-start(bf16[256,2048]{1,0:T(8,128)(2,1)} %refs_0_.1), channel_id=1, source_target_pairs={{0,4},{2,6},{4,0},{6,2},{1,5},{3,7},{5,1},{7,3},{8,12},{10,14},{12... | collective-permute-start | bytes 3145736 | tf_op jit(solution)/shard_map/ppermute | solution.py:335
  50.2 9.7 %collective-permute-start = (bf16[2,256,256]{2,1,0:T(8,128)(2,1)}, bf16[2,256,256]{2,1,0:T(8,128)(2,1)S(1)}, u32[]{:S(2)}, u32[]{:S(2)}) collective-permute-start(bf16[2,256,256]{2,1,0:T(8,128)(2,1)} %get-tuple-element.37), channel_id=1, source_target_pairs={{0,64},{64,128},{128,192},{192,256},{256,320},{320,384},{384,448},... | collective-permute-start | bytes 786440 | tf_op jit(solution)/shard_map/ppermute | solution.py:329
  54.3 8.8 %collective-permute-start.1 = (bf16[2,256,256]{2,1,0:T(8,128)(2,1)}, bf16[2,256,256]{2,1,0:T(8,128)(2,1)}, u32[]{:S(2)}, u32[]{:S(2)}) collective-permute-start(bf16[2,256,256]{2,1,0:T(8,128)(2,1)} %get-tuple-element.36), channel_id=1, source_target_pairs={{0,448},{64,0},{128,64},{192,128},{256,192},{320,256},{384,320},{4... | collective-permute-start | bytes 786440 | tf_op jit(solution)/shard_map/ppermute | solution.py:330
  59.9 13.5 %collective-permute-start.2 = (bf16[2,256,256]{2,1,0:T(8,128)(2,1)}, bf16[2,256,256]{2,1,0:T(8,128)(2,1)S(1)}, u32[]{:S(2)}, u32[]{:S(2)}) collective-permute-start(bf16[2,256,256]{2,1,0:T(8,128)(2,1)} %get-tuple-element.35), channel_id=1, source_target_pairs={{0,64},{64,128},{128,192},{192,256},{256,320},{320,384},{384,448},... | collective-permute-start | bytes 786440 | tf_op jit(solution)/shard_map/ppermute | solution.py:329
  63.0 13.5 %collective-permute-start.3 = (bf16[2,256,256]{2,1,0:T(8,128)(2,1)}, bf16[2,256,256]{2,1,0:T(8,128)(2,1)S(1)}, u32[]{:S(2)}, u32[]{:S(2)}) collective-permute-start(bf16[2,256,256]{2,1,0:T(8,128)(2,1)} %get-tuple-element.34), channel_id=1, source_target_pairs={{0,448},{64,0},{128,64},{192,128},{256,192},{320,256},{384,320},{4... | collective-permute-start | bytes 786440 | tf_op jit(solution)/shard_map/ppermute | solution.py:330
  67.1 1.2 copy-start.1
  73.4 27.3 %copy-start.2 = (bf16[256,2048]{1,0:T(8,128)(2,1)S(1)}, bf16[256,2048]{1,0:T(8,128)(2,1)}, u32[]{:S(2)}) copy-start(bf16[256,2048]{1,0:T(8,128)(2,1)} %refs_0_.1) | copy-start | bytes 3145732
  73.4 10.3 %collective-permute-start.4 = (bf16[512,256]{1,0:T(8,128)(2,1)S(1)}, bf16[512,256]{1,0:T(8,128)(2,1)S(1)}, u32[]{:S(2)}, u32[]{:S(2)}) collective-permute-start(bf16[512,256]{1,0:T(8,128)(2,1)S(1)} %shard_map.88.k_ref), channel_id=1, source_target_pairs={{0,8},{8,16},{16,24},{24,32},{32,40},{40,48},{48,56},{56,64},{64,7... | collective-permute-start | bytes 786440 | tf_op jit(solution)/shard_map/ppermute | solution.py:354
  78.3 11.1 %collective-permute-start.5 = (bf16[512,256]{1,0:T(8,128)(2,1)S(1)}, bf16[512,256]{1,0:T(8,128)(2,1)S(1)}, u32[]{:S(2)}, u32[]{:S(2)}) collective-permute-start(bf16[512,256]{1,0:T(8,128)(2,1)S(1)} %shard_map.89.v_ref), channel_id=1, source_target_pairs={{0,8},{8,16},{16,24},{24,32},{32,40},{40,48},{48,56},{56,64},{64,7... | collective-permute-start | bytes 786440 | tf_op jit(solution)/shard_map/ppermute | solution.py:355
  83.7 11.4 %collective-permute-start.6 = (bf16[512,256]{1,0:T(8,128)(2,1)S(1)}, bf16[512,256]{1,0:T(8,128)(2,1)S(1)}, u32[]{:S(2)}, u32[]{:S(2)}) collective-permute-start(bf16[512,256]{1,0:T(8,128)(2,1)S(1)} %collective-permute-done.4.k_ref), channel_id=1, source_target_pairs={{0,8},{8,16},{16,24},{24,32},{32,40},{40,48},{48,56},{56,64},{64,7... | collective-permute-start | bytes 786440 | tf_op jit(solution)/shard_map/ppermute | solution.py:354
  89.4 17.6 %collective-permute-start.7 = (bf16[512,256]{1,0:T(8,128)(2,1)S(1)}, bf16[512,256]{1,0:T(8,128)(2,1)S(1)}, u32[]{:S(2)}, u32[]{:S(2)}) collective-permute-start(bf16[512,256]{1,0:T(8,128)(2,1)S(1)} %collective-permute-done.5.v_ref), channel_id=1, source_target_pairs={{0,8},{8,16},{16,24},{24,32},{32,40},{40,48},{48,56},{56,64},{64,7... | collective-permute-start | bytes 786440 | tf_op jit(solution)/shard_map/ppermute | solution.py:355
  95.1 14.3 %collective-permute-start.8 = (bf16[512,256]{1,0:T(8,128)(2,1)S(1)}, bf16[512,256]{1,0:T(8,128)(2,1)S(1)}, u32[]{:S(2)}, u32[]{:S(2)}) collective-permute-start(bf16[512,256]{1,0:T(8,128)(2,1)S(1)} %collective-permute-done.6.refs_0_), channel_id=1, source_target_pairs={{0,8},{8,16},{16,24},{24,32},{32,40},{40,48},{48,56},{56,64},{64,7... | collective-permute-start | bytes 786440 | tf_op jit(solution)/shard_map/ppermute | solution.py:354
  100.7 61.9 %collective-permute-start.15 = (bf16[256,2048]{1,0:T(8,128)(2,1)S(1)}, bf16[256,2048]{1,0:T(8,128)(2,1)S(1)}, u32[]{:S(2)}, u32[]{:S(2)}) collective-permute-start(bf16[256,2048]{1,0:T(8,128)(2,1)S(1)} %copy-done.2), channel_id=1, source_target_pairs={{0,1},{1,0},{2,3},{3,2},{4,5},{5,4},{6,7},{7,6},{8,9},{9,8},{10,11... | collective-permute-start | bytes 3145736 | tf_op jit(solution)/shard_map/ppermute | solution.py:337
  102.6 60.0 %collective-permute-start.16 = (bf16[256,2048]{1,0:T(8,128)(2,1)}, bf16[256,2048]{1,0:T(8,128)(2,1)S(1)}, u32[]{:S(2)}, u32[]{:S(2)}) collective-permute-start(bf16[256,2048]{1,0:T(8,128)(2,1)} %collective-permute-done.12.refs_1_), channel_id=1, source_target_pairs={{0,1},{1,0},{2,3},{3,2},{4,5},{5,4},{6,7},{7,6},{8,9},{9,8},{10,11... | collective-permute-start | bytes 3145736 | tf_op jit(solution)/shard_map/ppermute | solution.py:337
  105.1 57.5 %collective-permute-start.17 = (bf16[256,2048]{1,0:T(8,128)(2,1)}, bf16[256,2048]{1,0:T(8,128)(2,1)}, u32[]{:S(2)}, u32[]{:S(2)}) collective-permute-start(bf16[256,2048]{1,0:T(8,128)(2,1)} %collective-permute-done.13.refs_2_), channel_id=1, source_target_pairs={{0,1},{1,0},{2,3},{3,2},{4,5},{5,4},{6,7},{7,6},{8,9},{9,8},{10,11... | collective-permute-start | bytes 3145736 | tf_op jit(solution)/shard_map/ppermute | solution.py:337
  107.0 55.6 %collective-permute-start.18 = (bf16[256,2048]{1,0:T(8,128)(2,1)}, bf16[256,2048]{1,0:T(8,128)(2,1)}, u32[]{:S(2)}, u32[]{:S(2)}) collective-permute-start(bf16[256,2048]{1,0:T(8,128)(2,1)} %collective-permute-done.14.refs_3_), channel_id=1, source_target_pairs={{0,1},{1,0},{2,3},{3,2},{4,5},{5,4},{6,7},{7,6},{8,9},{9,8},{10,11... | collective-permute-start | bytes 3145736 | tf_op jit(solution)/shard_map/ppermute | solution.py:337
  109.4 10.1 %collective-permute-start.9 = (bf16[512,256]{1,0:T(8,128)(2,1)S(1)}, bf16[512,256]{1,0:T(8,128)(2,1)S(1)}, u32[]{:S(2)}, u32[]{:S(2)}) collective-permute-start(bf16[512,256]{1,0:T(8,128)(2,1)S(1)} %collective-permute-done.7.refs_1_), channel_id=1, source_target_pairs={{0,8},{8,16},{16,24},{24,32},{32,40},{40,48},{48,56},{56,64},{64,7... | collective-permute-start | bytes 786440 | tf_op jit(solution)/shard_map/ppermute | solution.py:355
  119.5 9.2 %collective-permute-start.10 = (bf16[512,256]{1,0:T(8,128)(2,1)S(1)}, bf16[512,256]{1,0:T(8,128)(2,1)S(1)}, u32[]{:S(2)}, u32[]{:S(2)}) collective-permute-start(bf16[512,256]{1,0:T(8,128)(2,1)S(1)} %collective-permute-done.8.refs_0_), channel_id=1, source_target_pairs={{0,8},{8,16},{16,24},{24,32},{32,40},{40,48},{48,56},{56,64},{64,7... | collective-permute-start | bytes 786440 | tf_op jit(solution)/shard_map/ppermute | solution.py:354
  128.8 19.7 %collective-permute-start.11 = (bf16[512,256]{1,0:T(8,128)(2,1)S(1)}, bf16[512,256]{1,0:T(8,128)(2,1)S(1)}, u32[]{:S(2)}, u32[]{:S(2)}) collective-permute-start(bf16[512,256]{1,0:T(8,128)(2,1)S(1)} %collective-permute-done.9.refs_1_), channel_id=1, source_target_pairs={{0,8},{8,16},{16,24},{24,32},{32,40},{40,48},{48,56},{56,64},{64,7... | collective-permute-start | bytes 786440 | tf_op jit(solution)/shard_map/ppermute | solution.py:355
  148.5 19.4 %copy-start.5 = (f32[2048]{0:T(1024)S(1)}, f32[2048]{0:T(1024)}, u32[]{:S(2)}) copy-start(f32[2048]{0:T(1024)} %param.13) | copy-start | bytes 24580
  154.7 0.7 copy-start.6
  155.4 0.7 copy-start.3
  156.1 11.8 %all-to-all-start.1 = ((bf16[8,64,256]{2,1,0:T(8,128)(2,1)}), bf16[8,64,256]{2,1,0:T(8,128)(2,1)S(1)}, u32[]{:S(2)}, u32[]{:S(2)}) async-start(bf16[8,64,256]{2,1,0:T(8,128)(2,1)} %bitcast.11), calls=%async_computation.1 | async-start | bytes 524288 | tf_op jit(solution)/shard_map/all_to_all | solution.py:396
  160.4 0.9 copy-start.7

commit v2 on v1

--- a/solution.py
+++ b/solution.py
@@ -150,7 +150,7 @@
     return (i & 31) * 16 + (i >> 5) * 4 + cls
 
 
-def own_kernel(q_ref, k_ref, v_ref, max_ref, sum_ref, acc_ref, s_ref, p_ref, bias_ref, count_ref, stat_ref):
+def own_kernel(q_ref, k_ref, v_ref, max_ref, sum_ref, acc_ref, s_ref, p_ref, bias_ref, count_ref):
     keys, width = k_ref.shape
     heads = width // HEAD_DIM
     o = query_places(pl.program_id(0)) - natural(lax.broadcasted_iota(jnp.int32, (1, keys), 1))
@@ -164,36 +164,47 @@
         s = s_ref[r : r + step, :] + bias_ref[mask, :]
         m = jnp.max(s, axis=1, keepdims=True)
         p = jnp.exp(s - m) * count_ref[mask, :]
-        stat_ref[0, r : r + step, :] = jnp.broadcast_to(m, (step, width))
-        stat_ref[1, r : r + step, :] = jnp.broadcast_to(jnp.sum(p, axis=1, keepdims=True), (step, width))
+        max_ref[r : r + step, :] = jnp.broadcast_to(m, (step, 128))
+        sum_ref[r : r + step, :] = jnp.broadcast_to(jnp.sum(p, axis=1, keepdims=True), (step, 128))
         p_ref[r : r + step, :] = p.astype(BF16)
-    pv = jnp.dot(p_ref[...], v_ref[...], preferred_element_type=F32)
-    max_ref[...] = own_heads(stat_ref[0])
-    sum_ref[...] = own_heads(stat_ref[1])
-    acc_ref[...] = own_heads(pv)
-
-
-def merged(q, key, value, bias, count, max_ref, sum_ref, acc_ref, s_ref, p_ref, stat_ref):
-    width = max_ref.shape[1]
+    acc_ref[...] = own_heads(jnp.dot(p_ref[...], v_ref[...], preferred_element_type=F32))
+
+
+def tiles(parts):
+    low = lax.broadcasted_iota(jnp.int32, parts[0].shape, 1) < HEAD_DIM
+    return jnp.concatenate([jnp.where(low, a, b) for a, b in zip(parts[0::2], parts[1::2])], axis=1)
+
+
+def merged(q, key, value, bias, count, max_ref, sum_ref, acc_ref, s_ref, p_ref):
+    heads = q.shape[1] // HEAD_DIM
+    wide = key.shape[0] // 128
     s_ref[...] = lax.dot_general(stack_heads(q), key, NT, preferred_element_type=F32)
-    for h in range(width // HEAD_DIM):
+    tops, sums, scales = [], [], []
+    for h in range(heads):
         part = slice(h * 128, (h + 1) * 128)
         s = s_ref[part, :] + bias
-        m = jnp.maximum(jnp.max(s, axis=1, keepdims=True), max_ref[:, h * HEAD_DIM : h * HEAD_DIM + 1])
-        p = jnp.exp(s - m)
+        old = max_ref[part, :]
+        m = jnp.maximum(jnp.max(s, axis=1, keepdims=True), old)
+        p = jnp.exp(s - jnp.concatenate([m] * wide, axis=1))
         if count is not None:
             p = p * count
         p_ref[part, :] = p.astype(BF16)
-        stat_ref[0, part, :] = jnp.broadcast_to(m, (128, width))
-        stat_ref[1, part, :] = jnp.broadcast_to(jnp.sum(p, axis=1, keepdims=True), (128, width))
-    pv = jnp.dot(p_ref[...], value, preferred_element_type=F32)
-    m = own_heads(stat_ref[0])
-    alpha = jnp.exp(max_ref[...] - m)
-    total = sum_ref[...] * alpha + own_heads(stat_ref[1])
-    return m, total, acc_ref[...] * alpha + own_heads(pv)
-
-
-def before_kernel(place_ref, q_ref, max_ref, sum_ref, acc_ref, k_ref, v_ref, new_max, new_sum, new_acc, s_ref, p_ref, stat_ref, tail_ref):
+        scale = jnp.exp(old - m)
+        tops.append(m)
+        sums.append(sum_ref[part, :] * scale + jnp.sum(p, axis=1, keepdims=True))
+        scales.append(scale)
+    pv = own_heads(jnp.dot(p_ref[...], value, preferred_element_type=F32))
+    return tops, sums, acc_ref[...] * tiles(scales) + pv
+
+
+def store_state(state, max_ref, sum_ref, acc_ref):
+    tops, sums, acc_ref[...] = state
+    for h in range(len(tops)):
+        max_ref[h * 128 : (h + 1) * 128, :] = tops[h]
+        sum_ref[h * 128 : (h + 1) * 128, :] = sums[h]
+
+
+def before_kernel(place_ref, q_ref, max_ref, sum_ref, acc_ref, k_ref, v_ref, new_max, new_sum, new_acc, s_ref, p_ref, tail_ref):
     cls = pl.program_id(0)
     keys = k_ref.shape[0]
     mine = pl.ds(pl.multiple_of(cls * 128, 128), 128)
@@ -216,36 +227,33 @@
     bias = jnp.where(count > 0, 0.0, LOW).astype(F32)
     key = jnp.concatenate([k_ref[mine, :], tail_ref[0]], axis=0)
     value = jnp.concatenate([v_ref[mine, :], tail_ref[1]], axis=0)
-    state = merged(q_ref[...], key, value, bias, count, max_ref, sum_ref, acc_ref, s_ref, p_ref, stat_ref)
-    for ref, part in zip((new_max, new_sum, new_acc), state):
-        ref[...] = part
+    store_state(merged(q_ref[...], key, value, bias, count, max_ref, sum_ref, acc_ref, s_ref, p_ref), new_max, new_sum, new_acc)
 
 
 def far_kernel(backs, last, place_ref, q_ref, max_ref, sum_ref, acc_ref, *refs):
     count = len(backs)
     sources, outs = refs[: 2 * count], refs[2 * count :]
-    s_ref, p_ref, stat_ref = outs[-3:]
+    s_ref, p_ref = outs[-2:]
     bias = jnp.concatenate([far_bias(place_ref[0], back) for back in backs], axis=1)
     key = jnp.concatenate([ref[...] for ref in sources[0::2]], axis=0)
     value = jnp.concatenate([ref[...] for ref in sources[1::2]], axis=0)
-    m, total, acc = merged(q_ref[...], key, value, bias, None, max_ref, sum_ref, acc_ref, s_ref, p_ref, stat_ref)
-    if last:
-        cls = pl.program_id(0)
-        out_ref, log_ref, att_ref = outs[:3]
-        att_ref[pl.ds(pl.multiple_of(cls * 128, 128), 128), :] = (acc / total).astype(BF16)
-        lw = m + jnp.log(total)
-        lane = lax.broadcasted_iota(jnp.int32, log_ref.shape, 1)
-        compact = jnp.zeros(log_ref.shape, F32)
-        for h in range(lw.shape[1] // HEAD_DIM):
-            compact = jnp.where(lane == h, lw[:, h * HEAD_DIM : h * HEAD_DIM + 1], compact)
-        log_ref[...] = compact
-
-        @pl.when(cls == pl.num_programs(0) - 1)
-        def _():
-            out_ref[...] = permuted(to_natural(att_ref.shape[0]), att_ref[...])
-    else:
-        for ref, part in zip(outs[:3], (m, total, acc)):
-            ref[...] = part
+    state = merged(q_ref[...], key, value, bias, None, max_ref, sum_ref, acc_ref, s_ref, p_ref)
+    if not last:
+        store_state(state, *outs[:3])
+        return
+    tops, sums, acc = state
+    cls = pl.program_id(0)
+    out_ref, log_ref, att_ref = outs[:3]
+    att_ref[pl.ds(pl.multiple_of(cls * 128, 128), 128), :] = (acc / tiles(sums)).astype(BF16)
+    lane = lax.broadcasted_iota(jnp.int32, log_ref.shape, 1)
+    logs = jnp.zeros(log_ref.shape, F32)
+    for h in range(len(tops)):
+        logs = jnp.where(lane == h, tops[h] + jnp.log(sums[h]), logs)
+    log_ref[...] = logs
+
+    @pl.when(cls == pl.num_programs(0) - 1)
+    def _():
+        out_ref[...] = permuted(to_natural(att_ref.shape[0]), att_ref[...])
 
 
 def log_kernel(lw_ref, log_ref):
@@ -355,41 +363,44 @@
         values.append(lax.ppermute(values[-1], SP, forward))
     whole = pl.BlockSpec(row, lambda c: (0, 0))
     part = pl.BlockSpec((128, width), lambda c: (c, 0))
-    pair = ((512, 256), F32), ((512, 256), BF16), ((2, 512, width), F32)
+    stat = pl.BlockSpec((512, 128), lambda c: (c, 0))
+    stats = (4 * rows, 128)
+    outs = [(stats, F32), (stats, F32), (row, F32)]
+    pair = ((512, 256), F32), ((512, 256), BF16)
     state = kernel_call(
         own_kernel,
-        [(row, F32)] * 3,
+        outs,
         (query, keys[0], values[0]),
         8 * rows * rows * width,
-        10,
-        [((512, 512), F32), ((512, 512), BF16), ((128, 512), F32), ((128, 512), F32), ((2, 512, width), F32)],
+        12,
+        [((512, 512), F32), ((512, 512), BF16), ((128, 512), F32), ((128, 512), F32)],
         grid=(rows // 128,),
         in_specs=[part, whole, whole],
-        out_specs=(part,) * 3,
+        out_specs=(stat, stat, part),
     )
     state = kernel_call(
         before_kernel,
-        [(row, F32)] * 3,
+        outs,
         (place, query, *state, keys[1], values[1]),
         4 * rows * rows * width,
-        10,
+        12,
         [*pair, ((2, 128, width), BF16)],
         grid=(rows // 128,),
-        in_specs=[SMEM] + [part] * 4 + [whole, whole],
-        out_specs=(part,) * 3,
+        in_specs=[SMEM, part, stat, stat, part, whole, whole],
+        out_specs=(stat, stat, part),
     )
     for back in (2, 3, 4):
         last = back == 4
         state = kernel_call(
             functools.partial(far_kernel, (back,), last),
-            [(row, BF16), ((rows, 128), F32)] if last else [(row, F32)] * 3,
+            [(row, BF16), ((rows, 128), F32)] if last else outs,
             (place, query, *state, keys[back], values[back]),
             4 * rows * 512 * width,
             16,
-            ([(row, BF16)] if last else []) + [((512, 128), t) for t in (F32, BF16)] + [((2, 512, width), F32)],
+            ([(row, BF16)] if last else []) + [((512, 128), t) for t in (F32, BF16)],
             grid=(rows // 128,),
-            in_specs=[SMEM] + [part] * 6,
-            out_specs=(whole, pl.BlockSpec((128, 128), lambda c: (c, 0))) if last else (part,) * 3,
+            in_specs=[SMEM, part, stat, stat, part, part, part],
+            out_specs=(whole, pl.BlockSpec((128, 128), lambda c: (c, 0))) if last else (stat, stat, part),
         )
     attended, logs = state
 

time: 174 us -> 168 us (0.966)
  Pallas kernels: 36.5 us -> 30.6 us
    pallas_call x11, Pallas kernels: 36.5 us -> 30.6 us  [kernel_call(): pl.pallas_call(body, out_shape=tuple((jax.ShapeDtypeStruct(s, t) for s, t...]
  transfers between devices with their start and end apart: 21 -> 21, of which waited for: 9 -> 9; matrix products, arithmetic and copies ran while one was open for 1% -> 1% of each run, Pallas kernels for 17% -> 14%
where the time goes in v2:
time: 168 us; the launch traced here: 167 us
  starting transfers between devices  84.9 us (51%)
  waiting for transfers between devices  45.7 us (27%)
  Pallas kernels  30.6 us (18%)
  local copies, waits for them, and re-layouts  4.58 us (3%)
    pallas_call x11, Pallas kernels, kernel_call(): pl.pallas_call(body, out_shape=tuple((jax.ShapeDtypeStruct(s, t) for s, t...  30.6 us
    all_to_all x1, waiting for transfers between devices, layer(): lax.all_to_all(copies, ('zh', 'y'), split_axis=0, concat_axis=0, tiled=True)  19.3 us
    ppermute x4, starting transfers between devices, layer(): keys.append(lax.ppermute(keys[-1], SP, forward))  17 us
    all_to_all x1, starting transfers between devices, layer(): lax.all_to_all(copies, ('zh', 'y'), split_axis=0, concat_axis=0, tiled=True)  16.1 us
    ppermute x4, starting transfers between devices, layer(): values.append(lax.ppermute(values[-1], SP, forward))  14.1 us
    ppermute x3, starting transfers between devices, layer(): groups.append(lax.ppermute(out_proj, 'x', ring(4, steps)))  10.8 us
    ppermute x4, waiting for transfers between devices, layer(): keys.append(lax.ppermute(keys[-1], SP, forward))  9.63 us
    ppermute x4, waiting for transfers between devices, layer(): values.append(lax.ppermute(values[-1], SP, forward))  8.94 us
  transfers between devices with their start and end apart: 21, of which 9 were waited for; matrix products, arithmetic and copies ran while one was open for 1% of the time, Pallas kernels for 14%

profile of v2, /device:TPU:24, one launch (start us, length us, event | category | flops | bytes accessed | tf_op | source)
XLA Modules:
  0.0 167.2 jit_solution(16056567751317855821)
XLA Ops:
  0.6 2.3 %shard_map.87 = bf16[32,32,512]{2,1,0:T(8,128)(2,1)} custom-call(bf16[32,256]{1,0:T(8,128)(2,1)} %key_ref.1, bf16[32,256]{1,0:T(8,128)(2,1)} %value_ref.1), custom_call_target="tpu_custom_call" | custom-call | flops 1000 | bytes 32768 | tf_op jit(solution)/shard_map/pallas_call | solution.py:303
  2.9 16.1 %all-to-all-start = ((bf16[32,32,512]{2,1,0:T(8,128)(2,1)}), bf16[32,32,512]{2,1,0:T(8,128)(2,1)S(1)}, u32[]{:S(2)}, u32[]{:S(2)}) async-start(bf16[32,32,512]{2,1,0:T(8,128)(2,1)} %shard_map.87), calls=%async_computation | async-start | bytes 2097152 | tf_op jit(solution)/shard_map/all_to_all | solution.py:333
  19.0 3.4 %collective-permute-start.12 = (bf16[256,2048]{1,0:T(8,128)(2,1)}, bf16[256,2048]{1,0:T(8,128)(2,1)}, u32[]{:S(2)}, u32[]{:S(2)}) collective-permute-start(bf16[256,2048]{1,0:T(8,128)(2,1)} %refs_0_.1), channel_id=1, source_target_pairs={{0,2},{2,4},{4,6},{6,0},{1,3},{3,5},{5,7},{7,1},{8,10},{10,12},{12... | collective-permute-start | bytes 3145736 | tf_op jit(solution)/shard_map/ppermute | solution.py:343
  22.4 3.7 %collective-permute-start.13 = (bf16[256,2048]{1,0:T(8,128)(2,1)}, bf16[256,2048]{1,0:T(8,128)(2,1)}, u32[]{:S(2)}, u32[]{:S(2)}) collective-permute-start(bf16[256,2048]{1,0:T(8,128)(2,1)} %refs_0_.1), channel_id=1, source_target_pairs={{0,6},{2,0},{4,2},{6,4},{1,7},{3,1},{5,3},{7,5},{8,14},{10,8},{12,... | collective-permute-start | bytes 3145736 | tf_op jit(solution)/shard_map/ppermute | solution.py:343
  26.1 3.7 %collective-permute-start.14 = (bf16[256,2048]{1,0:T(8,128)(2,1)}, bf16[256,2048]{1,0:T(8,128)(2,1)}, u32[]{:S(2)}, u32[]{:S(2)}) collective-permute-start(bf16[256,2048]{1,0:T(8,128)(2,1)} %refs_0_.1), channel_id=1, source_target_pairs={{0,4},{2,6},{4,0},{6,2},{1,5},{3,7},{5,1},{7,3},{8,12},{10,14},{12... | collective-permute-start | bytes 3145736 | tf_op jit(solution)/shard_map/ppermute | solution.py:343
  29.9 19.3 %all-to-all-done = bf16[32,32,512]{2,1,0:T(8,128)(2,1)S(1)} async-done(((bf16[32,32,512]{2,1,0:T(8,128)(2,1)}), bf16[32,32,512]{2,1,0:T(8,128)(2,1)S(1)}, u32[]{:S(2)}, u32[]{:S(2)}) %all-to-all-start) | async-done | bytes 1048608 | tf_op jit(solution)/shard_map/all_to_all | solution.py:333
  49.2 1.0 fusion
  50.2 4.1 %collective-permute-start = (bf16[2,256,256]{2,1,0:T(8,128)(2,1)}, bf16[2,256,256]{2,1,0:T(8,128)(2,1)S(1)}, u32[]{:S(2)}, u32[]{:S(2)}) collective-permute-start(bf16[2,256,256]{2,1,0:T(8,128)(2,1)} %get-tuple-element.37), channel_id=1, source_target_pairs={{0,64},{64,128},{128,192},{192,256},{256,320},{320,384},{384,448},... | collective-permute-start | bytes 786440 | tf_op jit(solution)/shard_map/ppermute | solution.py:337
  54.3 3.0 %collective-permute-start.1 = (bf16[2,256,256]{2,1,0:T(8,128)(2,1)}, bf16[2,256,256]{2,1,0:T(8,128)(2,1)}, u32[]{:S(2)}, u32[]{:S(2)}) collective-permute-start(bf16[2,256,256]{2,1,0:T(8,128)(2,1)} %get-tuple-element.36), channel_id=1, source_target_pairs={{0,448},{64,0},{128,64},{192,128},{256,192},{320,256},{384,320},{4... | collective-permute-start | bytes 786440 | tf_op jit(solution)/shard_map/ppermute | solution.py:338
  57.3 0.3 multiply_cosine_fusion
  57.6 2.3 %collective-permute-done.below_ref = bf16[2,256,256]{2,1,0:T(8,128)(2,1)S(1)} collective-permute-done((bf16[2,256,256]{2,1,0:T(8,128)(2,1)}, bf16[2,256,256]{2,1,0:T(8,128)(2,1)S(1)}, u32[]{:S(2)}, u32[]{:S(2)}) %collective-permute-start) | collective-permute-done | bytes 262176 | tf_op jit(solution)/shard_map/ppermute | solution.py:337
  59.9 2.9 %collective-permute-start.2 = (bf16[2,256,256]{2,1,0:T(8,128)(2,1)}, bf16[2,256,256]{2,1,0:T(8,128)(2,1)S(1)}, u32[]{:S(2)}, u32[]{:S(2)}) collective-permute-start(bf16[2,256,256]{2,1,0:T(8,128)(2,1)} %get-tuple-element.35), channel_id=1, source_target_pairs={{0,64},{64,128},{128,192},{192,256},{256,320},{320,384},{384,448},... | collective-permute-start | bytes 786440 | tf_op jit(solution)/shard_map/ppermute | solution.py:337
  62.7 0.1 pad_add_fusion.place_ref
  62.8 0.2 collective-permute-done.1.above_ref
  63.0 4.0 %collective-permute-start.3 = (bf16[2,256,256]{2,1,0:T(8,128)(2,1)}, bf16[2,256,256]{2,1,0:T(8,128)(2,1)S(1)}, u32[]{:S(2)}, u32[]{:S(2)}) collective-permute-start(bf16[2,256,256]{2,1,0:T(8,128)(2,1)} %get-tuple-element.34), channel_id=1, source_target_pairs={{0,448},{64,0},{128,64},{192,128},{256,192},{320,256},{384,320},{4... | collective-permute-start | bytes 786440 | tf_op jit(solution)/shard_map/ppermute | solution.py:338
  67.1 0.0 copy-start.1
  67.1 1.2 copy-done.1
  68.3 2.7 %shard_map.86 = (bf16[512,2048]{1,0:T(8,128)(2,1)S(1)}, bf16[512,256]{1,0:T(8,128)(2,1)S(1)}) custom-call(bf16[512,2048]{1,0:T(8,128)(2,1)S(1)} %copy-done, f32[1,2048]{1,0:T(1,128)S(1)} %bitcast.12, bf16[2048,256]{1,0:T(8,128)(2,1)S(1)} %copy-done.1, f32[2,32,512]{2,1,0:T(8,128)S(1)} %pad_maximum_fusion.turn_ref), custom_call_target="tpu_custom_call" | custom-call | flops 536870912 | bytes 3284992 | tf_op jit(solution)/shard_map/pallas_call | solution.py:303
  71.0 2.4 %shard_map.88.k_ref = bf16[512,256]{1,0:T(8,128)(2,1)S(1)} custom-call(s32[4]{0:T(128)S(1)} %pad_add_fusion.place_ref, bf16[512,2048]{1,0:T(8,128)(2,1)S(1)} %get-tuple-element.19.normed_ref, bf16[4,256,512]{2,1,0:T(8,128)(2,1)S(1)} %bitcast.9, bf16[2,256,256]{2,1,0:T(8,128)(2,1)S(1)} %collective-permute-done.below_ref, ...), custom_call_target="tpu_custom_call" | custom-call | flops 536870912 | bytes 3801104 | tf_op jit(solution)/shard_map/pallas_call | solution.py:303
  73.4 0.0 copy-start.2
  73.4 0.0 collective-permute-done.2.below_ref
  73.4 3.1 %collective-permute-start.4 = (bf16[512,256]{1,0:T(8,128)(2,1)S(1)}, bf16[512,256]{1,0:T(8,128)(2,1)S(1)}, u32[]{:S(2)}, u32[]{:S(2)}) collective-permute-start(bf16[512,256]{1,0:T(8,128)(2,1)S(1)} %shard_map.88.k_ref), channel_id=1, source_target_pairs={{0,8},{8,16},{16,24},{24,32},{32,40},{40,48},{48,56},{56,64},{64,7... | collective-permute-start | bytes 786440 | tf_op jit(solution)/shard_map/ppermute | solution.py:362
  76.5 0.0 collective-permute-done.3.above_ref
  76.5 1.8 %shard_map.89.v_ref = bf16[512,256]{1,0:T(8,128)(2,1)S(1)} custom-call(s32[4]{0:T(128)S(1)} %pad_add_fusion.place_ref, bf16[512,2048]{1,0:T(8,128)(2,1)S(1)} %get-tuple-element.19.normed_ref, bf16[4,256,512]{2,1,0:T(8,128)(2,1)S(1)} %bitcast.10, bf16[2,256,256]{2,1,0:T(8,128)(2,1)S(1)} %collective-permute-done.2.below_ref, ...), custom_call_target="tpu_custom_call" | custom-call | flops 536870912 | bytes 3670032 | tf_op jit(solution)/shard_map/pallas_call | solution.py:303
  78.3 2.4 %collective-permute-start.5 = (bf16[512,256]{1,0:T(8,128)(2,1)S(1)}, bf16[512,256]{1,0:T(8,128)(2,1)S(1)}, u32[]{:S(2)}, u32[]{:S(2)}) collective-permute-start(bf16[512,256]{1,0:T(8,128)(2,1)S(1)} %shard_map.89.v_ref), channel_id=1, source_target_pairs={{0,8},{8,16},{16,24},{24,32},{32,40},{40,48},{48,56},{56,64},{64,7... | collective-permute-start | bytes 786440 | tf_op jit(solution)/shard_map/ppermute | solution.py:363
  80.7 3.0 %collective-permute-done.4.k_ref = bf16[512,256]{1,0:T(8,128)(2,1)S(1)} collective-permute-done((bf16[512,256]{1,0:T(8,128)(2,1)S(1)}, bf16[512,256]{1,0:T(8,128)(2,1)S(1)}, u32[]{:S(2)}, u32[]{:S(2)}) %collective-permute-start.4) | collective-permute-done | bytes 262176 | tf_op jit(solution)/shard_map/ppermute | solution.py:362
  83.7 4.9 %collective-permute-start.6 = (bf16[512,256]{1,0:T(8,128)(2,1)S(1)}, bf16[512,256]{1,0:T(8,128)(2,1)S(1)}, u32[]{:S(2)}, u32[]{:S(2)}) collective-permute-start(bf16[512,256]{1,0:T(8,128)(2,1)S(1)} %collective-permute-done.4.k_ref), channel_id=1, source_target_pairs={{0,8},{8,16},{16,24},{24,32},{32,40},{40,48},{48,56},{56,64},{64,7... | collective-permute-start | bytes 786440 | tf_op jit(solution)/shard_map/ppermute | solution.py:362
  88.6 0.7 collective-permute-done.5.v_ref
  89.4 4.9 %collective-permute-start.7 = (bf16[512,256]{1,0:T(8,128)(2,1)S(1)}, bf16[512,256]{1,0:T(8,128)(2,1)S(1)}, u32[]{:S(2)}, u32[]{:S(2)}) collective-permute-start(bf16[512,256]{1,0:T(8,128)(2,1)S(1)} %collective-permute-done.5.v_ref), channel_id=1, source_target_pairs={{0,8},{8,16},{16,24},{24,32},{32,40},{40,48},{48,56},{56,64},{64,7... | collective-permute-start | bytes 786440 | tf_op jit(solution)/shard_map/ppermute | solution.py:363
  94.2 0.8 collective-permute-done.6.refs_0_
  95.1 5.6 %collective-permute-start.8 = (bf16[512,256]{1,0:T(8,128)(2,1)S(1)}, bf16[512,256]{1,0:T(8,128)(2,1)S(1)}, u32[]{:S(2)}, u32[]{:S(2)}) collective-permute-start(bf16[512,256]{1,0:T(8,128)(2,1)S(1)} %collective-permute-done.6.refs_0_), channel_id=1, source_target_pairs={{0,8},{8,16},{16,24},{24,32},{32,40},{40,48},{48,56},{56,64},{64,7... | collective-permute-start | bytes 786440 | tf_op jit(solution)/shard_map/ppermute | solution.py:362
  100.7 0.0 collective-permute-done.12.refs_1_
  100.7 0.0 copy-done.2
  100.7 1.9 %collective-permute-start.15 = (bf16[256,2048]{1,0:T(8,128)(2,1)S(1)}, bf16[256,2048]{1,0:T(8,128)(2,1)S(1)}, u32[]{:S(2)}, u32[]{:S(2)}) collective-permute-start(bf16[256,2048]{1,0:T(8,128)(2,1)S(1)} %copy-done.2), channel_id=1, source_target_pairs={{0,1},{1,0},{2,3},{3,2},{4,5},{5,4},{6,7},{7,6},{8,9},{9,8},{10,11... | collective-permute-start | bytes 3145736 | tf_op jit(solution)/shard_map/ppermute | solution.py:345
  102.6 0.0 collective-permute-done.13.refs_2_
  102.6 2.4 %collective-permute-start.16 = (bf16[256,2048]{1,0:T(8,128)(2,1)}, bf16[256,2048]{1,0:T(8,128)(2,1)S(1)}, u32[]{:S(2)}, u32[]{:S(2)}) collective-permute-start(bf16[256,2048]{1,0:T(8,128)(2,1)} %collective-permute-done.12.refs_1_), channel_id=1, source_target_pairs={{0,1},{1,0},{2,3},{3,2},{4,5},{5,4},{6,7},{7,6},{8,9},{9,8},{10,11... | collective-permute-start | bytes 3145736 | tf_op jit(solution)/shard_map/ppermute | solution.py:345
  105.0 0.0 collective-permute-done.14.refs_3_
  105.1 1.9 %collective-permute-start.17 = (bf16[256,2048]{1,0:T(8,128)(2,1)}, bf16[256,2048]{1,0:T(8,128)(2,1)}, u32[]{:S(2)}, u32[]{:S(2)}) collective-permute-start(bf16[256,2048]{1,0:T(8,128)(2,1)} %collective-permute-done.13.refs_2_), channel_id=1, source_target_pairs={{0,1},{1,0},{2,3},{3,2},{4,5},{5,4},{6,7},{7,6},{8,9},{9,8},{10,11... | collective-permute-start | bytes 3145736 | tf_op jit(solution)/shard_map/ppermute | solution.py:345
  107.0 0.0 collective-permute-done.7.refs_1_
  107.0 2.4 %collective-permute-start.18 = (bf16[256,2048]{1,0:T(8,128)(2,1)}, bf16[256,2048]{1,0:T(8,128)(2,1)}, u32[]{:S(2)}, u32[]{:S(2)}) collective-permute-start(bf16[256,2048]{1,0:T(8,128)(2,1)} %collective-permute-done.14.refs_3_), channel_id=1, source_target_pairs={{0,1},{1,0},{2,3},{3,2},{4,5},{5,4},{6,7},{7,6},{8,9},{9,8},{10,11... | collective-permute-start | bytes 3145736 | tf_op jit(solution)/shard_map/ppermute | solution.py:345
  109.4 0.0 collective-permute-done.8.refs_0_
  109.4 1.9 %collective-permute-start.9 = (bf16[512,256]{1,0:T(8,128)(2,1)S(1)}, bf16[512,256]{1,0:T(8,128)(2,1)S(1)}, u32[]{:S(2)}, u32[]{:S(2)}) collective-permute-start(bf16[512,256]{1,0:T(8,128)(2,1)S(1)} %collective-permute-done.7.refs_1_), channel_id=1, source_target_pairs={{0,8},{8,16},{16,24},{24,32},{32,40},{40,48},{48,56},{56,64},{64,7... | collective-permute-start | bytes 786440 | tf_op jit(solution)/shard_map/ppermute | solution.py:363
  111.4 8.2 %collective-permute-done.9.refs_1_ = bf16[512,256]{1,0:T(8,128)(2,1)S(1)} collective-permute-done((bf16[512,256]{1,0:T(8,128)(2,1)S(1)}, bf16[512,256]{1,0:T(8,128)(2,1)S(1)}, u32[]{:S(2)}, u32[]{:S(2)}) %collective-permute-start.9) | collective-permute-done | bytes 262176 | tf_op jit(solution)/shard_map/ppermute | solution.py:363
  119.5 3.4 %collective-permute-start.10 = (bf16[512,256]{1,0:T(8,128)(2,1)S(1)}, bf16[512,256]{1,0:T(8,128)(2,1)S(1)}, u32[]{:S(2)}, u32[]{:S(2)}) collective-permute-start(bf16[512,256]{1,0:T(8,128)(2,1)S(1)} %collective-permute-done.8.refs_0_), channel_id=1, source_target_pairs={{0,8},{8,16},{16,24},{24,32},{32,40},{40,48},{48,56},{56,64},{64,7... | collective-permute-start | bytes 786440 | tf_op jit(solution)/shard_map/ppermute | solution.py:362
  122.9 5.8 %collective-permute-done.10.refs_0_ = bf16[512,256]{1,0:T(8,128)(2,1)S(1)} collective-permute-done((bf16[512,256]{1,0:T(8,128)(2,1)S(1)}, bf16[512,256]{1,0:T(8,128)(2,1)S(1)}, u32[]{:S(2)}, u32[]{:S(2)}) %collective-permute-start.10) | collective-permute-done | bytes 262176 | tf_op jit(solution)/shard_map/ppermute | solution.py:362
  128.8 4.9 %collective-permute-start.11 = (bf16[512,256]{1,0:T(8,128)(2,1)S(1)}, bf16[512,256]{1,0:T(8,128)(2,1)S(1)}, u32[]{:S(2)}, u32[]{:S(2)}) collective-permute-start(bf16[512,256]{1,0:T(8,128)(2,1)S(1)} %collective-permute-done.9.refs_1_), channel_id=1, source_target_pairs={{0,8},{8,16},{16,24},{24,32},{32,40},{40,48},{48,56},{56,64},{64,7... | collective-permute-start | bytes 786440 | tf_op jit(solution)/shard_map/ppermute | solution.py:363
  133.7 3.5 %shard_map.90 = (f32[2048,128]{1,0:T(8,128)S(1)}, f32[2048,128]{1,0:T(8,128)S(1)}, f32[512,256]{1,0:T(8,128)S(1)}) custom-call(bf16[512,256]{1,0:T(8,128)(2,1)S(1)} %get-tuple-element.18.q_ref, bf16[512,256]{1,0:T(8,128)(2,1)S(1)} %shard_map.88.k_ref, bf16[512,256]{1,0:T(8,128)(2,1)S(1)} %shard_map.89.v_ref), custom_call_target="tpu_custom_call" | custom-call | flops 536870912 | bytes 786432 | tf_op jit(solution)/shard_map/pallas_call | solution.py:303
  137.2 3.0 %shard_map.91 = (f32[2048,128]{1,0:T(8,128)S(1)}, f32[2048,128]{1,0:T(8,128)S(1)}, f32[512,256]{1,0:T(8,128)S(1)}) custom-call(s32[4]{0:T(128)S(1)} %pad_add_fusion.place_ref, bf16[512,256]{1,0:T(8,128)(2,1)S(1)} %get-tuple-element.18.q_ref, f32[2048,128]{1,0:T(8,128)S(1)} %get-tuple-element.20.max_ref, f32[2048,128]{1,0:T(8,128)S(1)} %get-tuple-element.21.sum_ref, ...), custom_call_target="tpu_custom_call" | custom-call | flops 268435456 | bytes 3407888 | tf_op jit(solution)/shard_map/pallas_call | solution.py:303
  140.2 2.8 %shard_map.92 = (f32[2048,128]{1,0:T(8,128)S(1)}, f32[2048,128]{1,0:T(8,128)S(1)}, f32[512,256]{1,0:T(8,128)S(1)}) custom-call(s32[4]{0:T(128)S(1)} %pad_add_fusion.place_ref, bf16[512,256]{1,0:T(8,128)(2,1)S(1)} %get-tuple-element.18.q_ref, f32[2048,128]{1,0:T(8,128)S(1)} %get-tuple-element.23.max_ref, f32[2048,128]{1,0:T(8,128)S(1)} %get-tuple-element.24.sum_ref, ...), custom_call_target="tpu_custom_call" | custom-call | flops 268435456 | bytes 3407888 | tf_op jit(solution)/shard_map/pallas_call | solution.py:303
  142.9 2.8 %shard_map.93 = (f32[2048,128]{1,0:T(8,128)S(1)}, f32[2048,128]{1,0:T(8,128)S(1)}, f32[512,256]{1,0:T(8,128)S(1)}) custom-call(s32[4]{0:T(128)S(1)} %pad_add_fusion.place_ref, bf16[512,256]{1,0:T(8,128)(2,1)S(1)} %get-tuple-element.18.q_ref, f32[2048,128]{1,0:T(8,128)S(1)} %get-tuple-element.26.max_ref, f32[2048,128]{1,0:T(8,128)S(1)} %get-tuple-element.27.sum_ref, ...), custom_call_target="tpu_custom_call" | custom-call | flops 268435456 | bytes 3407888 | tf_op jit(solution)/shard_map/pallas_call | solution.py:303
  145.7 0.0 collective-permute-done.11.refs_1_
  145.7 0.0 copy-start.5
  145.7 3.1 %shard_map.94 = (bf16[512,256]{1,0:T(8,128)(2,1)S(1)}, f32[512,128]{1,0:T(8,128)S(1)}) custom-call(s32[4]{0:T(128)S(1)} %pad_add_fusion.place_ref, bf16[512,256]{1,0:T(8,128)(2,1)S(1)} %get-tuple-element.18.q_ref, f32[2048,128]{1,0:T(8,128)S(1)} %get-tuple-element.29.max_ref, f32[2048,128]{1,0:T(8,128)S(1)} %get-tuple-element.30.sum_ref, ...), custom_call_target="tpu_custom_call" | custom-call | flops 268435456 | bytes 3407888 | tf_op jit(solution)/shard_map/pallas_call | solution.py:303
  148.8 0.7 copy-done.6
  149.5 0.7 copy-done.3
  150.2 4.3 %all-to-all-start.1 = ((bf16[8,64,256]{2,1,0:T(8,128)(2,1)}), bf16[8,64,256]{2,1,0:T(8,128)(2,1)S(1)}, u32[]{:S(2)}, u32[]{:S(2)}) async-start(bf16[8,64,256]{2,1,0:T(8,128)(2,1)} %bitcast.11), calls=%async_computation.1 | async-start | bytes 524288 | tf_op jit(solution)/shard_map/all_to_all | solution.py:407
  154.5 0.9 copy-done.7
  155.5 1.2 shard_map.96
  156.7 0.0 collective-permute-done.15.refs_4_
  156.7 0.0 collective-permute-done.16.refs_5_
  156.7 0.0 collective-permute-done.17.refs_6_
  156.7 0.0 collective-permute-done.18.refs_7_
  156.7 5.3 %all-to-all-done.1.att_ref = bf16[8,64,256]{2,1,0:T(8,128)(2,1)S(1)} async-done(((bf16[8,64,256]{2,1,0:T(8,128)(2,1)}), bf16[8,64,256]{2,1,0:T(8,128)(2,1)S(1)}, u32[]{:S(2)}, u32[]{:S(2)}) %all-to-all-start.1) | async-done | bytes 262176 | tf_op jit(solution)/shard_map/all_to_all | solution.py:407
  162.0 5.1 %shard_map.95 = bf16[64,2048]{1,0:T(8,128)(2,1)} custom-call(s32[4]{0:T(128)S(1)} %pad_add_fusion.place_ref, bf16[8,64,256]{2,1,0:T(8,128)(2,1)S(1)} %all-to-all-done.1.att_ref, bf16[256,2048]{1,0:T(8,128)(2,1)S(1)} %copy-done.2, bf16[256,2048]{1,0:T(8,128)(2,1)} %collective-permute-done.12.refs_1_, bf16[256,2048]{1,0:T(8,128)(2,1)} %collective-permute-done.13.refs_2_, ...), custom_call_target="tpu_custom_call" | custom-call | flops 536870912 | bytes 8658960 | tf_op jit(solution)/shard_map/pallas_call | solution.py:303
  (11 shorter events, 0.0 us)
Async XLA Ops:
  2.9 64.1 %copy-start = (bf16[512,2048]{1,0:T(8,128)(2,1)S(1)}, bf16[512,2048]{1,0:T(8,128)(2,1)}, u32[]{:S(2)}) copy-start(bf16[512,2048]{1,0:T(8,128)(2,1)} %hidden_ref.1) | copy-start | bytes 6291460
  2.9 64.1 %copy-start.4 = (f32[2048]{0:T(1024)S(1)}, f32[2048]{0:T(1024)}, u32[]{:S(2)}) copy-start(f32[2048]{0:T(1024)} %param.8) | copy-start | bytes 24580
  2.9 46.3 %all-to-all-start = ((bf16[32,32,512]{2,1,0:T(8,128)(2,1)}), bf16[32,32,512]{2,1,0:T(8,128)(2,1)S(1)}, u32[]{:S(2)}, u32[]{:S(2)}) async-start(bf16[32,32,512]{2,1,0:T(8,128)(2,1)} %shard_map.87), calls=%async_computation | async-start | bytes 2097152 | tf_op jit(solution)/shard_map/all_to_all | solution.py:333
  19.0 81.7 %collective-permute-start.12 = (bf16[256,2048]{1,0:T(8,128)(2,1)}, bf16[256,2048]{1,0:T(8,128)(2,1)}, u32[]{:S(2)}, u32[]{:S(2)}) collective-permute-start(bf16[256,2048]{1,0:T(8,128)(2,1)} %refs_0_.1), channel_id=1, source_target_pairs={{0,2},{2,4},{4,6},{6,0},{1,3},{3,5},{5,7},{7,1},{8,10},{10,12},{12... | collective-permute-start | bytes 3145736 | tf_op jit(solution)/shard_map/ppermute | solution.py:343
  22.4 80.2 %collective-permute-start.13 = (bf16[256,2048]{1,0:T(8,128)(2,1)}, bf16[256,2048]{1,0:T(8,128)(2,1)}, u32[]{:S(2)}, u32[]{:S(2)}) collective-permute-start(bf16[256,2048]{1,0:T(8,128)(2,1)} %refs_0_.1), channel_id=1, source_target_pairs={{0,6},{2,0},{4,2},{6,4},{1,7},{3,1},{5,3},{7,5},{8,14},{10,8},{12,... | collective-permute-start | bytes 3145736 | tf_op jit(solution)/shard_map/ppermute | solution.py:343
  26.1 78.9 %collective-permute-start.14 = (bf16[256,2048]{1,0:T(8,128)(2,1)}, bf16[256,2048]{1,0:T(8,128)(2,1)}, u32[]{:S(2)}, u32[]{:S(2)}) collective-permute-start(bf16[256,2048]{1,0:T(8,128)(2,1)} %refs_0_.1), channel_id=1, source_target_pairs={{0,4},{2,6},{4,0},{6,2},{1,5},{3,7},{5,1},{7,3},{8,12},{10,14},{12... | collective-permute-start | bytes 3145736 | tf_op jit(solution)/shard_map/ppermute | solution.py:343
  50.2 9.7 %collective-permute-start = (bf16[2,256,256]{2,1,0:T(8,128)(2,1)}, bf16[2,256,256]{2,1,0:T(8,128)(2,1)S(1)}, u32[]{:S(2)}, u32[]{:S(2)}) collective-permute-start(bf16[2,256,256]{2,1,0:T(8,128)(2,1)} %get-tuple-element.37), channel_id=1, source_target_pairs={{0,64},{64,128},{128,192},{192,256},{256,320},{320,384},{384,448},... | collective-permute-start | bytes 786440 | tf_op jit(solution)/shard_map/ppermute | solution.py:337
  54.3 8.8 %collective-permute-start.1 = (bf16[2,256,256]{2,1,0:T(8,128)(2,1)}, bf16[2,256,256]{2,1,0:T(8,128)(2,1)}, u32[]{:S(2)}, u32[]{:S(2)}) collective-permute-start(bf16[2,256,256]{2,1,0:T(8,128)(2,1)} %get-tuple-element.36), channel_id=1, source_target_pairs={{0,448},{64,0},{128,64},{192,128},{256,192},{320,256},{384,320},{4... | collective-permute-start | bytes 786440 | tf_op jit(solution)/shard_map/ppermute | solution.py:338
  59.9 13.5 %collective-permute-start.2 = (bf16[2,256,256]{2,1,0:T(8,128)(2,1)}, bf16[2,256,256]{2,1,0:T(8,128)(2,1)S(1)}, u32[]{:S(2)}, u32[]{:S(2)}) collective-permute-start(bf16[2,256,256]{2,1,0:T(8,128)(2,1)} %get-tuple-element.35), channel_id=1, source_target_pairs={{0,64},{64,128},{128,192},{192,256},{256,320},{320,384},{384,448},... | collective-permute-start | bytes 786440 | tf_op jit(solution)/shard_map/ppermute | solution.py:337
  63.0 13.5 %collective-permute-start.3 = (bf16[2,256,256]{2,1,0:T(8,128)(2,1)}, bf16[2,256,256]{2,1,0:T(8,128)(2,1)S(1)}, u32[]{:S(2)}, u32[]{:S(2)}) collective-permute-start(bf16[2,256,256]{2,1,0:T(8,128)(2,1)} %get-tuple-element.34), channel_id=1, source_target_pairs={{0,448},{64,0},{128,64},{192,128},{256,192},{320,256},{384,320},{4... | collective-permute-start | bytes 786440 | tf_op jit(solution)/shard_map/ppermute | solution.py:338
  67.1 1.2 copy-start.1
  73.4 27.3 %copy-start.2 = (bf16[256,2048]{1,0:T(8,128)(2,1)S(1)}, bf16[256,2048]{1,0:T(8,128)(2,1)}, u32[]{:S(2)}) copy-start(bf16[256,2048]{1,0:T(8,128)(2,1)} %refs_0_.1) | copy-start | bytes 3145732
  73.4 10.3 %collective-permute-start.4 = (bf16[512,256]{1,0:T(8,128)(2,1)S(1)}, bf16[512,256]{1,0:T(8,128)(2,1)S(1)}, u32[]{:S(2)}, u32[]{:S(2)}) collective-permute-start(bf16[512,256]{1,0:T(8,128)(2,1)S(1)} %shard_map.88.k_ref), channel_id=1, source_target_pairs={{0,8},{8,16},{16,24},{24,32},{32,40},{40,48},{48,56},{56,64},{64,7... | collective-permute-start | bytes 786440 | tf_op jit(solution)/shard_map/ppermute | solution.py:362
  78.3 11.1 %collective-permute-start.5 = (bf16[512,256]{1,0:T(8,128)(2,1)S(1)}, bf16[512,256]{1,0:T(8,128)(2,1)S(1)}, u32[]{:S(2)}, u32[]{:S(2)}) collective-permute-start(bf16[512,256]{1,0:T(8,128)(2,1)S(1)} %shard_map.89.v_ref), channel_id=1, source_target_pairs={{0,8},{8,16},{16,24},{24,32},{32,40},{40,48},{48,56},{56,64},{64,7... | collective-permute-start | bytes 786440 | tf_op jit(solution)/shard_map/ppermute | solution.py:363
  83.7 11.4 %collective-permute-start.6 = (bf16[512,256]{1,0:T(8,128)(2,1)S(1)}, bf16[512,256]{1,0:T(8,128)(2,1)S(1)}, u32[]{:S(2)}, u32[]{:S(2)}) collective-permute-start(bf16[512,256]{1,0:T(8,128)(2,1)S(1)} %collective-permute-done.4.k_ref), channel_id=1, source_target_pairs={{0,8},{8,16},{16,24},{24,32},{32,40},{40,48},{48,56},{56,64},{64,7... | collective-permute-start | bytes 786440 | tf_op jit(solution)/shard_map/ppermute | solution.py:362
  89.4 17.6 %collective-permute-start.7 = (bf16[512,256]{1,0:T(8,128)(2,1)S(1)}, bf16[512,256]{1,0:T(8,128)(2,1)S(1)}, u32[]{:S(2)}, u32[]{:S(2)}) collective-permute-start(bf16[512,256]{1,0:T(8,128)(2,1)S(1)} %collective-permute-done.5.v_ref), channel_id=1, source_target_pairs={{0,8},{8,16},{16,24},{24,32},{32,40},{40,48},{48,56},{56,64},{64,7... | collective-permute-start | bytes 786440 | tf_op jit(solution)/shard_map/ppermute | solution.py:363
  95.1 14.3 %collective-permute-start.8 = (bf16[512,256]{1,0:T(8,128)(2,1)S(1)}, bf16[512,256]{1,0:T(8,128)(2,1)S(1)}, u32[]{:S(2)}, u32[]{:S(2)}) collective-permute-start(bf16[512,256]{1,0:T(8,128)(2,1)S(1)} %collective-permute-done.6.refs_0_), channel_id=1, source_target_pairs={{0,8},{8,16},{16,24},{24,32},{32,40},{40,48},{48,56},{56,64},{64,7... | collective-permute-start | bytes 786440 | tf_op jit(solution)/shard_map/ppermute | solution.py:362
  100.7 56.0 %collective-permute-start.15 = (bf16[256,2048]{1,0:T(8,128)(2,1)S(1)}, bf16[256,2048]{1,0:T(8,128)(2,1)S(1)}, u32[]{:S(2)}, u32[]{:S(2)}) collective-permute-start(bf16[256,2048]{1,0:T(8,128)(2,1)S(1)} %copy-done.2), channel_id=1, source_target_pairs={{0,1},{1,0},{2,3},{3,2},{4,5},{5,4},{6,7},{7,6},{8,9},{9,8},{10,11... | collective-permute-start | bytes 3145736 | tf_op jit(solution)/shard_map/ppermute | solution.py:345
  102.6 54.1 %collective-permute-start.16 = (bf16[256,2048]{1,0:T(8,128)(2,1)}, bf16[256,2048]{1,0:T(8,128)(2,1)S(1)}, u32[]{:S(2)}, u32[]{:S(2)}) collective-permute-start(bf16[256,2048]{1,0:T(8,128)(2,1)} %collective-permute-done.12.refs_1_), channel_id=1, source_target_pairs={{0,1},{1,0},{2,3},{3,2},{4,5},{5,4},{6,7},{7,6},{8,9},{9,8},{10,11... | collective-permute-start | bytes 3145736 | tf_op jit(solution)/shard_map/ppermute | solution.py:345
  105.1 51.7 %collective-permute-start.17 = (bf16[256,2048]{1,0:T(8,128)(2,1)}, bf16[256,2048]{1,0:T(8,128)(2,1)}, u32[]{:S(2)}, u32[]{:S(2)}) collective-permute-start(bf16[256,2048]{1,0:T(8,128)(2,1)} %collective-permute-done.13.refs_2_), channel_id=1, source_target_pairs={{0,1},{1,0},{2,3},{3,2},{4,5},{5,4},{6,7},{7,6},{8,9},{9,8},{10,11... | collective-permute-start | bytes 3145736 | tf_op jit(solution)/shard_map/ppermute | solution.py:345
  107.0 49.7 %collective-permute-start.18 = (bf16[256,2048]{1,0:T(8,128)(2,1)}, bf16[256,2048]{1,0:T(8,128)(2,1)}, u32[]{:S(2)}, u32[]{:S(2)}) collective-permute-start(bf16[256,2048]{1,0:T(8,128)(2,1)} %collective-permute-done.14.refs_3_), channel_id=1, source_target_pairs={{0,1},{1,0},{2,3},{3,2},{4,5},{5,4},{6,7},{7,6},{8,9},{9,8},{10,11... | collective-permute-start | bytes 3145736 | tf_op jit(solution)/shard_map/ppermute | solution.py:345
  109.4 10.1 %collective-permute-start.9 = (bf16[512,256]{1,0:T(8,128)(2,1)S(1)}, bf16[512,256]{1,0:T(8,128)(2,1)S(1)}, u32[]{:S(2)}, u32[]{:S(2)}) collective-permute-start(bf16[512,256]{1,0:T(8,128)(2,1)S(1)} %collective-permute-done.7.refs_1_), channel_id=1, source_target_pairs={{0,8},{8,16},{16,24},{24,32},{32,40},{40,48},{48,56},{56,64},{64,7... | collective-permute-start | bytes 786440 | tf_op jit(solution)/shard_map/ppermute | solution.py:363
  119.5 9.2 %collective-permute-start.10 = (bf16[512,256]{1,0:T(8,128)(2,1)S(1)}, bf16[512,256]{1,0:T(8,128)(2,1)S(1)}, u32[]{:S(2)}, u32[]{:S(2)}) collective-permute-start(bf16[512,256]{1,0:T(8,128)(2,1)S(1)} %collective-permute-done.8.refs_0_), channel_id=1, source_target_pairs={{0,8},{8,16},{16,24},{24,32},{32,40},{40,48},{48,56},{56,64},{64,7... | collective-permute-start | bytes 786440 | tf_op jit(solution)/shard_map/ppermute | solution.py:362
  128.8 16.9 %collective-permute-start.11 = (bf16[512,256]{1,0:T(8,128)(2,1)S(1)}, bf16[512,256]{1,0:T(8,128)(2,1)S(1)}, u32[]{:S(2)}, u32[]{:S(2)}) collective-permute-start(bf16[512,256]{1,0:T(8,128)(2,1)S(1)} %collective-permute-done.9.refs_1_), channel_id=1, source_target_pairs={{0,8},{8,16},{16,24},{24,32},{32,40},{40,48},{48,56},{56,64},{64,7... | collective-permute-start | bytes 786440 | tf_op jit(solution)/shard_map/ppermute | solution.py:363
  145.7 16.4 %copy-start.5 = (f32[2048]{0:T(1024)S(1)}, f32[2048]{0:T(1024)}, u32[]{:S(2)}) copy-start(f32[2048]{0:T(1024)} %param.13) | copy-start | bytes 24580
  148.8 0.7 copy-start.6
  149.5 0.7 copy-start.3
  150.2 11.9 %all-to-all-start.1 = ((bf16[8,64,256]{2,1,0:T(8,128)(2,1)}), bf16[8,64,256]{2,1,0:T(8,128)(2,1)S(1)}, u32[]{:S(2)}, u32[]{:S(2)}) async-start(bf16[8,64,256]{2,1,0:T(8,128)(2,1)} %bitcast.11), calls=%async_computation.1 | async-start | bytes 524288 | tf_op jit(solution)/shard_map/all_to_all | solution.py:407
  154.5 0.9 copy-start.7

commit v3 on v2

--- a/solution.py
+++ b/solution.py
@@ -230,26 +230,40 @@
     store_state(merged(q_ref[...], key, value, bias, count, max_ref, sum_ref, acc_ref, s_ref, p_ref), new_max, new_sum, new_acc)
 
 
-def far_kernel(backs, last, place_ref, q_ref, max_ref, sum_ref, acc_ref, *refs):
-    count = len(backs)
-    sources, outs = refs[: 2 * count], refs[2 * count :]
-    s_ref, p_ref = outs[-2:]
-    bias = jnp.concatenate([far_bias(place_ref[0], back) for back in backs], axis=1)
-    key = jnp.concatenate([ref[...] for ref in sources[0::2]], axis=0)
-    value = jnp.concatenate([ref[...] for ref in sources[1::2]], axis=0)
-    state = merged(q_ref[...], key, value, bias, None, max_ref, sum_ref, acc_ref, s_ref, p_ref)
-    if not last:
-        store_state(state, *outs[:3])
-        return
-    tops, sums, acc = state
-    cls = pl.program_id(0)
-    out_ref, log_ref, att_ref = outs[:3]
-    att_ref[pl.ds(pl.multiple_of(cls * 128, 128), 128), :] = (acc / tiles(sums)).astype(BF16)
+def far_kernel(back, place_ref, q_ref, max_ref, sum_ref, acc_ref, k_ref, v_ref, new_max, new_sum, new_acc, s_ref, p_ref):
+    bias = far_bias(place_ref[0], back)
+    state = merged(q_ref[...], k_ref[...], v_ref[...], bias, None, max_ref, sum_ref, acc_ref, s_ref, p_ref)
+    store_state(state, new_max, new_sum, new_acc)
+
+
+def score_kernel(back, place_ref, q_ref, max_ref, sum_ref, acc_ref, k_ref, p_ref, scaled_ref, total_ref, log_ref, s_ref):
+    bias = far_bias(place_ref[0], back)
+    s_ref[...] = lax.dot_general(stack_heads(q_ref[...]), k_ref[...], NT, preferred_element_type=F32)
     lane = lax.broadcasted_iota(jnp.int32, log_ref.shape, 1)
     logs = jnp.zeros(log_ref.shape, F32)
-    for h in range(len(tops)):
-        logs = jnp.where(lane == h, tops[h] + jnp.log(sums[h]), logs)
+    sums, scales = [], []
+    for h in range(q_ref.shape[1] // HEAD_DIM):
+        part = slice(h * 128, (h + 1) * 128)
+        s = s_ref[part, :] + bias
+        old = max_ref[part, :]
+        m = jnp.maximum(jnp.max(s, axis=1, keepdims=True), old)
+        p = jnp.exp(s - m)
+        p_ref[part, :] = p.astype(BF16)
+        scale = jnp.exp(old - m)
+        total = sum_ref[part, :] * scale + jnp.sum(p, axis=1, keepdims=True)
+        scales.append(scale)
+        sums.append(total)
+        logs = jnp.where(lane == h, m + jnp.log(total), logs)
+    scaled_ref[...] = acc_ref[...] * tiles(scales)
+    total_ref[...] = tiles(sums)
     log_ref[...] = logs
+
+
+def finish_kernel(p_ref, v_ref, scaled_ref, total_ref, out_ref, att_ref):
+    cls = pl.program_id(0)
+    pv = own_heads(jnp.dot(p_ref[...], v_ref[...], preferred_element_type=F32))
+    att = (scaled_ref[...] + pv) / total_ref[...]
+    att_ref[pl.ds(pl.multiple_of(cls * 128, 128), 128), :] = att.astype(BF16)
 
     @pl.when(cls == pl.num_programs(0) - 1)
     def _():
@@ -326,9 +340,9 @@
         (key_proj, value_proj),
         1000,
         56,
-        grid=(4,),
+        grid=(2,),
         in_specs=[shard_spec] * 2,
-        out_specs=(pl.BlockSpec((8, key_proj.shape[0], 2 * width), lambda n: (n, 0, 0)),),
+        out_specs=(pl.BlockSpec((16, key_proj.shape[0], 2 * width), lambda n: (n, 0, 0)),),
     )
     mine = lax.all_to_all(copies, ("zh", "y"), split_axis=0, concat_axis=0, tiled=True)
     mine = mine.reshape(4, 256, 2 * width)
@@ -389,20 +403,41 @@
         in_specs=[SMEM, part, stat, stat, part, whole, whole],
         out_specs=(stat, stat, part),
     )
-    for back in (2, 3, 4):
-        last = back == 4
+    scores = ((512, 128), F32)
+    for back in (2, 3):
         state = kernel_call(
-            functools.partial(far_kernel, (back,), last),
-            [(row, BF16), ((rows, 128), F32)] if last else outs,
+            functools.partial(far_kernel, back),
+            outs,
             (place, query, *state, keys[back], values[back]),
             4 * rows * 512 * width,
             16,
-            ([(row, BF16)] if last else []) + [((512, 128), t) for t in (F32, BF16)],
+            [scores, ((512, 128), BF16)],
             grid=(rows // 128,),
             in_specs=[SMEM, part, stat, stat, part, part, part],
-            out_specs=(whole, pl.BlockSpec((128, 128), lambda c: (c, 0))) if last else (stat, stat, part),
+            out_specs=(stat, stat, part),
         )
-    attended, logs = state
+    shares, scaled, total, logs = kernel_call(
+        functools.partial(score_kernel, 4),
+        [(stats, BF16), (row, F32), (row, F32), ((rows, 128), F32)],
+        (place, query, *state, keys[4]),
+        2 * rows * 512 * width,
+        16,
+        [scores],
+        grid=(rows // 128,),
+        in_specs=[SMEM, part, stat, stat, part, part],
+        out_specs=(stat, part, part, pl.BlockSpec((128, 128), lambda c: (c, 0))),
+    )
+    (attended,) = kernel_call(
+        finish_kernel,
+        [(row, BF16)],
+        (shares, values[4], scaled, total),
+        2 * rows * 512 * width,
+        16,
+        [(row, BF16)],
+        grid=(rows // 128,),
+        in_specs=[stat, part, part, part],
+        out_specs=(whole,),
+    )
 
     arrived = lax.all_to_all(attended.reshape(8, piece, width), TP, split_axis=0, concat_axis=0, tiled=True)
     (log_weight,) = kernel_call(log_kernel, [((heads, rows), F32)], (logs,), 6 * rows * rows * width, 8)

time: 168 us -> 167 us (level)
    unnamed x16 -> x14, local copies, waits for them, and re-layouts: 3.58 us -> 2.19 us
    pallas_call x11 -> x12, Pallas kernels: 30.6 us -> 31.2 us  [kernel_call(): pl.pallas_call(body, out_shape=tuple((jax.ShapeDtypeStruct(s, t) for s, t...]
  transfers between devices with their start and end apart: 21 -> 21, of which waited for: 9 -> 9; matrix products, arithmetic and copies ran while one was open for 1% -> 1% of each run, Pallas kernels for 14% -> 15%
where the time goes in v3:
time: 167 us; the launch traced here: 166 us
  starting transfers between devices  84.8 us (51%)
  waiting for transfers between devices  45.7 us (27%)
  Pallas kernels  31.2 us (19%)
  local copies, waits for them, and re-layouts  3.19 us (2%)
    pallas_call x12, Pallas kernels, kernel_call(): pl.pallas_call(body, out_shape=tuple((jax.ShapeDtypeStruct(s, t) for s, t...  31.2 us
    all_to_all x1, waiting for transfers between devices, layer(): lax.all_to_all(copies, ('zh', 'y'), split_axis=0, concat_axis=0, tiled=True)  19.3 us
    ppermute x4, starting transfers between devices, layer(): keys.append(lax.ppermute(keys[-1], SP, forward))  17 us
    all_to_all x1, starting transfers between devices, layer(): lax.all_to_all(copies, ('zh', 'y'), split_axis=0, concat_axis=0, tiled=True)  16.1 us
    ppermute x4, starting transfers between devices, layer(): values.append(lax.ppermute(values[-1], SP, forward))  14.1 us
    ppermute x3, starting transfers between devices, layer(): groups.append(lax.ppermute(out_proj, 'x', ring(4, steps)))  10.8 us
    ppermute x4, waiting for transfers between devices, layer(): keys.append(lax.ppermute(keys[-1], SP, forward))  9.63 us
    ppermute x4, waiting for transfers between devices, layer(): values.append(lax.ppermute(values[-1], SP, forward))  8.95 us
  transfers between devices with their start and end apart: 21, of which 9 were waited for; matrix products, arithmetic and copies ran while one was open for 1% of the time, Pallas kernels for 15%

profile of v3, /device:TPU:24, one launch (start us, length us, event | category | flops | bytes accessed | tf_op | source)
XLA Modules:
  0.0 166.4 jit_solution(7594243637090256219)
XLA Ops:
  0.6 1.8 %shard_map.87 = bf16[32,32,512]{2,1,0:T(8,128)(2,1)} custom-call(bf16[32,256]{1,0:T(8,128)(2,1)} %key_ref.1, bf16[32,256]{1,0:T(8,128)(2,1)} %value_ref.1), custom_call_target="tpu_custom_call" | custom-call | flops 1000 | bytes 32768 | tf_op jit(solution)/shard_map/pallas_call | solution.py:317
  2.4 16.1 %all-to-all-start = ((bf16[32,32,512]{2,1,0:T(8,128)(2,1)}), bf16[32,32,512]{2,1,0:T(8,128)(2,1)S(1)}, u32[]{:S(2)}, u32[]{:S(2)}) async-start(bf16[32,32,512]{2,1,0:T(8,128)(2,1)} %shard_map.87), calls=%async_computation | async-start | bytes 2097152 | tf_op jit(solution)/shard_map/all_to_all | solution.py:347
  18.5 3.4 %collective-permute-start.12 = (bf16[256,2048]{1,0:T(8,128)(2,1)}, bf16[256,2048]{1,0:T(8,128)(2,1)}, u32[]{:S(2)}, u32[]{:S(2)}) collective-permute-start(bf16[256,2048]{1,0:T(8,128)(2,1)} %refs_0_.1), channel_id=1, source_target_pairs={{0,2},{2,4},{4,6},{6,0},{1,3},{3,5},{5,7},{7,1},{8,10},{10,12},{12... | collective-permute-start | bytes 3145736 | tf_op jit(solution)/shard_map/ppermute | solution.py:357
  21.9 3.7 %collective-permute-start.13 = (bf16[256,2048]{1,0:T(8,128)(2,1)}, bf16[256,2048]{1,0:T(8,128)(2,1)}, u32[]{:S(2)}, u32[]{:S(2)}) collective-permute-start(bf16[256,2048]{1,0:T(8,128)(2,1)} %refs_0_.1), channel_id=1, source_target_pairs={{0,6},{2,0},{4,2},{6,4},{1,7},{3,1},{5,3},{7,5},{8,14},{10,8},{12,... | collective-permute-start | bytes 3145736 | tf_op jit(solution)/shard_map/ppermute | solution.py:357
  25.6 3.7 %collective-permute-start.14 = (bf16[256,2048]{1,0:T(8,128)(2,1)}, bf16[256,2048]{1,0:T(8,128)(2,1)}, u32[]{:S(2)}, u32[]{:S(2)}) collective-permute-start(bf16[256,2048]{1,0:T(8,128)(2,1)} %refs_0_.1), channel_id=1, source_target_pairs={{0,4},{2,6},{4,0},{6,2},{1,5},{3,7},{5,1},{7,3},{8,12},{10,14},{12... | collective-permute-start | bytes 3145736 | tf_op jit(solution)/shard_map/ppermute | solution.py:357
  29.3 19.3 %all-to-all-done = bf16[32,32,512]{2,1,0:T(8,128)(2,1)S(1)} async-done(((bf16[32,32,512]{2,1,0:T(8,128)(2,1)}), bf16[32,32,512]{2,1,0:T(8,128)(2,1)S(1)}, u32[]{:S(2)}, u32[]{:S(2)}) %all-to-all-start) | async-done | bytes 1048608 | tf_op jit(solution)/shard_map/all_to_all | solution.py:347
  48.7 1.0 fusion
  49.7 4.1 %collective-permute-start = (bf16[2,256,256]{2,1,0:T(8,128)(2,1)}, bf16[2,256,256]{2,1,0:T(8,128)(2,1)S(1)}, u32[]{:S(2)}, u32[]{:S(2)}) collective-permute-start(bf16[2,256,256]{2,1,0:T(8,128)(2,1)} %get-tuple-element.41), channel_id=1, source_target_pairs={{0,64},{64,128},{128,192},{192,256},{256,320},{320,384},{384,448},... | collective-permute-start | bytes 786440 | tf_op jit(solution)/shard_map/ppermute | solution.py:351
  53.8 3.0 %collective-permute-start.1 = (bf16[2,256,256]{2,1,0:T(8,128)(2,1)}, bf16[2,256,256]{2,1,0:T(8,128)(2,1)}, u32[]{:S(2)}, u32[]{:S(2)}) collective-permute-start(bf16[2,256,256]{2,1,0:T(8,128)(2,1)} %get-tuple-element.40), channel_id=1, source_target_pairs={{0,448},{64,0},{128,64},{192,128},{256,192},{320,256},{384,320},{4... | collective-permute-start | bytes 786440 | tf_op jit(solution)/shard_map/ppermute | solution.py:352
  56.8 0.3 multiply_cosine_fusion
  57.1 2.3 %collective-permute-done.below_ref = bf16[2,256,256]{2,1,0:T(8,128)(2,1)S(1)} collective-permute-done((bf16[2,256,256]{2,1,0:T(8,128)(2,1)}, bf16[2,256,256]{2,1,0:T(8,128)(2,1)S(1)}, u32[]{:S(2)}, u32[]{:S(2)}) %collective-permute-start) | collective-permute-done | bytes 262176 | tf_op jit(solution)/shard_map/ppermute | solution.py:351
  59.4 2.9 %collective-permute-start.2 = (bf16[2,256,256]{2,1,0:T(8,128)(2,1)}, bf16[2,256,256]{2,1,0:T(8,128)(2,1)S(1)}, u32[]{:S(2)}, u32[]{:S(2)}) collective-permute-start(bf16[2,256,256]{2,1,0:T(8,128)(2,1)} %get-tuple-element.39), channel_id=1, source_target_pairs={{0,64},{64,128},{128,192},{192,256},{256,320},{320,384},{384,448},... | collective-permute-start | bytes 786440 | tf_op jit(solution)/shard_map/ppermute | solution.py:351
  62.2 0.1 pad_add_fusion.place_ref
  62.3 0.2 collective-permute-done.1.above_ref
  62.5 4.0 %collective-permute-start.3 = (bf16[2,256,256]{2,1,0:T(8,128)(2,1)}, bf16[2,256,256]{2,1,0:T(8,128)(2,1)S(1)}, u32[]{:S(2)}, u32[]{:S(2)}) collective-permute-start(bf16[2,256,256]{2,1,0:T(8,128)(2,1)} %get-tuple-element.38), channel_id=1, source_target_pairs={{0,448},{64,0},{128,64},{192,128},{256,192},{320,256},{384,320},{4... | collective-permute-start | bytes 786440 | tf_op jit(solution)/shard_map/ppermute | solution.py:352
  66.5 0.0 copy-done
  66.6 0.0 copy-done.3
  66.6 0.0 copy-start.1
  66.6 1.2 copy-done.1
  67.8 2.7 %shard_map.86 = (bf16[512,2048]{1,0:T(8,128)(2,1)S(1)}, bf16[512,256]{1,0:T(8,128)(2,1)S(1)}) custom-call(bf16[512,2048]{1,0:T(8,128)(2,1)S(1)} %copy-done, f32[1,2048]{1,0:T(1,128)S(1)} %bitcast.11, bf16[2048,256]{1,0:T(8,128)(2,1)S(1)} %copy-done.1, f32[2,32,512]{2,1,0:T(8,128)S(1)} %pad_maximum_fusion.turn_ref), custom_call_target="tpu_custom_call" | custom-call | flops 536870912 | bytes 3284992 | tf_op jit(solution)/shard_map/pallas_call | solution.py:317
  70.5 2.4 %shard_map.88.k_ref = bf16[512,256]{1,0:T(8,128)(2,1)S(1)} custom-call(s32[4]{0:T(128)S(1)} %pad_add_fusion.place_ref, bf16[512,2048]{1,0:T(8,128)(2,1)S(1)} %get-tuple-element.21.normed_ref, bf16[4,256,512]{2,1,0:T(8,128)(2,1)S(1)} %bitcast.9, bf16[2,256,256]{2,1,0:T(8,128)(2,1)S(1)} %collective-permute-done.below_ref, ...), custom_call_target="tpu_custom_call" | custom-call | flops 536870912 | bytes 3801104 | tf_op jit(solution)/shard_map/pallas_call | solution.py:317
  72.9 0.0 copy-start.2
  72.9 0.0 collective-permute-done.2.below_ref
  72.9 3.1 %collective-permute-start.4 = (bf16[512,256]{1,0:T(8,128)(2,1)S(1)}, bf16[512,256]{1,0:T(8,128)(2,1)S(1)}, u32[]{:S(2)}, u32[]{:S(2)}) collective-permute-start(bf16[512,256]{1,0:T(8,128)(2,1)S(1)} %shard_map.88.k_ref), channel_id=1, source_target_pairs={{0,8},{8,16},{16,24},{24,32},{32,40},{40,48},{48,56},{56,64},{64,7... | collective-permute-start | bytes 786440 | tf_op jit(solution)/shard_map/ppermute | solution.py:376
  76.0 0.0 collective-permute-done.3.above_ref
  76.0 1.8 %shard_map.89.v_ref = bf16[512,256]{1,0:T(8,128)(2,1)S(1)} custom-call(s32[4]{0:T(128)S(1)} %pad_add_fusion.place_ref, bf16[512,2048]{1,0:T(8,128)(2,1)S(1)} %get-tuple-element.21.normed_ref, bf16[4,256,512]{2,1,0:T(8,128)(2,1)S(1)} %bitcast.10, bf16[2,256,256]{2,1,0:T(8,128)(2,1)S(1)} %collective-permute-done.2.below_ref, ...), custom_call_target="tpu_custom_call" | custom-call | flops 536870912 | bytes 3670032 | tf_op jit(solution)/shard_map/pallas_call | solution.py:317
  77.8 2.4 %collective-permute-start.5 = (bf16[512,256]{1,0:T(8,128)(2,1)S(1)}, bf16[512,256]{1,0:T(8,128)(2,1)S(1)}, u32[]{:S(2)}, u32[]{:S(2)}) collective-permute-start(bf16[512,256]{1,0:T(8,128)(2,1)S(1)} %shard_map.89.v_ref), channel_id=1, source_target_pairs={{0,8},{8,16},{16,24},{24,32},{32,40},{40,48},{48,56},{56,64},{64,7... | collective-permute-start | bytes 786440 | tf_op jit(solution)/shard_map/ppermute | solution.py:377
  80.2 2.9 %collective-permute-done.4.k_ref = bf16[512,256]{1,0:T(8,128)(2,1)S(1)} collective-permute-done((bf16[512,256]{1,0:T(8,128)(2,1)S(1)}, bf16[512,256]{1,0:T(8,128)(2,1)S(1)}, u32[]{:S(2)}, u32[]{:S(2)}) %collective-permute-start.4) | collective-permute-done | bytes 262176 | tf_op jit(solution)/shard_map/ppermute | solution.py:376
  83.2 4.9 %collective-permute-start.6 = (bf16[512,256]{1,0:T(8,128)(2,1)S(1)}, bf16[512,256]{1,0:T(8,128)(2,1)S(1)}, u32[]{:S(2)}, u32[]{:S(2)}) collective-permute-start(bf16[512,256]{1,0:T(8,128)(2,1)S(1)} %collective-permute-done.4.k_ref), channel_id=1, source_target_pairs={{0,8},{8,16},{16,24},{24,32},{32,40},{40,48},{48,56},{56,64},{64,7... | collective-permute-start | bytes 786440 | tf_op jit(solution)/shard_map/ppermute | solution.py:376
  88.1 0.8 collective-permute-done.5.v_ref
  88.9 4.9 %collective-permute-start.7 = (bf16[512,256]{1,0:T(8,128)(2,1)S(1)}, bf16[512,256]{1,0:T(8,128)(2,1)S(1)}, u32[]{:S(2)}, u32[]{:S(2)}) collective-permute-start(bf16[512,256]{1,0:T(8,128)(2,1)S(1)} %collective-permute-done.5.v_ref), channel_id=1, source_target_pairs={{0,8},{8,16},{16,24},{24,32},{32,40},{40,48},{48,56},{56,64},{64,7... | collective-permute-start | bytes 786440 | tf_op jit(solution)/shard_map/ppermute | solution.py:377
  93.7 0.8 collective-permute-done.6.k_ref
  94.6 5.6 %collective-permute-start.8 = (bf16[512,256]{1,0:T(8,128)(2,1)S(1)}, bf16[512,256]{1,0:T(8,128)(2,1)S(1)}, u32[]{:S(2)}, u32[]{:S(2)}) collective-permute-start(bf16[512,256]{1,0:T(8,128)(2,1)S(1)} %collective-permute-done.6.k_ref), channel_id=1, source_target_pairs={{0,8},{8,16},{16,24},{24,32},{32,40},{40,48},{48,56},{56,64},{64,7... | collective-permute-start | bytes 786440 | tf_op jit(solution)/shard_map/ppermute | solution.py:376
  100.2 0.0 collective-permute-done.12.refs_1_
  100.2 1.9 %collective-permute-start.15 = (bf16[256,2048]{1,0:T(8,128)(2,1)S(1)}, bf16[256,2048]{1,0:T(8,128)(2,1)S(1)}, u32[]{:S(2)}, u32[]{:S(2)}) collective-permute-start(bf16[256,2048]{1,0:T(8,128)(2,1)S(1)} %copy-done.2), channel_id=1, source_target_pairs={{0,1},{1,0},{2,3},{3,2},{4,5},{5,4},{6,7},{7,6},{8,9},{9,8},{10,11... | collective-permute-start | bytes 3145736 | tf_op jit(solution)/shard_map/ppermute | solution.py:359
  102.1 0.0 collective-permute-done.13.refs_2_
  102.1 2.4 %collective-permute-start.16 = (bf16[256,2048]{1,0:T(8,128)(2,1)}, bf16[256,2048]{1,0:T(8,128)(2,1)S(1)}, u32[]{:S(2)}, u32[]{:S(2)}) collective-permute-start(bf16[256,2048]{1,0:T(8,128)(2,1)} %collective-permute-done.12.refs_1_), channel_id=1, source_target_pairs={{0,1},{1,0},{2,3},{3,2},{4,5},{5,4},{6,7},{7,6},{8,9},{9,8},{10,11... | collective-permute-start | bytes 3145736 | tf_op jit(solution)/shard_map/ppermute | solution.py:359
  104.5 0.0 collective-permute-done.14.refs_3_
  104.6 1.9 %collective-permute-start.17 = (bf16[256,2048]{1,0:T(8,128)(2,1)}, bf16[256,2048]{1,0:T(8,128)(2,1)}, u32[]{:S(2)}, u32[]{:S(2)}) collective-permute-start(bf16[256,2048]{1,0:T(8,128)(2,1)} %collective-permute-done.13.refs_2_), channel_id=1, source_target_pairs={{0,1},{1,0},{2,3},{3,2},{4,5},{5,4},{6,7},{7,6},{8,9},{9,8},{10,11... | collective-permute-start | bytes 3145736 | tf_op jit(solution)/shard_map/ppermute | solution.py:359
  106.5 0.0 collective-permute-done.7.v_ref
  106.5 2.4 %collective-permute-start.18 = (bf16[256,2048]{1,0:T(8,128)(2,1)}, bf16[256,2048]{1,0:T(8,128)(2,1)}, u32[]{:S(2)}, u32[]{:S(2)}) collective-permute-start(bf16[256,2048]{1,0:T(8,128)(2,1)} %collective-permute-done.14.refs_3_), channel_id=1, source_target_pairs={{0,1},{1,0},{2,3},{3,2},{4,5},{5,4},{6,7},{7,6},{8,9},{9,8},{10,11... | collective-permute-start | bytes 3145736 | tf_op jit(solution)/shard_map/ppermute | solution.py:359
  108.9 0.0 collective-permute-done.8.k_ref
  108.9 1.9 %collective-permute-start.9 = (bf16[512,256]{1,0:T(8,128)(2,1)S(1)}, bf16[512,256]{1,0:T(8,128)(2,1)S(1)}, u32[]{:S(2)}, u32[]{:S(2)}) collective-permute-start(bf16[512,256]{1,0:T(8,128)(2,1)S(1)} %collective-permute-done.7.v_ref), channel_id=1, source_target_pairs={{0,8},{8,16},{16,24},{24,32},{32,40},{40,48},{48,56},{56,64},{64,7... | collective-permute-start | bytes 786440 | tf_op jit(solution)/shard_map/ppermute | solution.py:377
  110.9 8.2 %collective-permute-done.9.v_ref = bf16[512,256]{1,0:T(8,128)(2,1)S(1)} collective-permute-done((bf16[512,256]{1,0:T(8,128)(2,1)S(1)}, bf16[512,256]{1,0:T(8,128)(2,1)S(1)}, u32[]{:S(2)}, u32[]{:S(2)}) %collective-permute-start.9) | collective-permute-done | bytes 262176 | tf_op jit(solution)/shard_map/ppermute | solution.py:377
  119.0 3.4 %collective-permute-start.10 = (bf16[512,256]{1,0:T(8,128)(2,1)S(1)}, bf16[512,256]{1,0:T(8,128)(2,1)S(1)}, u32[]{:S(2)}, u32[]{:S(2)}) collective-permute-start(bf16[512,256]{1,0:T(8,128)(2,1)S(1)} %collective-permute-done.8.k_ref), channel_id=1, source_target_pairs={{0,8},{8,16},{16,24},{24,32},{32,40},{40,48},{48,56},{56,64},{64,7... | collective-permute-start | bytes 786440 | tf_op jit(solution)/shard_map/ppermute | solution.py:376
  122.4 5.8 %collective-permute-done.10.k_ref = bf16[512,256]{1,0:T(8,128)(2,1)S(1)} collective-permute-done((bf16[512,256]{1,0:T(8,128)(2,1)S(1)}, bf16[512,256]{1,0:T(8,128)(2,1)S(1)}, u32[]{:S(2)}, u32[]{:S(2)}) %collective-permute-start.10) | collective-permute-done | bytes 262176 | tf_op jit(solution)/shard_map/ppermute | solution.py:376
  128.3 4.9 %collective-permute-start.11 = (bf16[512,256]{1,0:T(8,128)(2,1)S(1)}, bf16[512,256]{1,0:T(8,128)(2,1)S(1)}, u32[]{:S(2)}, u32[]{:S(2)}) collective-permute-start(bf16[512,256]{1,0:T(8,128)(2,1)S(1)} %collective-permute-done.9.v_ref), channel_id=1, source_target_pairs={{0,8},{8,16},{16,24},{24,32},{32,40},{40,48},{48,56},{56,64},{64,7... | collective-permute-start | bytes 786440 | tf_op jit(solution)/shard_map/ppermute | solution.py:377
  133.2 3.5 %shard_map.90 = (f32[2048,128]{1,0:T(8,128)S(1)}, f32[2048,128]{1,0:T(8,128)S(1)}, f32[512,256]{1,0:T(8,128)S(1)}) custom-call(bf16[512,256]{1,0:T(8,128)(2,1)S(1)} %get-tuple-element.20.q_ref, bf16[512,256]{1,0:T(8,128)(2,1)S(1)} %shard_map.88.k_ref, bf16[512,256]{1,0:T(8,128)(2,1)S(1)} %shard_map.89.v_ref), custom_call_target="tpu_custom_call" | custom-call | flops 536870912 | bytes 786432 | tf_op jit(solution)/shard_map/pallas_call | solution.py:317
  136.7 3.0 %shard_map.91 = (f32[2048,128]{1,0:T(8,128)S(1)}, f32[2048,128]{1,0:T(8,128)S(1)}, f32[512,256]{1,0:T(8,128)S(1)}) custom-call(s32[4]{0:T(128)S(1)} %pad_add_fusion.place_ref, bf16[512,256]{1,0:T(8,128)(2,1)S(1)} %get-tuple-element.20.q_ref, f32[2048,128]{1,0:T(8,128)S(1)} %get-tuple-element.22.max_ref, f32[2048,128]{1,0:T(8,128)S(1)} %get-tuple-element.23.sum_ref, ...), custom_call_target="tpu_custom_call" | custom-call | flops 268435456 | bytes 3407888 | tf_op jit(solution)/shard_map/pallas_call | solution.py:317
  139.7 2.8 %shard_map.92 = (f32[2048,128]{1,0:T(8,128)S(1)}, f32[2048,128]{1,0:T(8,128)S(1)}, f32[512,256]{1,0:T(8,128)S(1)}) custom-call(s32[4]{0:T(128)S(1)} %pad_add_fusion.place_ref, bf16[512,256]{1,0:T(8,128)(2,1)S(1)} %get-tuple-element.20.q_ref, f32[2048,128]{1,0:T(8,128)S(1)} %get-tuple-element.25.max_ref, f32[2048,128]{1,0:T(8,128)S(1)} %get-tuple-element.26.sum_ref, ...), custom_call_target="tpu_custom_call" | custom-call | flops 268435456 | bytes 3407888 | tf_op jit(solution)/shard_map/pallas_call | solution.py:317
  142.4 2.8 %shard_map.93 = (f32[2048,128]{1,0:T(8,128)S(1)}, f32[2048,128]{1,0:T(8,128)S(1)}, f32[512,256]{1,0:T(8,128)S(1)}) custom-call(s32[4]{0:T(128)S(1)} %pad_add_fusion.place_ref, bf16[512,256]{1,0:T(8,128)(2,1)S(1)} %get-tuple-element.20.q_ref, f32[2048,128]{1,0:T(8,128)S(1)} %get-tuple-element.28.max_ref, f32[2048,128]{1,0:T(8,128)S(1)} %get-tuple-element.29.sum_ref, ...), custom_call_target="tpu_custom_call" | custom-call | flops 268435456 | bytes 3407888 | tf_op jit(solution)/shard_map/pallas_call | solution.py:317
  145.2 2.3 %shard_map.94 = (bf16[2048,128]{1,0:T(8,128)(2,1)S(1)}, f32[512,256]{1,0:T(8,128)S(1)}, f32[512,256]{1,0:T(8,128)S(1)}, f32[512,128]{1,0:T(8,128)S(1)}) custom-call(s32[4]{0:T(128)S(1)} %pad_add_fusion.place_ref, bf16[512,256]{1,0:T(8,128)(2,1)S(1)} %get-tuple-element.20.q_ref, f32[2048,128]{1,0:T(8,128)S(1)} %get-tuple-element.31.max_ref, ...), custom_call_target="tpu_custom_call" | custom-call | flops 134217728 | bytes 3145744 | tf_op jit(solution)/shard_map/pallas_call | solution.py:317
  147.5 0.0 copy-start.4
  147.5 0.0 collective-permute-done.11.v_ref
  147.5 1.9 %shard_map.95 = bf16[512,256]{1,0:T(8,128)(2,1)} custom-call(bf16[2048,128]{1,0:T(8,128)(2,1)S(1)} %get-tuple-element.34.p_ref, bf16[512,256]{1,0:T(8,128)(2,1)S(1)} %collective-permute-done.11.v_ref, f32[512,256]{1,0:T(8,128)S(1)} %get-tuple-element.35.scaled_ref, f32[512,256]{1,0:T(8,128)S(1)} %get-tuple-element.36.total_ref), custom_call_target="tpu_custom_call" | custom-call | flops 134217728 | bytes 1835008 | tf_op jit(solution)/shard_map/pallas_call | solution.py:317
  149.4 4.3 %all-to-all-start.1 = ((bf16[8,64,256]{2,1,0:T(8,128)(2,1)}), bf16[8,64,256]{2,1,0:T(8,128)(2,1)S(1)}, u32[]{:S(2)}, u32[]{:S(2)}) async-start(bf16[8,64,256]{2,1,0:T(8,128)(2,1)} %bitcast.6), calls=%async_computation.1 | async-start | bytes 524288 | tf_op jit(solution)/shard_map/all_to_all | solution.py:442
  153.7 0.9 copy-done.6
  154.7 1.2 shard_map.97
  155.9 0.0 collective-permute-done.15.refs_4_
  155.9 0.0 collective-permute-done.16.refs_5_
  155.9 0.0 collective-permute-done.17.refs_6_
  155.9 0.0 collective-permute-done.18.refs_7_
  155.9 5.3 %all-to-all-done.1.att_ref = bf16[8,64,256]{2,1,0:T(8,128)(2,1)S(1)} async-done(((bf16[8,64,256]{2,1,0:T(8,128)(2,1)}), bf16[8,64,256]{2,1,0:T(8,128)(2,1)S(1)}, u32[]{:S(2)}, u32[]{:S(2)}) %all-to-all-start.1) | async-done | bytes 262176 | tf_op jit(solution)/shard_map/all_to_all | solution.py:442
  161.2 5.1 %shard_map.96 = bf16[64,2048]{1,0:T(8,128)(2,1)} custom-call(s32[4]{0:T(128)S(1)} %pad_add_fusion.place_ref, bf16[8,64,256]{2,1,0:T(8,128)(2,1)S(1)} %all-to-all-done.1.att_ref, bf16[256,2048]{1,0:T(8,128)(2,1)S(1)} %copy-done.2, bf16[256,2048]{1,0:T(8,128)(2,1)} %collective-permute-done.12.refs_1_, bf16[256,2048]{1,0:T(8,128)(2,1)} %collective-permute-done.13.refs_2_, ...), custom_call_target="tpu_custom_call" | custom-call | flops 536870912 | bytes 8658960 | tf_op jit(solution)/shard_map/pallas_call | solution.py:317
  (10 shorter events, 0.0 us)
Async XLA Ops:
  2.4 64.1 %copy-start = (bf16[512,2048]{1,0:T(8,128)(2,1)S(1)}, bf16[512,2048]{1,0:T(8,128)(2,1)}, u32[]{:S(2)}) copy-start(bf16[512,2048]{1,0:T(8,128)(2,1)} %hidden_ref.1) | copy-start | bytes 6291460
  2.4 64.1 %copy-start.3 = (f32[2048]{0:T(1024)S(1)}, f32[2048]{0:T(1024)}, u32[]{:S(2)}) copy-start(f32[2048]{0:T(1024)} %param.8) | copy-start | bytes 24580
  2.4 46.3 %all-to-all-start = ((bf16[32,32,512]{2,1,0:T(8,128)(2,1)}), bf16[32,32,512]{2,1,0:T(8,128)(2,1)S(1)}, u32[]{:S(2)}, u32[]{:S(2)}) async-start(bf16[32,32,512]{2,1,0:T(8,128)(2,1)} %shard_map.87), calls=%async_computation | async-start | bytes 2097152 | tf_op jit(solution)/shard_map/all_to_all | solution.py:347
  18.5 81.7 %collective-permute-start.12 = (bf16[256,2048]{1,0:T(8,128)(2,1)}, bf16[256,2048]{1,0:T(8,128)(2,1)}, u32[]{:S(2)}, u32[]{:S(2)}) collective-permute-start(bf16[256,2048]{1,0:T(8,128)(2,1)} %refs_0_.1), channel_id=1, source_target_pairs={{0,2},{2,4},{4,6},{6,0},{1,3},{3,5},{5,7},{7,1},{8,10},{10,12},{12... | collective-permute-start | bytes 3145736 | tf_op jit(solution)/shard_map/ppermute | solution.py:357
  21.9 80.2 %collective-permute-start.13 = (bf16[256,2048]{1,0:T(8,128)(2,1)}, bf16[256,2048]{1,0:T(8,128)(2,1)}, u32[]{:S(2)}, u32[]{:S(2)}) collective-permute-start(bf16[256,2048]{1,0:T(8,128)(2,1)} %refs_0_.1), channel_id=1, source_target_pairs={{0,6},{2,0},{4,2},{6,4},{1,7},{3,1},{5,3},{7,5},{8,14},{10,8},{12,... | collective-permute-start | bytes 3145736 | tf_op jit(solution)/shard_map/ppermute | solution.py:357
  25.6 79.0 %collective-permute-start.14 = (bf16[256,2048]{1,0:T(8,128)(2,1)}, bf16[256,2048]{1,0:T(8,128)(2,1)}, u32[]{:S(2)}, u32[]{:S(2)}) collective-permute-start(bf16[256,2048]{1,0:T(8,128)(2,1)} %refs_0_.1), channel_id=1, source_target_pairs={{0,4},{2,6},{4,0},{6,2},{1,5},{3,7},{5,1},{7,3},{8,12},{10,14},{12... | collective-permute-start | bytes 3145736 | tf_op jit(solution)/shard_map/ppermute | solution.py:357
  49.7 9.7 %collective-permute-start = (bf16[2,256,256]{2,1,0:T(8,128)(2,1)}, bf16[2,256,256]{2,1,0:T(8,128)(2,1)S(1)}, u32[]{:S(2)}, u32[]{:S(2)}) collective-permute-start(bf16[2,256,256]{2,1,0:T(8,128)(2,1)} %get-tuple-element.41), channel_id=1, source_target_pairs={{0,64},{64,128},{128,192},{192,256},{256,320},{320,384},{384,448},... | collective-permute-start | bytes 786440 | tf_op jit(solution)/shard_map/ppermute | solution.py:351
  53.8 8.8 %collective-permute-start.1 = (bf16[2,256,256]{2,1,0:T(8,128)(2,1)}, bf16[2,256,256]{2,1,0:T(8,128)(2,1)}, u32[]{:S(2)}, u32[]{:S(2)}) collective-permute-start(bf16[2,256,256]{2,1,0:T(8,128)(2,1)} %get-tuple-element.40), channel_id=1, source_target_pairs={{0,448},{64,0},{128,64},{192,128},{256,192},{320,256},{384,320},{4... | collective-permute-start | bytes 786440 | tf_op jit(solution)/shard_map/ppermute | solution.py:352
  59.4 13.5 %collective-permute-start.2 = (bf16[2,256,256]{2,1,0:T(8,128)(2,1)}, bf16[2,256,256]{2,1,0:T(8,128)(2,1)S(1)}, u32[]{:S(2)}, u32[]{:S(2)}) collective-permute-start(bf16[2,256,256]{2,1,0:T(8,128)(2,1)} %get-tuple-element.39), channel_id=1, source_target_pairs={{0,64},{64,128},{128,192},{192,256},{256,320},{320,384},{384,448},... | collective-permute-start | bytes 786440 | tf_op jit(solution)/shard_map/ppermute | solution.py:351
  62.5 13.5 %collective-permute-start.3 = (bf16[2,256,256]{2,1,0:T(8,128)(2,1)}, bf16[2,256,256]{2,1,0:T(8,128)(2,1)S(1)}, u32[]{:S(2)}, u32[]{:S(2)}) collective-permute-start(bf16[2,256,256]{2,1,0:T(8,128)(2,1)} %get-tuple-element.38), channel_id=1, source_target_pairs={{0,448},{64,0},{128,64},{192,128},{256,192},{320,256},{384,320},{4... | collective-permute-start | bytes 786440 | tf_op jit(solution)/shard_map/ppermute | solution.py:352
  66.6 1.2 copy-start.1
  72.9 27.3 %copy-start.2 = (bf16[256,2048]{1,0:T(8,128)(2,1)S(1)}, bf16[256,2048]{1,0:T(8,128)(2,1)}, u32[]{:S(2)}) copy-start(bf16[256,2048]{1,0:T(8,128)(2,1)} %refs_0_.1) | copy-start | bytes 3145732
  72.9 10.3 %collective-permute-start.4 = (bf16[512,256]{1,0:T(8,128)(2,1)S(1)}, bf16[512,256]{1,0:T(8,128)(2,1)S(1)}, u32[]{:S(2)}, u32[]{:S(2)}) collective-permute-start(bf16[512,256]{1,0:T(8,128)(2,1)S(1)} %shard_map.88.k_ref), channel_id=1, source_target_pairs={{0,8},{8,16},{16,24},{24,32},{32,40},{40,48},{48,56},{56,64},{64,7... | collective-permute-start | bytes 786440 | tf_op jit(solution)/shard_map/ppermute | solution.py:376
  77.8 11.1 %collective-permute-start.5 = (bf16[512,256]{1,0:T(8,128)(2,1)S(1)}, bf16[512,256]{1,0:T(8,128)(2,1)S(1)}, u32[]{:S(2)}, u32[]{:S(2)}) collective-permute-start(bf16[512,256]{1,0:T(8,128)(2,1)S(1)} %shard_map.89.v_ref), channel_id=1, source_target_pairs={{0,8},{8,16},{16,24},{24,32},{32,40},{40,48},{48,56},{56,64},{64,7... | collective-permute-start | bytes 786440 | tf_op jit(solution)/shard_map/ppermute | solution.py:377
  83.2 11.4 %collective-permute-start.6 = (bf16[512,256]{1,0:T(8,128)(2,1)S(1)}, bf16[512,256]{1,0:T(8,128)(2,1)S(1)}, u32[]{:S(2)}, u32[]{:S(2)}) collective-permute-start(bf16[512,256]{1,0:T(8,128)(2,1)S(1)} %collective-permute-done.4.k_ref), channel_id=1, source_target_pairs={{0,8},{8,16},{16,24},{24,32},{32,40},{40,48},{48,56},{56,64},{64,7... | collective-permute-start | bytes 786440 | tf_op jit(solution)/shard_map/ppermute | solution.py:376
  88.9 17.6 %collective-permute-start.7 = (bf16[512,256]{1,0:T(8,128)(2,1)S(1)}, bf16[512,256]{1,0:T(8,128)(2,1)S(1)}, u32[]{:S(2)}, u32[]{:S(2)}) collective-permute-start(bf16[512,256]{1,0:T(8,128)(2,1)S(1)} %collective-permute-done.5.v_ref), channel_id=1, source_target_pairs={{0,8},{8,16},{16,24},{24,32},{32,40},{40,48},{48,56},{56,64},{64,7... | collective-permute-start | bytes 786440 | tf_op jit(solution)/shard_map/ppermute | solution.py:377
  94.6 14.3 %collective-permute-start.8 = (bf16[512,256]{1,0:T(8,128)(2,1)S(1)}, bf16[512,256]{1,0:T(8,128)(2,1)S(1)}, u32[]{:S(2)}, u32[]{:S(2)}) collective-permute-start(bf16[512,256]{1,0:T(8,128)(2,1)S(1)} %collective-permute-done.6.k_ref), channel_id=1, source_target_pairs={{0,8},{8,16},{16,24},{24,32},{32,40},{40,48},{48,56},{56,64},{64,7... | collective-permute-start | bytes 786440 | tf_op jit(solution)/shard_map/ppermute | solution.py:376
  100.2 55.7 %collective-permute-start.15 = (bf16[256,2048]{1,0:T(8,128)(2,1)S(1)}, bf16[256,2048]{1,0:T(8,128)(2,1)S(1)}, u32[]{:S(2)}, u32[]{:S(2)}) collective-permute-start(bf16[256,2048]{1,0:T(8,128)(2,1)S(1)} %copy-done.2), channel_id=1, source_target_pairs={{0,1},{1,0},{2,3},{3,2},{4,5},{5,4},{6,7},{7,6},{8,9},{9,8},{10,11... | collective-permute-start | bytes 3145736 | tf_op jit(solution)/shard_map/ppermute | solution.py:359
  102.1 53.8 %collective-permute-start.16 = (bf16[256,2048]{1,0:T(8,128)(2,1)}, bf16[256,2048]{1,0:T(8,128)(2,1)S(1)}, u32[]{:S(2)}, u32[]{:S(2)}) collective-permute-start(bf16[256,2048]{1,0:T(8,128)(2,1)} %collective-permute-done.12.refs_1_), channel_id=1, source_target_pairs={{0,1},{1,0},{2,3},{3,2},{4,5},{5,4},{6,7},{7,6},{8,9},{9,8},{10,11... | collective-permute-start | bytes 3145736 | tf_op jit(solution)/shard_map/ppermute | solution.py:359
  104.6 51.4 %collective-permute-start.17 = (bf16[256,2048]{1,0:T(8,128)(2,1)}, bf16[256,2048]{1,0:T(8,128)(2,1)}, u32[]{:S(2)}, u32[]{:S(2)}) collective-permute-start(bf16[256,2048]{1,0:T(8,128)(2,1)} %collective-permute-done.13.refs_2_), channel_id=1, source_target_pairs={{0,1},{1,0},{2,3},{3,2},{4,5},{5,4},{6,7},{7,6},{8,9},{9,8},{10,11... | collective-permute-start | bytes 3145736 | tf_op jit(solution)/shard_map/ppermute | solution.py:359
  106.5 49.4 %collective-permute-start.18 = (bf16[256,2048]{1,0:T(8,128)(2,1)}, bf16[256,2048]{1,0:T(8,128)(2,1)}, u32[]{:S(2)}, u32[]{:S(2)}) collective-permute-start(bf16[256,2048]{1,0:T(8,128)(2,1)} %collective-permute-done.14.refs_3_), channel_id=1, source_target_pairs={{0,1},{1,0},{2,3},{3,2},{4,5},{5,4},{6,7},{7,6},{8,9},{9,8},{10,11... | collective-permute-start | bytes 3145736 | tf_op jit(solution)/shard_map/ppermute | solution.py:359
  108.9 10.1 %collective-permute-start.9 = (bf16[512,256]{1,0:T(8,128)(2,1)S(1)}, bf16[512,256]{1,0:T(8,128)(2,1)S(1)}, u32[]{:S(2)}, u32[]{:S(2)}) collective-permute-start(bf16[512,256]{1,0:T(8,128)(2,1)S(1)} %collective-permute-done.7.v_ref), channel_id=1, source_target_pairs={{0,8},{8,16},{16,24},{24,32},{32,40},{40,48},{48,56},{56,64},{64,7... | collective-permute-start | bytes 786440 | tf_op jit(solution)/shard_map/ppermute | solution.py:377
  119.0 9.2 %collective-permute-start.10 = (bf16[512,256]{1,0:T(8,128)(2,1)S(1)}, bf16[512,256]{1,0:T(8,128)(2,1)S(1)}, u32[]{:S(2)}, u32[]{:S(2)}) collective-permute-start(bf16[512,256]{1,0:T(8,128)(2,1)S(1)} %collective-permute-done.8.k_ref), channel_id=1, source_target_pairs={{0,8},{8,16},{16,24},{24,32},{32,40},{40,48},{48,56},{56,64},{64,7... | collective-permute-start | bytes 786440 | tf_op jit(solution)/shard_map/ppermute | solution.py:376
  128.3 19.2 %collective-permute-start.11 = (bf16[512,256]{1,0:T(8,128)(2,1)S(1)}, bf16[512,256]{1,0:T(8,128)(2,1)S(1)}, u32[]{:S(2)}, u32[]{:S(2)}) collective-permute-start(bf16[512,256]{1,0:T(8,128)(2,1)S(1)} %collective-permute-done.9.v_ref), channel_id=1, source_target_pairs={{0,8},{8,16},{16,24},{24,32},{32,40},{40,48},{48,56},{56,64},{64,7... | collective-permute-start | bytes 786440 | tf_op jit(solution)/shard_map/ppermute | solution.py:377
  147.5 1.9 %copy-start.5 = (f32[512,128]{1,0:T(8,128)}, f32[512,128]{1,0:T(8,128)S(1)}, u32[]{:S(2)}) copy-start(f32[512,128]{1,0:T(8,128)S(1)} %get-tuple-element.37.lw_ref) | copy-start | bytes 786436
  147.5 13.7 %copy-start.4 = (f32[2048]{0:T(1024)S(1)}, f32[2048]{0:T(1024)}, u32[]{:S(2)}) copy-start(f32[2048]{0:T(1024)} %param.13) | copy-start | bytes 24580
  149.4 11.8 %all-to-all-start.1 = ((bf16[8,64,256]{2,1,0:T(8,128)(2,1)}), bf16[8,64,256]{2,1,0:T(8,128)(2,1)S(1)}, u32[]{:S(2)}, u32[]{:S(2)}) async-start(bf16[8,64,256]{2,1,0:T(8,128)(2,1)} %bitcast.6), calls=%async_computation.1 | async-start | bytes 524288 | tf_op jit(solution)/shard_map/all_to_all | solution.py:442
  153.7 0.9 copy-start.6

commit v4 on v3

--- a/solution.py
+++ b/solution.py
@@ -254,15 +254,16 @@
         scales.append(scale)
         sums.append(total)
         logs = jnp.where(lane == h, m + jnp.log(total), logs)
-    scaled_ref[...] = acc_ref[...] * tiles(scales)
-    total_ref[...] = tiles(sums)
+    inverse = 1.0 / tiles(sums)
+    scaled_ref[...] = acc_ref[...] * tiles(scales) * inverse
+    total_ref[...] = inverse
     log_ref[...] = logs
 
 
 def finish_kernel(p_ref, v_ref, scaled_ref, total_ref, out_ref, att_ref):
     cls = pl.program_id(0)
     pv = own_heads(jnp.dot(p_ref[...], v_ref[...], preferred_element_type=F32))
-    att = (scaled_ref[...] + pv) / total_ref[...]
+    att = scaled_ref[...] + pv * total_ref[...]
     att_ref[pl.ds(pl.multiple_of(cls * 128, 128), 128), :] = att.astype(BF16)
 
     @pl.when(cls == pl.num_programs(0) - 1)
@@ -340,9 +341,9 @@
         (key_proj, value_proj),
         1000,
         56,
-        grid=(2,),
+        grid=(1,),
         in_specs=[shard_spec] * 2,
-        out_specs=(pl.BlockSpec((16, key_proj.shape[0], 2 * width), lambda n: (n, 0, 0)),),
+        out_specs=(pl.BlockSpec((32, key_proj.shape[0], 2 * width), lambda n: (n, 0, 0)),),
     )
     mine = lax.all_to_all(copies, ("zh", "y"), split_axis=0, concat_axis=0, tiled=True)
     mine = mine.reshape(4, 256, 2 * width)

time: 167 us -> 167 us (level)
  no operation moved by 1% of the time
where the time goes in v4:
time: 167 us; the launch traced here: 166 us
  starting transfers between devices  84.9 us (51%)
  waiting for transfers between devices  45.7 us (27%)
  Pallas kernels  31.2 us (19%)
  local copies, waits for them, and re-layouts  3.19 us (2%)
    pallas_call x12, Pallas kernels, kernel_call(): pl.pallas_call(body, out_shape=tuple((jax.ShapeDtypeStruct(s, t) for s, t...  31.2 us
    all_to_all x1, waiting for transfers between devices, layer(): lax.all_to_all(copies, ('zh', 'y'), split_axis=0, concat_axis=0, tiled=True)  19.3 us
    ppermute x4, starting transfers between devices, layer(): keys.append(lax.ppermute(keys[-1], SP, forward))  17.1 us
    all_to_all x1, starting transfers between devices, layer(): lax.all_to_all(copies, ('zh', 'y'), split_axis=0, concat_axis=0, tiled=True)  16.1 us
    ppermute x4, starting transfers between devices, layer(): values.append(lax.ppermute(values[-1], SP, forward))  14.1 us
    ppermute x3, starting transfers between devices, layer(): groups.append(lax.ppermute(out_proj, 'x', ring(4, steps)))  10.8 us
    ppermute x4, waiting for transfers between devices, layer(): keys.append(lax.ppermute(keys[-1], SP, forward))  9.6 us
    ppermute x4, waiting for transfers between devices, layer(): values.append(lax.ppermute(values[-1], SP, forward))  8.94 us
  transfers between devices with their start and end apart: 21, of which 9 were waited for; matrix products, arithmetic and copies ran while one was open for 1% of the time, Pallas kernels for 15%

profile of v4, /device:TPU:24, one launch (start us, length us, event | category | flops | bytes accessed | tf_op | source)
XLA Modules:
  0.0 166.4 jit_solution(15158769617502449158)
XLA Ops:
  0.6 1.8 %shard_map.87 = bf16[32,32,512]{2,1,0:T(8,128)(2,1)} custom-call(bf16[32,256]{1,0:T(8,128)(2,1)} %key_ref.1, bf16[32,256]{1,0:T(8,128)(2,1)} %value_ref.1), custom_call_target="tpu_custom_call" | custom-call | flops 1000 | bytes 32768 | tf_op jit(solution)/shard_map/pallas_call | solution.py:318
  2.5 16.1 %all-to-all-start = ((bf16[32,32,512]{2,1,0:T(8,128)(2,1)}), bf16[32,32,512]{2,1,0:T(8,128)(2,1)S(1)}, u32[]{:S(2)}, u32[]{:S(2)}) async-start(bf16[32,32,512]{2,1,0:T(8,128)(2,1)} %shard_map.87), calls=%async_computation | async-start | bytes 2097152 | tf_op jit(solution)/shard_map/all_to_all | solution.py:348
  18.6 3.4 %collective-permute-start.12 = (bf16[256,2048]{1,0:T(8,128)(2,1)}, bf16[256,2048]{1,0:T(8,128)(2,1)}, u32[]{:S(2)}, u32[]{:S(2)}) collective-permute-start(bf16[256,2048]{1,0:T(8,128)(2,1)} %refs_0_.1), channel_id=1, source_target_pairs={{0,2},{2,4},{4,6},{6,0},{1,3},{3,5},{5,7},{7,1},{8,10},{10,12},{12... | collective-permute-start | bytes 3145736 | tf_op jit(solution)/shard_map/ppermute | solution.py:358
  22.0 3.7 %collective-permute-start.13 = (bf16[256,2048]{1,0:T(8,128)(2,1)}, bf16[256,2048]{1,0:T(8,128)(2,1)}, u32[]{:S(2)}, u32[]{:S(2)}) collective-permute-start(bf16[256,2048]{1,0:T(8,128)(2,1)} %refs_0_.1), channel_id=1, source_target_pairs={{0,6},{2,0},{4,2},{6,4},{1,7},{3,1},{5,3},{7,5},{8,14},{10,8},{12,... | collective-permute-start | bytes 3145736 | tf_op jit(solution)/shard_map/ppermute | solution.py:358
  25.6 3.7 %collective-permute-start.14 = (bf16[256,2048]{1,0:T(8,128)(2,1)}, bf16[256,2048]{1,0:T(8,128)(2,1)}, u32[]{:S(2)}, u32[]{:S(2)}) collective-permute-start(bf16[256,2048]{1,0:T(8,128)(2,1)} %refs_0_.1), channel_id=1, source_target_pairs={{0,4},{2,6},{4,0},{6,2},{1,5},{3,7},{5,1},{7,3},{8,12},{10,14},{12... | collective-permute-start | bytes 3145736 | tf_op jit(solution)/shard_map/ppermute | solution.py:358
  29.4 19.3 %all-to-all-done = bf16[32,32,512]{2,1,0:T(8,128)(2,1)S(1)} async-done(((bf16[32,32,512]{2,1,0:T(8,128)(2,1)}), bf16[32,32,512]{2,1,0:T(8,128)(2,1)S(1)}, u32[]{:S(2)}, u32[]{:S(2)}) %all-to-all-start) | async-done | bytes 1048608 | tf_op jit(solution)/shard_map/all_to_all | solution.py:348
  48.7 1.0 fusion
  49.7 4.1 %collective-permute-start = (bf16[2,256,256]{2,1,0:T(8,128)(2,1)}, bf16[2,256,256]{2,1,0:T(8,128)(2,1)S(1)}, u32[]{:S(2)}, u32[]{:S(2)}) collective-permute-start(bf16[2,256,256]{2,1,0:T(8,128)(2,1)} %get-tuple-element.41), channel_id=1, source_target_pairs={{0,64},{64,128},{128,192},{192,256},{256,320},{320,384},{384,448},... | collective-permute-start | bytes 786440 | tf_op jit(solution)/shard_map/ppermute | solution.py:352
  53.8 3.0 %collective-permute-start.1 = (bf16[2,256,256]{2,1,0:T(8,128)(2,1)}, bf16[2,256,256]{2,1,0:T(8,128)(2,1)}, u32[]{:S(2)}, u32[]{:S(2)}) collective-permute-start(bf16[2,256,256]{2,1,0:T(8,128)(2,1)} %get-tuple-element.40), channel_id=1, source_target_pairs={{0,448},{64,0},{128,64},{192,128},{256,192},{320,256},{384,320},{4... | collective-permute-start | bytes 786440 | tf_op jit(solution)/shard_map/ppermute | solution.py:353
  56.8 0.3 multiply_cosine_fusion
  57.1 2.3 %collective-permute-done.below_ref = bf16[2,256,256]{2,1,0:T(8,128)(2,1)S(1)} collective-permute-done((bf16[2,256,256]{2,1,0:T(8,128)(2,1)}, bf16[2,256,256]{2,1,0:T(8,128)(2,1)S(1)}, u32[]{:S(2)}, u32[]{:S(2)}) %collective-permute-start) | collective-permute-done | bytes 262176 | tf_op jit(solution)/shard_map/ppermute | solution.py:352
  59.4 2.9 %collective-permute-start.2 = (bf16[2,256,256]{2,1,0:T(8,128)(2,1)}, bf16[2,256,256]{2,1,0:T(8,128)(2,1)S(1)}, u32[]{:S(2)}, u32[]{:S(2)}) collective-permute-start(bf16[2,256,256]{2,1,0:T(8,128)(2,1)} %get-tuple-element.39), channel_id=1, source_target_pairs={{0,64},{64,128},{128,192},{192,256},{256,320},{320,384},{384,448},... | collective-permute-start | bytes 786440 | tf_op jit(solution)/shard_map/ppermute | solution.py:352
  62.3 0.1 pad_add_fusion.place_ref
  62.4 0.2 collective-permute-done.1.above_ref
  62.6 4.0 %collective-permute-start.3 = (bf16[2,256,256]{2,1,0:T(8,128)(2,1)}, bf16[2,256,256]{2,1,0:T(8,128)(2,1)S(1)}, u32[]{:S(2)}, u32[]{:S(2)}) collective-permute-start(bf16[2,256,256]{2,1,0:T(8,128)(2,1)} %get-tuple-element.38), channel_id=1, source_target_pairs={{0,448},{64,0},{128,64},{192,128},{256,192},{320,256},{384,320},{4... | collective-permute-start | bytes 786440 | tf_op jit(solution)/shard_map/ppermute | solution.py:353
  66.6 0.0 copy-done
  66.6 0.0 copy-done.3
  66.6 0.0 copy-start.1
  66.6 1.2 copy-done.1
  67.8 2.7 %shard_map.86 = (bf16[512,2048]{1,0:T(8,128)(2,1)S(1)}, bf16[512,256]{1,0:T(8,128)(2,1)S(1)}) custom-call(bf16[512,2048]{1,0:T(8,128)(2,1)S(1)} %copy-done, f32[1,2048]{1,0:T(1,128)S(1)} %bitcast.11, bf16[2048,256]{1,0:T(8,128)(2,1)S(1)} %copy-done.1, f32[2,32,512]{2,1,0:T(8,128)S(1)} %pad_maximum_fusion.turn_ref), custom_call_target="tpu_custom_call" | custom-call | flops 536870912 | bytes 3284992 | tf_op jit(solution)/shard_map/pallas_call | solution.py:318
  70.5 2.4 %shard_map.88.k_ref = bf16[512,256]{1,0:T(8,128)(2,1)S(1)} custom-call(s32[4]{0:T(128)S(1)} %pad_add_fusion.place_ref, bf16[512,2048]{1,0:T(8,128)(2,1)S(1)} %get-tuple-element.21.normed_ref, bf16[4,256,512]{2,1,0:T(8,128)(2,1)S(1)} %bitcast.9, bf16[2,256,256]{2,1,0:T(8,128)(2,1)S(1)} %collective-permute-done.below_ref, ...), custom_call_target="tpu_custom_call" | custom-call | flops 536870912 | bytes 3801104 | tf_op jit(solution)/shard_map/pallas_call | solution.py:318
  72.9 0.0 copy-start.2
  72.9 0.0 collective-permute-done.2.below_ref
  72.9 3.1 %collective-permute-start.4 = (bf16[512,256]{1,0:T(8,128)(2,1)S(1)}, bf16[512,256]{1,0:T(8,128)(2,1)S(1)}, u32[]{:S(2)}, u32[]{:S(2)}) collective-permute-start(bf16[512,256]{1,0:T(8,128)(2,1)S(1)} %shard_map.88.k_ref), channel_id=1, source_target_pairs={{0,8},{8,16},{16,24},{24,32},{32,40},{40,48},{48,56},{56,64},{64,7... | collective-permute-start | bytes 786440 | tf_op jit(solution)/shard_map/ppermute | solution.py:377
  76.1 0.0 collective-permute-done.3.above_ref
  76.1 1.8 %shard_map.89.v_ref = bf16[512,256]{1,0:T(8,128)(2,1)S(1)} custom-call(s32[4]{0:T(128)S(1)} %pad_add_fusion.place_ref, bf16[512,2048]{1,0:T(8,128)(2,1)S(1)} %get-tuple-element.21.normed_ref, bf16[4,256,512]{2,1,0:T(8,128)(2,1)S(1)} %bitcast.10, bf16[2,256,256]{2,1,0:T(8,128)(2,1)S(1)} %collective-permute-done.2.below_ref, ...), custom_call_target="tpu_custom_call" | custom-call | flops 536870912 | bytes 3670032 | tf_op jit(solution)/shard_map/pallas_call | solution.py:318
  77.8 2.4 %collective-permute-start.5 = (bf16[512,256]{1,0:T(8,128)(2,1)S(1)}, bf16[512,256]{1,0:T(8,128)(2,1)S(1)}, u32[]{:S(2)}, u32[]{:S(2)}) collective-permute-start(bf16[512,256]{1,0:T(8,128)(2,1)S(1)} %shard_map.89.v_ref), channel_id=1, source_target_pairs={{0,8},{8,16},{16,24},{24,32},{32,40},{40,48},{48,56},{56,64},{64,7... | collective-permute-start | bytes 786440 | tf_op jit(solution)/shard_map/ppermute | solution.py:378
  80.3 2.9 %collective-permute-done.4.k_ref = bf16[512,256]{1,0:T(8,128)(2,1)S(1)} collective-permute-done((bf16[512,256]{1,0:T(8,128)(2,1)S(1)}, bf16[512,256]{1,0:T(8,128)(2,1)S(1)}, u32[]{:S(2)}, u32[]{:S(2)}) %collective-permute-start.4) | collective-permute-done | bytes 262176 | tf_op jit(solution)/shard_map/ppermute | solution.py:377
  83.2 5.0 %collective-permute-start.6 = (bf16[512,256]{1,0:T(8,128)(2,1)S(1)}, bf16[512,256]{1,0:T(8,128)(2,1)S(1)}, u32[]{:S(2)}, u32[]{:S(2)}) collective-permute-start(bf16[512,256]{1,0:T(8,128)(2,1)S(1)} %collective-permute-done.4.k_ref), channel_id=1, source_target_pairs={{0,8},{8,16},{16,24},{24,32},{32,40},{40,48},{48,56},{56,64},{64,7... | collective-permute-start | bytes 786440 | tf_op jit(solution)/shard_map/ppermute | solution.py:377
  88.2 0.7 collective-permute-done.5.v_ref
  88.9 4.9 %collective-permute-start.7 = (bf16[512,256]{1,0:T(8,128)(2,1)S(1)}, bf16[512,256]{1,0:T(8,128)(2,1)S(1)}, u32[]{:S(2)}, u32[]{:S(2)}) collective-permute-start(bf16[512,256]{1,0:T(8,128)(2,1)S(1)} %collective-permute-done.5.v_ref), channel_id=1, source_target_pairs={{0,8},{8,16},{16,24},{24,32},{32,40},{40,48},{48,56},{56,64},{64,7... | collective-permute-start | bytes 786440 | tf_op jit(solution)/shard_map/ppermute | solution.py:378
  93.8 0.8 collective-permute-done.6.k_ref
  94.6 5.6 %collective-permute-start.8 = (bf16[512,256]{1,0:T(8,128)(2,1)S(1)}, bf16[512,256]{1,0:T(8,128)(2,1)S(1)}, u32[]{:S(2)}, u32[]{:S(2)}) collective-permute-start(bf16[512,256]{1,0:T(8,128)(2,1)S(1)} %collective-permute-done.6.k_ref), channel_id=1, source_target_pairs={{0,8},{8,16},{16,24},{24,32},{32,40},{40,48},{48,56},{56,64},{64,7... | collective-permute-start | bytes 786440 | tf_op jit(solution)/shard_map/ppermute | solution.py:377
  100.2 0.0 collective-permute-done.12.refs_1_
  100.2 1.9 %collective-permute-start.15 = (bf16[256,2048]{1,0:T(8,128)(2,1)S(1)}, bf16[256,2048]{1,0:T(8,128)(2,1)S(1)}, u32[]{:S(2)}, u32[]{:S(2)}) collective-permute-start(bf16[256,2048]{1,0:T(8,128)(2,1)S(1)} %copy-done.2), channel_id=1, source_target_pairs={{0,1},{1,0},{2,3},{3,2},{4,5},{5,4},{6,7},{7,6},{8,9},{9,8},{10,11... | collective-permute-start | bytes 3145736 | tf_op jit(solution)/shard_map/ppermute | solution.py:360
  102.1 0.0 collective-permute-done.13.refs_2_
  102.2 2.4 %collective-permute-start.16 = (bf16[256,2048]{1,0:T(8,128)(2,1)}, bf16[256,2048]{1,0:T(8,128)(2,1)S(1)}, u32[]{:S(2)}, u32[]{:S(2)}) collective-permute-start(bf16[256,2048]{1,0:T(8,128)(2,1)} %collective-permute-done.12.refs_1_), channel_id=1, source_target_pairs={{0,1},{1,0},{2,3},{3,2},{4,5},{5,4},{6,7},{7,6},{8,9},{9,8},{10,11... | collective-permute-start | bytes 3145736 | tf_op jit(solution)/shard_map/ppermute | solution.py:360
  104.6 0.0 collective-permute-done.14.refs_3_
  104.6 1.9 %collective-permute-start.17 = (bf16[256,2048]{1,0:T(8,128)(2,1)}, bf16[256,2048]{1,0:T(8,128)(2,1)}, u32[]{:S(2)}, u32[]{:S(2)}) collective-permute-start(bf16[256,2048]{1,0:T(8,128)(2,1)} %collective-permute-done.13.refs_2_), channel_id=1, source_target_pairs={{0,1},{1,0},{2,3},{3,2},{4,5},{5,4},{6,7},{7,6},{8,9},{9,8},{10,11... | collective-permute-start | bytes 3145736 | tf_op jit(solution)/shard_map/ppermute | solution.py:360
  106.5 0.0 collective-permute-done.7.v_ref
  106.5 2.4 %collective-permute-start.18 = (bf16[256,2048]{1,0:T(8,128)(2,1)}, bf16[256,2048]{1,0:T(8,128)(2,1)}, u32[]{:S(2)}, u32[]{:S(2)}) collective-permute-start(bf16[256,2048]{1,0:T(8,128)(2,1)} %collective-permute-done.14.refs_3_), channel_id=1, source_target_pairs={{0,1},{1,0},{2,3},{3,2},{4,5},{5,4},{6,7},{7,6},{8,9},{9,8},{10,11... | collective-permute-start | bytes 3145736 | tf_op jit(solution)/shard_map/ppermute | solution.py:360
  108.9 0.0 collective-permute-done.8.k_ref
  108.9 1.9 %collective-permute-start.9 = (bf16[512,256]{1,0:T(8,128)(2,1)S(1)}, bf16[512,256]{1,0:T(8,128)(2,1)S(1)}, u32[]{:S(2)}, u32[]{:S(2)}) collective-permute-start(bf16[512,256]{1,0:T(8,128)(2,1)S(1)} %collective-permute-done.7.v_ref), channel_id=1, source_target_pairs={{0,8},{8,16},{16,24},{24,32},{32,40},{40,48},{48,56},{56,64},{64,7... | collective-permute-start | bytes 786440 | tf_op jit(solution)/shard_map/ppermute | solution.py:378
  110.9 8.2 %collective-permute-done.9.v_ref = bf16[512,256]{1,0:T(8,128)(2,1)S(1)} collective-permute-done((bf16[512,256]{1,0:T(8,128)(2,1)S(1)}, bf16[512,256]{1,0:T(8,128)(2,1)S(1)}, u32[]{:S(2)}, u32[]{:S(2)}) %collective-permute-start.9) | collective-permute-done | bytes 262176 | tf_op jit(solution)/shard_map/ppermute | solution.py:378
  119.1 3.4 %collective-permute-start.10 = (bf16[512,256]{1,0:T(8,128)(2,1)S(1)}, bf16[512,256]{1,0:T(8,128)(2,1)S(1)}, u32[]{:S(2)}, u32[]{:S(2)}) collective-permute-start(bf16[512,256]{1,0:T(8,128)(2,1)S(1)} %collective-permute-done.8.k_ref), channel_id=1, source_target_pairs={{0,8},{8,16},{16,24},{24,32},{32,40},{40,48},{48,56},{56,64},{64,7... | collective-permute-start | bytes 786440 | tf_op jit(solution)/shard_map/ppermute | solution.py:377
  122.5 5.8 %collective-permute-done.10.k_ref = bf16[512,256]{1,0:T(8,128)(2,1)S(1)} collective-permute-done((bf16[512,256]{1,0:T(8,128)(2,1)S(1)}, bf16[512,256]{1,0:T(8,128)(2,1)S(1)}, u32[]{:S(2)}, u32[]{:S(2)}) %collective-permute-start.10) | collective-permute-done | bytes 262176 | tf_op jit(solution)/shard_map/ppermute | solution.py:377
  128.3 4.9 %collective-permute-start.11 = (bf16[512,256]{1,0:T(8,128)(2,1)S(1)}, bf16[512,256]{1,0:T(8,128)(2,1)S(1)}, u32[]{:S(2)}, u32[]{:S(2)}) collective-permute-start(bf16[512,256]{1,0:T(8,128)(2,1)S(1)} %collective-permute-done.9.v_ref), channel_id=1, source_target_pairs={{0,8},{8,16},{16,24},{24,32},{32,40},{40,48},{48,56},{56,64},{64,7... | collective-permute-start | bytes 786440 | tf_op jit(solution)/shard_map/ppermute | solution.py:378
  133.2 3.5 %shard_map.90 = (f32[2048,128]{1,0:T(8,128)S(1)}, f32[2048,128]{1,0:T(8,128)S(1)}, f32[512,256]{1,0:T(8,128)S(1)}) custom-call(bf16[512,256]{1,0:T(8,128)(2,1)S(1)} %get-tuple-element.20.q_ref, bf16[512,256]{1,0:T(8,128)(2,1)S(1)} %shard_map.88.k_ref, bf16[512,256]{1,0:T(8,128)(2,1)S(1)} %shard_map.89.v_ref), custom_call_target="tpu_custom_call" | custom-call | flops 536870912 | bytes 786432 | tf_op jit(solution)/shard_map/pallas_call | solution.py:318
  136.7 3.0 %shard_map.91 = (f32[2048,128]{1,0:T(8,128)S(1)}, f32[2048,128]{1,0:T(8,128)S(1)}, f32[512,256]{1,0:T(8,128)S(1)}) custom-call(s32[4]{0:T(128)S(1)} %pad_add_fusion.place_ref, bf16[512,256]{1,0:T(8,128)(2,1)S(1)} %get-tuple-element.20.q_ref, f32[2048,128]{1,0:T(8,128)S(1)} %get-tuple-element.22.max_ref, f32[2048,128]{1,0:T(8,128)S(1)} %get-tuple-element.23.sum_ref, ...), custom_call_target="tpu_custom_call" | custom-call | flops 268435456 | bytes 3407888 | tf_op jit(solution)/shard_map/pallas_call | solution.py:318
  139.7 2.8 %shard_map.92 = (f32[2048,128]{1,0:T(8,128)S(1)}, f32[2048,128]{1,0:T(8,128)S(1)}, f32[512,256]{1,0:T(8,128)S(1)}) custom-call(s32[4]{0:T(128)S(1)} %pad_add_fusion.place_ref, bf16[512,256]{1,0:T(8,128)(2,1)S(1)} %get-tuple-element.20.q_ref, f32[2048,128]{1,0:T(8,128)S(1)} %get-tuple-element.25.max_ref, f32[2048,128]{1,0:T(8,128)S(1)} %get-tuple-element.26.sum_ref, ...), custom_call_target="tpu_custom_call" | custom-call | flops 268435456 | bytes 3407888 | tf_op jit(solution)/shard_map/pallas_call | solution.py:318
  142.5 2.8 %shard_map.93 = (f32[2048,128]{1,0:T(8,128)S(1)}, f32[2048,128]{1,0:T(8,128)S(1)}, f32[512,256]{1,0:T(8,128)S(1)}) custom-call(s32[4]{0:T(128)S(1)} %pad_add_fusion.place_ref, bf16[512,256]{1,0:T(8,128)(2,1)S(1)} %get-tuple-element.20.q_ref, f32[2048,128]{1,0:T(8,128)S(1)} %get-tuple-element.28.max_ref, f32[2048,128]{1,0:T(8,128)S(1)} %get-tuple-element.29.sum_ref, ...), custom_call_target="tpu_custom_call" | custom-call | flops 268435456 | bytes 3407888 | tf_op jit(solution)/shard_map/pallas_call | solution.py:318
  145.2 2.2 %shard_map.94 = (bf16[2048,128]{1,0:T(8,128)(2,1)S(1)}, f32[512,256]{1,0:T(8,128)S(1)}, f32[512,256]{1,0:T(8,128)S(1)}, f32[512,128]{1,0:T(8,128)S(1)}) custom-call(s32[4]{0:T(128)S(1)} %pad_add_fusion.place_ref, bf16[512,256]{1,0:T(8,128)(2,1)S(1)} %get-tuple-element.20.q_ref, f32[2048,128]{1,0:T(8,128)S(1)} %get-tuple-element.31.max_ref, ...), custom_call_target="tpu_custom_call" | custom-call | flops 134217728 | bytes 3145744 | tf_op jit(solution)/shard_map/pallas_call | solution.py:318
  147.5 0.0 copy-start.4
  147.5 0.0 collective-permute-done.11.v_ref
  147.5 1.9 %shard_map.95 = bf16[512,256]{1,0:T(8,128)(2,1)} custom-call(bf16[2048,128]{1,0:T(8,128)(2,1)S(1)} %get-tuple-element.34.p_ref, bf16[512,256]{1,0:T(8,128)(2,1)S(1)} %collective-permute-done.11.v_ref, f32[512,256]{1,0:T(8,128)S(1)} %get-tuple-element.35.scaled_ref, f32[512,256]{1,0:T(8,128)S(1)} %get-tuple-element.36.total_ref), custom_call_target="tpu_custom_call" | custom-call | flops 134217728 | bytes 1835008 | tf_op jit(solution)/shard_map/pallas_call | solution.py:318
  149.4 4.3 %all-to-all-start.1 = ((bf16[8,64,256]{2,1,0:T(8,128)(2,1)}), bf16[8,64,256]{2,1,0:T(8,128)(2,1)S(1)}, u32[]{:S(2)}, u32[]{:S(2)}) async-start(bf16[8,64,256]{2,1,0:T(8,128)(2,1)} %bitcast.6), calls=%async_computation.1 | async-start | bytes 524288 | tf_op jit(solution)/shard_map/all_to_all | solution.py:443
  153.7 0.9 copy-done.6
  154.7 1.2 shard_map.97
  155.9 0.0 collective-permute-done.15.refs_4_
  155.9 0.0 collective-permute-done.16.refs_5_
  155.9 0.0 collective-permute-done.17.refs_6_
  155.9 0.0 collective-permute-done.18.refs_7_
  155.9 5.3 %all-to-all-done.1.att_ref = bf16[8,64,256]{2,1,0:T(8,128)(2,1)S(1)} async-done(((bf16[8,64,256]{2,1,0:T(8,128)(2,1)}), bf16[8,64,256]{2,1,0:T(8,128)(2,1)S(1)}, u32[]{:S(2)}, u32[]{:S(2)}) %all-to-all-start.1) | async-done | bytes 262176 | tf_op jit(solution)/shard_map/all_to_all | solution.py:443
  161.2 5.1 %shard_map.96 = bf16[64,2048]{1,0:T(8,128)(2,1)} custom-call(s32[4]{0:T(128)S(1)} %pad_add_fusion.place_ref, bf16[8,64,256]{2,1,0:T(8,128)(2,1)S(1)} %all-to-all-done.1.att_ref, bf16[256,2048]{1,0:T(8,128)(2,1)S(1)} %copy-done.2, bf16[256,2048]{1,0:T(8,128)(2,1)} %collective-permute-done.12.refs_1_, bf16[256,2048]{1,0:T(8,128)(2,1)} %collective-permute-done.13.refs_2_, ...), custom_call_target="tpu_custom_call" | custom-call | flops 536870912 | bytes 8658960 | tf_op jit(solution)/shard_map/pallas_call | solution.py:318
  (10 shorter events, 0.0 us)
Async XLA Ops:
  2.5 64.1 %copy-start = (bf16[512,2048]{1,0:T(8,128)(2,1)S(1)}, bf16[512,2048]{1,0:T(8,128)(2,1)}, u32[]{:S(2)}) copy-start(bf16[512,2048]{1,0:T(8,128)(2,1)} %hidden_ref.1) | copy-start | bytes 6291460
  2.5 64.1 %copy-start.3 = (f32[2048]{0:T(1024)S(1)}, f32[2048]{0:T(1024)}, u32[]{:S(2)}) copy-start(f32[2048]{0:T(1024)} %param.8) | copy-start | bytes 24580
  2.5 46.3 %all-to-all-start = ((bf16[32,32,512]{2,1,0:T(8,128)(2,1)}), bf16[32,32,512]{2,1,0:T(8,128)(2,1)S(1)}, u32[]{:S(2)}, u32[]{:S(2)}) async-start(bf16[32,32,512]{2,1,0:T(8,128)(2,1)} %shard_map.87), calls=%async_computation | async-start | bytes 2097152 | tf_op jit(solution)/shard_map/all_to_all | solution.py:348
  18.6 81.6 %collective-permute-start.12 = (bf16[256,2048]{1,0:T(8,128)(2,1)}, bf16[256,2048]{1,0:T(8,128)(2,1)}, u32[]{:S(2)}, u32[]{:S(2)}) collective-permute-start(bf16[256,2048]{1,0:T(8,128)(2,1)} %refs_0_.1), channel_id=1, source_target_pairs={{0,2},{2,4},{4,6},{6,0},{1,3},{3,5},{5,7},{7,1},{8,10},{10,12},{12... | collective-permute-start | bytes 3145736 | tf_op jit(solution)/shard_map/ppermute | solution.py:358
  22.0 80.2 %collective-permute-start.13 = (bf16[256,2048]{1,0:T(8,128)(2,1)}, bf16[256,2048]{1,0:T(8,128)(2,1)}, u32[]{:S(2)}, u32[]{:S(2)}) collective-permute-start(bf16[256,2048]{1,0:T(8,128)(2,1)} %refs_0_.1), channel_id=1, source_target_pairs={{0,6},{2,0},{4,2},{6,4},{1,7},{3,1},{5,3},{7,5},{8,14},{10,8},{12,... | collective-permute-start | bytes 3145736 | tf_op jit(solution)/shard_map/ppermute | solution.py:358
  25.6 78.9 %collective-permute-start.14 = (bf16[256,2048]{1,0:T(8,128)(2,1)}, bf16[256,2048]{1,0:T(8,128)(2,1)}, u32[]{:S(2)}, u32[]{:S(2)}) collective-permute-start(bf16[256,2048]{1,0:T(8,128)(2,1)} %refs_0_.1), channel_id=1, source_target_pairs={{0,4},{2,6},{4,0},{6,2},{1,5},{3,7},{5,1},{7,3},{8,12},{10,14},{12... | collective-permute-start | bytes 3145736 | tf_op jit(solution)/shard_map/ppermute | solution.py:358
  49.7 9.7 %collective-permute-start = (bf16[2,256,256]{2,1,0:T(8,128)(2,1)}, bf16[2,256,256]{2,1,0:T(8,128)(2,1)S(1)}, u32[]{:S(2)}, u32[]{:S(2)}) collective-permute-start(bf16[2,256,256]{2,1,0:T(8,128)(2,1)} %get-tuple-element.41), channel_id=1, source_target_pairs={{0,64},{64,128},{128,192},{192,256},{256,320},{320,384},{384,448},... | collective-permute-start | bytes 786440 | tf_op jit(solution)/shard_map/ppermute | solution.py:352
  53.8 8.8 %collective-permute-start.1 = (bf16[2,256,256]{2,1,0:T(8,128)(2,1)}, bf16[2,256,256]{2,1,0:T(8,128)(2,1)}, u32[]{:S(2)}, u32[]{:S(2)}) collective-permute-start(bf16[2,256,256]{2,1,0:T(8,128)(2,1)} %get-tuple-element.40), channel_id=1, source_target_pairs={{0,448},{64,0},{128,64},{192,128},{256,192},{320,256},{384,320},{4... | collective-permute-start | bytes 786440 | tf_op jit(solution)/shard_map/ppermute | solution.py:353
  59.4 13.5 %collective-permute-start.2 = (bf16[2,256,256]{2,1,0:T(8,128)(2,1)}, bf16[2,256,256]{2,1,0:T(8,128)(2,1)S(1)}, u32[]{:S(2)}, u32[]{:S(2)}) collective-permute-start(bf16[2,256,256]{2,1,0:T(8,128)(2,1)} %get-tuple-element.39), channel_id=1, source_target_pairs={{0,64},{64,128},{128,192},{192,256},{256,320},{320,384},{384,448},... | collective-permute-start | bytes 786440 | tf_op jit(solution)/shard_map/ppermute | solution.py:352
  62.6 13.5 %collective-permute-start.3 = (bf16[2,256,256]{2,1,0:T(8,128)(2,1)}, bf16[2,256,256]{2,1,0:T(8,128)(2,1)S(1)}, u32[]{:S(2)}, u32[]{:S(2)}) collective-permute-start(bf16[2,256,256]{2,1,0:T(8,128)(2,1)} %get-tuple-element.38), channel_id=1, source_target_pairs={{0,448},{64,0},{128,64},{192,128},{256,192},{320,256},{384,320},{4... | collective-permute-start | bytes 786440 | tf_op jit(solution)/shard_map/ppermute | solution.py:353
  66.6 1.2 copy-start.1
  72.9 27.3 %copy-start.2 = (bf16[256,2048]{1,0:T(8,128)(2,1)S(1)}, bf16[256,2048]{1,0:T(8,128)(2,1)}, u32[]{:S(2)}) copy-start(bf16[256,2048]{1,0:T(8,128)(2,1)} %refs_0_.1) | copy-start | bytes 3145732
  72.9 10.3 %collective-permute-start.4 = (bf16[512,256]{1,0:T(8,128)(2,1)S(1)}, bf16[512,256]{1,0:T(8,128)(2,1)S(1)}, u32[]{:S(2)}, u32[]{:S(2)}) collective-permute-start(bf16[512,256]{1,0:T(8,128)(2,1)S(1)} %shard_map.88.k_ref), channel_id=1, source_target_pairs={{0,8},{8,16},{16,24},{24,32},{32,40},{40,48},{48,56},{56,64},{64,7... | collective-permute-start | bytes 786440 | tf_op jit(solution)/shard_map/ppermute | solution.py:377
  77.8 11.1 %collective-permute-start.5 = (bf16[512,256]{1,0:T(8,128)(2,1)S(1)}, bf16[512,256]{1,0:T(8,128)(2,1)S(1)}, u32[]{:S(2)}, u32[]{:S(2)}) collective-permute-start(bf16[512,256]{1,0:T(8,128)(2,1)S(1)} %shard_map.89.v_ref), channel_id=1, source_target_pairs={{0,8},{8,16},{16,24},{24,32},{32,40},{40,48},{48,56},{56,64},{64,7... | collective-permute-start | bytes 786440 | tf_op jit(solution)/shard_map/ppermute | solution.py:378
  83.2 11.4 %collective-permute-start.6 = (bf16[512,256]{1,0:T(8,128)(2,1)S(1)}, bf16[512,256]{1,0:T(8,128)(2,1)S(1)}, u32[]{:S(2)}, u32[]{:S(2)}) collective-permute-start(bf16[512,256]{1,0:T(8,128)(2,1)S(1)} %collective-permute-done.4.k_ref), channel_id=1, source_target_pairs={{0,8},{8,16},{16,24},{24,32},{32,40},{40,48},{48,56},{56,64},{64,7... | collective-permute-start | bytes 786440 | tf_op jit(solution)/shard_map/ppermute | solution.py:377
  88.9 17.6 %collective-permute-start.7 = (bf16[512,256]{1,0:T(8,128)(2,1)S(1)}, bf16[512,256]{1,0:T(8,128)(2,1)S(1)}, u32[]{:S(2)}, u32[]{:S(2)}) collective-permute-start(bf16[512,256]{1,0:T(8,128)(2,1)S(1)} %collective-permute-done.5.v_ref), channel_id=1, source_target_pairs={{0,8},{8,16},{16,24},{24,32},{32,40},{40,48},{48,56},{56,64},{64,7... | collective-permute-start | bytes 786440 | tf_op jit(solution)/shard_map/ppermute | solution.py:378
  94.6 14.3 %collective-permute-start.8 = (bf16[512,256]{1,0:T(8,128)(2,1)S(1)}, bf16[512,256]{1,0:T(8,128)(2,1)S(1)}, u32[]{:S(2)}, u32[]{:S(2)}) collective-permute-start(bf16[512,256]{1,0:T(8,128)(2,1)S(1)} %collective-permute-done.6.k_ref), channel_id=1, source_target_pairs={{0,8},{8,16},{16,24},{24,32},{32,40},{40,48},{48,56},{56,64},{64,7... | collective-permute-start | bytes 786440 | tf_op jit(solution)/shard_map/ppermute | solution.py:377
  100.2 55.7 %collective-permute-start.15 = (bf16[256,2048]{1,0:T(8,128)(2,1)S(1)}, bf16[256,2048]{1,0:T(8,128)(2,1)S(1)}, u32[]{:S(2)}, u32[]{:S(2)}) collective-permute-start(bf16[256,2048]{1,0:T(8,128)(2,1)S(1)} %copy-done.2), channel_id=1, source_target_pairs={{0,1},{1,0},{2,3},{3,2},{4,5},{5,4},{6,7},{7,6},{8,9},{9,8},{10,11... | collective-permute-start | bytes 3145736 | tf_op jit(solution)/shard_map/ppermute | solution.py:360
  102.2 53.8 %collective-permute-start.16 = (bf16[256,2048]{1,0:T(8,128)(2,1)}, bf16[256,2048]{1,0:T(8,128)(2,1)S(1)}, u32[]{:S(2)}, u32[]{:S(2)}) collective-permute-start(bf16[256,2048]{1,0:T(8,128)(2,1)} %collective-permute-done.12.refs_1_), channel_id=1, source_target_pairs={{0,1},{1,0},{2,3},{3,2},{4,5},{5,4},{6,7},{7,6},{8,9},{9,8},{10,11... | collective-permute-start | bytes 3145736 | tf_op jit(solution)/shard_map/ppermute | solution.py:360
  104.6 51.3 %collective-permute-start.17 = (bf16[256,2048]{1,0:T(8,128)(2,1)}, bf16[256,2048]{1,0:T(8,128)(2,1)}, u32[]{:S(2)}, u32[]{:S(2)}) collective-permute-start(bf16[256,2048]{1,0:T(8,128)(2,1)} %collective-permute-done.13.refs_2_), channel_id=1, source_target_pairs={{0,1},{1,0},{2,3},{3,2},{4,5},{5,4},{6,7},{7,6},{8,9},{9,8},{10,11... | collective-permute-start | bytes 3145736 | tf_op jit(solution)/shard_map/ppermute | solution.py:360
  106.5 49.4 %collective-permute-start.18 = (bf16[256,2048]{1,0:T(8,128)(2,1)}, bf16[256,2048]{1,0:T(8,128)(2,1)}, u32[]{:S(2)}, u32[]{:S(2)}) collective-permute-start(bf16[256,2048]{1,0:T(8,128)(2,1)} %collective-permute-done.14.refs_3_), channel_id=1, source_target_pairs={{0,1},{1,0},{2,3},{3,2},{4,5},{5,4},{6,7},{7,6},{8,9},{9,8},{10,11... | collective-permute-start | bytes 3145736 | tf_op jit(solution)/shard_map/ppermute | solution.py:360
  108.9 10.1 %collective-permute-start.9 = (bf16[512,256]{1,0:T(8,128)(2,1)S(1)}, bf16[512,256]{1,0:T(8,128)(2,1)S(1)}, u32[]{:S(2)}, u32[]{:S(2)}) collective-permute-start(bf16[512,256]{1,0:T(8,128)(2,1)S(1)} %collective-permute-done.7.v_ref), channel_id=1, source_target_pairs={{0,8},{8,16},{16,24},{24,32},{32,40},{40,48},{48,56},{56,64},{64,7... | collective-permute-start | bytes 786440 | tf_op jit(solution)/shard_map/ppermute | solution.py:378
  119.1 9.2 %collective-permute-start.10 = (bf16[512,256]{1,0:T(8,128)(2,1)S(1)}, bf16[512,256]{1,0:T(8,128)(2,1)S(1)}, u32[]{:S(2)}, u32[]{:S(2)}) collective-permute-start(bf16[512,256]{1,0:T(8,128)(2,1)S(1)} %collective-permute-done.8.k_ref), channel_id=1, source_target_pairs={{0,8},{8,16},{16,24},{24,32},{32,40},{40,48},{48,56},{56,64},{64,7... | collective-permute-start | bytes 786440 | tf_op jit(solution)/shard_map/ppermute | solution.py:377
  128.3 19.2 %collective-permute-start.11 = (bf16[512,256]{1,0:T(8,128)(2,1)S(1)}, bf16[512,256]{1,0:T(8,128)(2,1)S(1)}, u32[]{:S(2)}, u32[]{:S(2)}) collective-permute-start(bf16[512,256]{1,0:T(8,128)(2,1)S(1)} %collective-permute-done.9.v_ref), channel_id=1, source_target_pairs={{0,8},{8,16},{16,24},{24,32},{32,40},{40,48},{48,56},{56,64},{64,7... | collective-permute-start | bytes 786440 | tf_op jit(solution)/shard_map/ppermute | solution.py:378
  147.5 1.9 %copy-start.5 = (f32[512,128]{1,0:T(8,128)}, f32[512,128]{1,0:T(8,128)S(1)}, u32[]{:S(2)}) copy-start(f32[512,128]{1,0:T(8,128)S(1)} %get-tuple-element.37.lw_ref) | copy-start | bytes 786436
  147.5 13.8 %copy-start.4 = (f32[2048]{0:T(1024)S(1)}, f32[2048]{0:T(1024)}, u32[]{:S(2)}) copy-start(f32[2048]{0:T(1024)} %param.13) | copy-start | bytes 24580
  149.4 11.8 %all-to-all-start.1 = ((bf16[8,64,256]{2,1,0:T(8,128)(2,1)}), bf16[8,64,256]{2,1,0:T(8,128)(2,1)S(1)}, u32[]{:S(2)}, u32[]{:S(2)}) async-start(bf16[8,64,256]{2,1,0:T(8,128)(2,1)} %bitcast.6), calls=%async_computation.1 | async-start | bytes 524288 | tf_op jit(solution)/shard_map/all_to_all | solution.py:443
  153.7 0.9 copy-start.6
